TPU v7x, 32 devices: a whole 2x2x4 slice. The times are simulated.
32 devices in a mesh: dp: 4 (over y, x), kv: 4 (over z), tp: 2 (over core).
Axes of the slice: x: 2, y: 2, z: 4, core: 2. Of those that a mesh axis runs over, the one named last changes fastest.
Arguments:
- tokens: bfloat16 [64, 16, 2048], P('dp'), may hold values from -6 to 6
- norm_gain: float32 [2048], replicated, may hold values from 0.1 to 1.9
- query_weight: bfloat16 [2048, 1024], P(None, 'tp'), may hold values from -0.125 to 0.125
- key_weight: bfloat16 [2048, 256], P(None, 'tp'), may hold values from -0.125 to 0.125
- value_weight: bfloat16 [2048, 256], P(None, 'tp'), may hold values from -0.125 to 0.125
- forget_weight: bfloat16 [2048, 8], replicated, may hold values from -0.125 to 0.125
- forget_bias: float32 [8], replicated, may hold values from 0 to 4
- query_gain: float32 [128], replicated, may hold values from 0.1 to 1.9
- key_gain: float32 [128], replicated, may hold values from 0.1 to 1.9
- output_weight: bfloat16 [1024, 2048], P('tp', 'kv'), may hold values from -0.1875 to 0.1875
- cache_keys: bfloat16 [64, 1024, 2, 128], P('dp', 'kv', 'tp'), may hold values from -512 to 512
- cache_values: bfloat16 [64, 1024, 2, 128], P('dp', 'kv', 'tp'), may hold values from -6 to 6
- cache_logcum: float32 [64, 1024, 8], P('dp', 'kv', 'tp'), may hold values from -205 to 0, as said below
- pending_keys: bfloat16 [64, 4, 2, 128], P('dp', None, 'tp'), may hold values from -6 to 6
- pending_values: bfloat16 [64, 4, 2, 128], P('dp', None, 'tp'), may hold values from -6 to 6
- pending_logcum: float32 [64, 4, 8], P('dp', None, 'tp'), may hold values from -205 to 0, as said below
- lengths: int32 [64], P('dp'), may hold values from 512 to 1020, as said below
- accepted: int32 [64], P('dp'), may hold values from 1 to 4
- parents: int32 [64, 16], P('dp'), may hold values from -1 to 14, as said below
Outputs:
- result: bfloat16 [64, 16, 2048], P('dp', None, ('kv', 'tp'))
Inputs may be any that keep to these rules, and one draw needn't show every extreme that they name: Positions below lengths hold a sequence's past; the last step's accepted proposals go to positions lengths to lengths + accepted - 1. `parents`: the parent of proposal i is -1 (the last accepted token) or a proposal before i. `cache_logcum`: non-increasing along positions for every sequence and head. `pending_logcum`: the cumulative log gates at positions lengths to lengths + 3, continuing cache_logcum.
All inputs are finite; a program needn't handle non-finite values.
Results may differ from a plain program's by a relative error of at most 0.014.
Values may be sent and summed in bfloat16 or wider, within the bound.
No kernel may reach another device: no remote copies, remote signals or barrier semaphores. Data moves between devices by JAX's collectives and lax.ppermute only.
A program may use at most 128 MiB of HBM per device.

v0:
```python
import jax
import jax.numpy as jnp
from jax import lax
from jax.sharding import PartitionSpec as P

EPSILON = 1e-06
NEG_LARGE = -1e30
HIGHEST = lax.Precision.HIGHEST


def joined(shard, axis, join):
    gathered = jax.tree.map(
        lambda a, kind: lax.all_gather(a.astype(kind), axis),
        shard,
        (jnp.bfloat16, jnp.bfloat16, jnp.bfloat16),
    )

    def take(source):
        return jax.tree.map(
            lambda a, own: lax.dynamic_index_in_dim(a, source, 0, False).astype(own.dtype),
            gathered,
            shard,
        )

    return lax.fori_loop(
        1, lax.axis_size(axis), lambda source, state: join(state, take(source)), take(0)
    )


def head_norm(vectors, gain_vec):
    return (
        vectors
        * lax.rsqrt(jnp.mean(vectors * vectors, axis=-1, keepdims=True) + EPSILON)
        * gain_vec
    )


def ancestors(parents):
    node_count = parents.shape[-1]
    indices = jnp.arange(node_count, dtype=jnp.int32)
    reachable = (parents[..., None] == indices).astype(jnp.float32) + jnp.eye(
        node_count, dtype=jnp.float32
    )
    for doubling in range((node_count - 1).bit_length()):
        reachable = jnp.minimum(
            jnp.einsum("sij,sjk->sik", reachable, reachable, precision=HIGHEST), 1.0
        )
    return reachable


def join_blocks(earlier, later):
    larger = jnp.maximum(earlier[0], later[0])
    left_factor = jnp.exp(earlier[0] - larger)
    right_factor = jnp.exp(later[0] - larger)
    return (
        larger,
        earlier[1] * left_factor + later[1] * right_factor,
        earlier[2] * left_factor[..., None] + later[2] * right_factor[..., None],
    )


def to_rows(values):
    moved = jnp.swapaxes(values, 1, 2)
    return moved.reshape((moved.shape[0] * moved.shape[1],) + moved.shape[2:])


def finish_rows(cache_max, cache_sum, cache_acc, tree_max, tree_sum, tree_acc):
    overall = jnp.maximum(cache_max, tree_max)
    factor_cache = jnp.exp(cache_max - overall)
    factor_tree = jnp.exp(tree_max - overall)
    denominator = cache_sum * factor_cache + tree_sum * factor_tree
    numerator = cache_acc * factor_cache[..., None] + tree_acc * factor_tree[..., None]
    attended = (numerator / denominator[..., None]).astype(jnp.bfloat16)
    return attended.reshape(attended.shape[0], attended.shape[1] * attended.shape[2])


def shards(
    tokens,
    norm_gain,
    query_weight,
    key_weight,
    value_weight,
    forget_weight,
    forget_bias,
    query_gain,
    key_gain,
    output_weight,
    cache_keys,
    cache_values,
    cache_logcum,
    pending_keys,
    pending_values,
    pending_logcum,
    lengths,
    accepted,
    parents,
):
    seq_count, node_count, model_width = tokens.shape
    token_rows = seq_count * node_count
    head_size = query_gain.shape[0]
    query_cols = query_weight.shape[1]
    key_cols = key_weight.shape[1]
    local_heads = query_cols // head_size
    key_heads = key_cols // head_size
    sharing = local_heads // key_heads
    block_len = cache_keys.shape[1]
    most_taken = pending_keys.shape[1]
    scaling = head_size ** (-0.5)
    widened = tokens.reshape(token_rows, model_width).astype(jnp.float32)
    normed = (
        widened
        * lax.rsqrt(jnp.mean(widened * widened, axis=-1, keepdims=True) + EPSILON)
        * norm_gain
    ).astype(jnp.bfloat16)
    joined_weight = jnp.concatenate([query_weight, key_weight, value_weight], axis=1)
    summed = jnp.dot(normed, joined_weight, preferred_element_type=jnp.float32)
    query_part = head_norm(
        summed[:, :query_cols].reshape(token_rows, local_heads, head_size), query_gain
    )
    key_part = head_norm(
        summed[:, query_cols : query_cols + key_cols].reshape(token_rows, key_heads, head_size),
        key_gain,
    )
    queries = query_part.astype(jnp.bfloat16).reshape(
        seq_count, node_count, key_heads, sharing, head_size
    )
    keys_new = key_part.astype(jnp.bfloat16).reshape(seq_count, node_count, key_heads, head_size)
    values_new = (
        summed[:, query_cols + key_cols :]
        .astype(jnp.bfloat16)
        .reshape(seq_count, node_count, key_heads, head_size)
    )
    head_start = lax.axis_index("tp") * local_heads
    forget_cols = lax.dynamic_slice_in_dim(forget_weight, head_start, local_heads, 1)
    gate_bias = lax.dynamic_slice_in_dim(forget_bias, head_start, local_heads, 0)
    log_gates = jax.nn.log_sigmoid(
        jnp.dot(normed, forget_cols, preferred_element_type=jnp.float32) + gate_bias
    ).reshape(seq_count, node_count, local_heads)
    ancestry = ancestors(parents)
    choose = (jnp.arange(most_taken, dtype=jnp.int32)[None, :] == (accepted - 1)[:, None]).astype(
        jnp.float32
    )
    base_gate = jnp.einsum("sa,sah->sh", choose, pending_logcum, precision=HIGHEST)
    cumulative = base_gate[:, None, :] + jnp.einsum(
        "sij,sjh->sih", ancestry, log_gates, precision=HIGHEST
    )
    gate_rows = jnp.swapaxes(cumulative, 1, 2)
    token_place = lax.axis_index("kv") * block_len + jnp.arange(block_len, dtype=jnp.int32)
    offset = token_place[None, :] - lengths[:, None]
    inserted = (offset >= 0) & (offset < accepted[:, None])
    one_hot = (offset[..., None] == jnp.arange(most_taken, dtype=jnp.int32)) & inserted[..., None]
    hot_low = one_hot.astype(jnp.bfloat16)
    merged_keys = jnp.where(
        inserted[..., None, None],
        jnp.einsum(
            "sla,sakd->slkd", hot_low, pending_keys, preferred_element_type=jnp.float32
        ).astype(jnp.bfloat16),
        cache_keys,
    )
    merged_values = jnp.where(
        inserted[..., None, None],
        jnp.einsum(
            "sla,sakd->slkd", hot_low, pending_values, preferred_element_type=jnp.float32
        ).astype(jnp.bfloat16),
        cache_values,
    )
    log_cache = jnp.where(
        inserted[..., None],
        jnp.einsum("sla,sah->slh", one_hot.astype(jnp.float32), pending_logcum, precision=HIGHEST),
        cache_logcum,
    )
    usable = token_place[None, :] < (lengths + accepted)[:, None]
    raw_scores = jnp.einsum(
        "spkgd,slkd->skgpl", queries, merged_keys, preferred_element_type=jnp.float32
    )
    scores = (
        raw_scores.reshape(seq_count, local_heads, node_count, block_len) * scaling
        + gate_rows[..., None]
        - jnp.swapaxes(log_cache, 1, 2)[:, :, None, :]
    )
    visible = usable[:, None, None, :]
    block_max = jnp.max(jnp.where(visible, scores, NEG_LARGE), axis=-1)
    weights = jnp.where(visible, jnp.exp(scores - block_max[..., None]), 0.0)
    block_sum = jnp.sum(weights, axis=-1)
    block_acc = jnp.einsum(
        "skgpl,slkd->skgpd",
        weights.astype(jnp.bfloat16).reshape(seq_count, key_heads, sharing, node_count, block_len),
        merged_values,
        preferred_element_type=jnp.float32,
    )
    block_acc = block_acc.reshape(seq_count, local_heads, node_count, head_size)
    tree_raw = jnp.einsum(
        "spkgd,sjkd->skgpj", queries, keys_new, preferred_element_type=jnp.float32
    )
    tree_scores = (
        tree_raw.reshape(seq_count, local_heads, node_count, node_count) * scaling
        + gate_rows[..., :, None]
        - gate_rows[..., None, :]
    )
    tree_mask = ancestry[:, None] > 0.5
    tree_max = jnp.max(jnp.where(tree_mask, tree_scores, NEG_LARGE), axis=-1)
    tree_weights = jnp.where(tree_mask, jnp.exp(tree_scores - tree_max[..., None]), 0.0)
    tree_sum = jnp.sum(tree_weights, axis=-1)
    tree_acc = jnp.einsum(
        "skgpj,sjkd->skgpd",
        tree_weights.astype(jnp.bfloat16).reshape(
            seq_count, key_heads, sharing, node_count, node_count
        ),
        values_new,
        preferred_element_type=jnp.float32,
    )
    tree_acc = tree_acc.reshape(seq_count, local_heads, node_count, head_size)
    tree_max_rows = to_rows(tree_max)
    tree_sum_rows = to_rows(tree_sum)
    tree_acc_rows = to_rows(tree_acc)
    cache_max, cache_sum, cache_acc = joined((block_max, block_sum, block_acc), "kv", join_blocks)
    attended = finish_rows(
        to_rows(cache_max),
        to_rows(cache_sum),
        to_rows(cache_acc),
        tree_max_rows,
        tree_sum_rows,
        tree_acc_rows,
    )
    head_part = jnp.dot(attended, output_weight, preferred_element_type=jnp.float32)
    head_part = head_part.reshape(seq_count, node_count, output_weight.shape[1])
    return lax.psum_scatter(head_part.astype(jnp.bfloat16), "tp", scatter_dimension=2, tiled=True)


def solution(mesh):
    placed = (
        P("dp", None, None),
        P(),
        P(None, "tp"),
        P(None, "tp"),
        P(None, "tp"),
        P(),
        P(),
        P(),
        P(),
        P("tp", "kv"),
        P("dp", "kv", "tp", None),
        P("dp", "kv", "tp", None),
        P("dp", "kv", "tp"),
        P("dp", None, "tp", None),
        P("dp", None, "tp", None),
        P("dp", None, "tp"),
        P("dp"),
        P("dp"),
        P("dp", None),
    )
    return jax.shard_map(
        shards, mesh=mesh, in_specs=placed, out_specs=P("dp", None, ("kv", "tp")), check_vma=False
    )
```

profile of v0, /device:TPU:0, one launch (start us, length us, event | category | flops | bytes accessed | tf_op | source)
XLA Modules:
  0.0 88.6 jit_solution(2335608490506081253)
XLA Ops:
  6.6 0.8 fusion.90
  7.5 0.7 broadcast_subtract_fusion
  8.2 1.3 %broadcast_compare_fusion.1 = (pred[16,256]{1,0:T(8,128)(4,1)}, pred[16,256]{1,0:T(8,128)(4,1)}) fusion(s32[256]{0:T(256)S(1)} %iota_add_fusion, s32[16]{0:T(128)S(1)} %get-tuple-element.211, s32[16]{0:T(128)} %param.38, s32[16]{0:T(128)} %param.37), kind=kLoop, calls=%fused_computation.112 | loop fusion | flops 20480 | bytes 9408 | tf_op jit(solution)/shard_map/lt | solution.py:172
  9.6 1.5 %multiply_reduce_fusion = f32[16,16]{1,0:T(8,128)S(1)} fusion(bf16[16,16,2048]{2,1,0:T(8,128)(2,1)} %param.21), kind=kLoop, calls=%fused_computation.17 | loop fusion | flops 1572608 | bytes 1049600 | tf_op jit(solution)/shard_map/reduce_sum | solution.py:112
  11.1 0.8 copy.88
  12.0 1.1 %convolution_minimum_fusion.3 = f32[16,16,16]{2,1,0:T(8,128)S(1)} fusion(f32[16,16]{1,0:T(8,128)S(1)} %fusion.72, s32[16,16]{1,0:T(8,128)} %param.39), kind=kOutput, calls=%fused_computation.30 | convolution fusion | flops 802816 | bytes 18432 | tf_op jit(solution)/shard_map/sij,sjk->sik/dot_general | solution.py:46
  13.6 0.9 %broadcast_compare_fusion = (pred[16,16,16]{2,1,0:T(8,128)(4,1)}, f32[16,16,16]{2,1,0:T(8,128)}) fusion(f32[16,16,16]{2,1,0:T(8,128)S(1)} %convolution_minimum_fusion.1), kind=kOutput, calls=%fused_computation.93 | convolution fusion | flops 794624 | bytes 36864 | tf_op jit(solution)/shard_map/sij,sjk->sik/dot_general | solution.py:46
  14.6 0.3 fusion.10
  14.9 0.4 fusion.75
  15.4 2.9 %fusion.3 = f32[256,768]{1,0:T(8,128)S(1)} fusion(bf16[256,2048]{1,0:T(8,128)(2,1)S(1)} %fusion.10, bf16[2048,128]{1,0:T(8,128)(2,1)} %param.25, bf16[2048,128]{1,0:T(8,128)(2,1)} %param.24, bf16[2048,512]{1,0:T(8,128)(2,1)} %param.23), kind=kOutput, calls=%fused_computation.8 | convolution fusion | flops 814743552 | bytes 4980736 | tf_op jit(solution)/shard_map/dot_general | solution.py:116
  18.7 0.3 reduce_sum.46
  19.1 0.8 copy.85
  20.5 0.3 convolution_add_fusion
  20.8 3.1 %select_reduce_fusion.1 = (f32[16,4,16]{2,1,0:T(4,128)S(1)}, f32[16,256,16,4]{1,2,3,0:T(8,128)S(1)}) fusion(f32[16,4,256]{2,1,0:T(4,128)S(1)} %fusion.13, f32[16,4,16]{2,1,0:T(4,128)S(1)} %convolution_add_fusion, pred[16,256]{1,0:T(8,128)(4,1)} %get-tuple-element.209, f32[16,16,4,128]{3,2,1,0:T(4,128)S(1)} %reshape.401, f32[128]{0:T(128)} %param.28, ...), kind=kOutput, calls=%fused_computation.51 | convolution fusion | flops 74087424 | bytes 2740736 | tf_op jit(solution)/shard_map/spkgd,slkd->skgpl/dot_general | solution.py:173
  24.0 3.6 %convolution_convert_fusion.3 = bf16[16,4,16,128]{3,2,1,0:T(8,128)(2,1)} fusion(bf16[16,256,1,128]{3,1,2,0:T(8,128)(2,1)} %param.32, pred[16,256]{1,0:T(8,128)(4,1)} %get-tuple-element.210, f32[16,256,16,4]{1,2,3,0:T(8,128)S(1)} %get-tuple-element.218, f32[16,4,16]{2,1,0:T(4,128)S(1)} %get-tuple-element.217, f32[16,4,256]{2,1,0:T(4,128)S(1)} %fusion.13, ...), kind=kOutput, calls=%fused_computation.26 | convolution fusion | flops 73826304 | bytes 2473984 | tf_op jit(solution)/shard_map/skgpl,slkd->skgpd/dot_general | solution.py:185
  27.8 0.6 slice.32
  28.7 1.6 %select_reduce_fusion.3 = (f32[16,4,16]{2,1,0:T(4,128)S(1)}, f32[16,16,16,4]{2,1,3,0:T(8,128)S(1)}) fusion(f32[16,4,16]{2,1,0:T(4,128)S(1)} %convolution_add_fusion, pred[16,16,16]{1,2,0:T(8,128)(4,1)S(1)} %copy.92, bf16[16,16,128,1]{2,1,3,0:T(8,128)(2,1)S(1)} %bitcast.218, f32[16,16,4,128]{3,2,1,0:T(4,128)S(1)} %copy-done.3, f32[128]{0:T(128)} %param.28, ...), kind=kOutput, calls=%fused_computation.73 | convolution fusion | flops 4668416 | bytes 672256 | tf_op jit(solution)/shard_map/spkgd,sjkd->skgpj/dot_general | solution.py:192
  30.9 15.3 %all-gather = bf16[64,4,16]{2,1,0:T(4,128)(2,1)S(1)} all-gather(bf16[16,4,16]{2,1,0:T(4,128)(2,1)S(1)} %convert_element_type.163), channel_id=2, replica_groups=mesh['dp'=4,'kv'=4,'tp'=2] {'kv'}, dimensions={0}, use_global_device_ids=true | all-gather | bytes 10240 | tf_op jit(solution)/shard_map/all_gather | solution.py:13
  46.2 1.2 %select_reduce_fusion = bf16[16,4,16]{2,1,0:T(4,128)(2,1)S(1)} fusion(f32[16,256,16,4]{1,2,3,0:T(8,128)S(1)} %get-tuple-element.218, f32[16,4,16]{2,1,0:T(4,128)S(1)} %copy-done.7, f32[16,4,256]{2,1,0:T(4,128)S(1)} %fusion.13, f32[16,4,16]{2,1,0:T(4,128)S(1)} %convolution_add_fusion, pred[16,256]{1,0:T(8,128)(4,1)} %get-tuple-element.209), kind=kLoop, calls=%fused_computation.50 | loop fusion | flops 1309696 | bytes 1128448 | tf_op jit(solution)/shard_map/reduce_sum | solution.py:184
  47.4 13.9 %all-gather.1 = bf16[64,4,16]{2,1,0:T(4,128)(2,1)S(1)} all-gather(bf16[16,4,16]{2,1,0:T(4,128)(2,1)S(1)} %select_reduce_fusion), channel_id=3, replica_groups=mesh['dp'=4,'kv'=4,'tp'=2] {'kv'}, dimensions={0}, use_global_device_ids=true | all-gather | bytes 10240 | tf_op jit(solution)/shard_map/all_gather | solution.py:13
  61.4 0.6 convolution_bitcast_fusion
  62.0 1.0 %slice_convert_fusion = f32[16,4,16,128]{3,2,1,0:T(8,128)S(1)} fusion(bf16[64,4,16,128]{3,2,1,0:T(8,128)(2,1)} %all-gather.5.cloned.1.call-done), kind=kLoop, calls=%fused_computation.80 | loop fusion | flops 131072 | bytes 786432 | tf_op jit(solution)/shard_map/convert_element_type | solution.py:20
  63.0 4.6 %while.19 = (s32[]{:T(128)}, f32[16,4,16]{2,1,0:T(4,128)S(1)}, f32[16,4,16]{2,1,0:T(4,128)S(1)}, f32[16,4,16,128]{3,2,1,0:T(8,128)S(1)}, bf16[4,16,4,16]{3,2,1,0...) while((s32[]{:T(128)}, f32[16,4,16]{2,1,0:T(4,128)S(1)}, ...), condition=%wide.region_5.6_spmd, body=%wide.region_4.5_spmd.sunk | while | flops 532485 | bytes 1347727 | solution.py:25
  63.1 1.4 %fusion.112 = f32[16,4,16,128]{3,2,1,0:T(8,128)S(1)} fusion(f32[16,4,16,128]{3,2,1,0:T(8,128)S(1)} %get-tuple-element.283, f32[16,4,16]{2,1,0:T(4,128)S(1)} %get-tuple-element.268, bf16[4,16,4,16,128]{4,3,2,1,0:T(8,128)(2,1)} %get-tuple-element.296, s32[]{:T(128)S(6)} %select_n.103, f32[16,4,16]{2,1,0:T(4,128)S(1)} %get-tuple-element.269), kind=kLoop, calls=%fused_computation.1.clone.1 | loop fusion | flops 524288 | bytes 1318916 | tf_op jit(solution)/shard_map/while/body/eval_jaxpr/add | solution.py:58
  64.6 1.4 %fusion.112 = f32[16,4,16,128]{3,2,1,0:T(8,128)S(1)} fusion(f32[16,4,16,128]{3,2,1,0:T(8,128)S(1)} %get-tuple-element.283, f32[16,4,16]{2,1,0:T(4,128)S(1)} %get-tuple-element.268, bf16[4,16,4,16,128]{4,3,2,1,0:T(8,128)(2,1)} %get-tuple-element.296, s32[]{:T(128)S(6)} %select_n.103, f32[16,4,16]{2,1,0:T(4,128)S(1)} %get-tuple-element.269), kind=kLoop, calls=%fused_computation.1.clone.1 | loop fusion | flops 524288 | bytes 1318916 | tf_op jit(solution)/shard_map/while/body/eval_jaxpr/add | solution.py:58
  66.2 1.4 %fusion.112 = f32[16,4,16,128]{3,2,1,0:T(8,128)S(1)} fusion(f32[16,4,16,128]{3,2,1,0:T(8,128)S(1)} %get-tuple-element.283, f32[16,4,16]{2,1,0:T(4,128)S(1)} %get-tuple-element.268, bf16[4,16,4,16,128]{4,3,2,1,0:T(8,128)(2,1)} %get-tuple-element.296, s32[]{:T(128)S(6)} %select_n.103, f32[16,4,16]{2,1,0:T(4,128)S(1)} %get-tuple-element.269), kind=kLoop, calls=%fused_computation.1.clone.1 | loop fusion | flops 524288 | bytes 1318916 | tf_op jit(solution)/shard_map/while/body/eval_jaxpr/add | solution.py:58
  68.3 0.3 mul.253
  68.8 0.3 mul.250
  69.4 0.3 div.36
  69.7 1.0 %div.37 = f32[16,16,512]{2,1,0:T(8,128)} reshape(f32[256,4,128]{2,1,0:T(4,128)S(1)} %div.36) | data formatting | bytes 1048576 | tf_op jit(solution)/shard_map/div | solution.py:73
  70.7 2.1 %convolution_convert_fusion.2 = bf16[16,16,512]{2,1,0:T(8,128)(2,1)} fusion(bf16[512,512]{1,0:T(8,128)(2,1)S(1)} %copy-done, f32[16,16,512]{2,1,0:T(8,128)} %div.37, f32[16,16,512]{2,1,0:T(8,128)S(1)} %mul.254, f32[16,4,2,8,128]{4,3,2,1,0:T(8,128)S(1)} %convolution_bitcast_fusion, f32[16,16,512]{2,1,0:T(8,128)S(1)} %mul.251, ...), kind=kOutput, calls=%fused_computation.25 | convolution fusion | flops 135004160 | bytes 3407872 | tf_op jit(solution)/shard_map/dot_general | solution.py:225
  72.8 9.0 %reduce-scatter.2.cloned.1.call-done = bf16[16,16,256]{2,1,0:T(8,128)(2,1)} async-done(((bf16[16,16,512]{2,1,0:T(8,128)(2,1)}), bf16[16,16,256]{2,1,0:T(8,128)(2,1)}) %reduce-scatter.2.cloned.1.call-update) | async-done | bytes 131088 | tf_op jit(solution)/shard_map/reduce_scatter | solution.py:227
  (75 shorter events, 4.0 us)
Async XLA Ops:
  6.5 64.2 %copy-start = (bf16[512,512]{1,0:T(8,128)(2,1)S(1)}, bf16[512,512]{1,0:T(8,128)(2,1)}, u32[]{:S(2)}) copy-start(bf16[512,512]{1,0:T(8,128)(2,1)} %param.30) | copy-start | bytes 1572868
  6.5 8.1 %copy-start.1 = (bf16[16,16,2048]{2,1,0:T(8,128)(2,1)S(1)}, bf16[16,16,2048]{2,1,0:T(8,128)(2,1)}, u32[]{:S(2)}) copy-start(bf16[16,16,2048]{2,1,0:T(8,128)(2,1)} %param.21) | copy-start | bytes 3145732
  6.5 8.0 %copy-start.14 = (f32[8]{0:T(128)S(1)}, f32[8]{0:T(128)}, u32[]{:S(2)}) copy-start(f32[8]{0:T(128)} %param.27) | copy-start | bytes 100
  6.5 8.1 %copy-start.12 = (f32[2048]{0:T(1024)S(1)}, f32[2048]{0:T(1024)}, u32[]{:S(2)}) copy-start(f32[2048]{0:T(1024)} %param.22) | copy-start | bytes 24580
  6.5 55.5 %all-gather.5.cloned.1.call-start = ((), (), s32[]{:S(2)}) async-start(), calls=%async_computation.2 | async-start | bytes 1310720 | tf_op jit(solution)/shard_map/all_gather | solution.py:13
  9.5 5.4 %copy-start.11 = (bf16[2048,8]{0,1:T(8,128)(2,1)S(1)}, bf16[2048,8]{0,1:T(8,128)(2,1)}, u32[]{:S(2)}) copy-start(bf16[2048,8]{0,1:T(8,128)(2,1)} %param.26) | copy-start | bytes 98308
  18.3 1.9 %copy-start.9 = (f32[16,256,4]{1,2,0:T(4,128)S(1)}, f32[16,256,4]{1,2,0:T(4,128)}, u32[]{:S(2)}) copy-start(f32[16,256,4]{1,2,0:T(4,128)} %param.33) | copy-start | bytes 196612
  18.4 1.9 %copy-start.10 = (pred[16,256]{1,0:T(8,128)(4,1)S(1)}, pred[16,256]{1,0:T(8,128)(4,1)}, u32[]{:S(2)}) copy-start(pred[16,256]{1,0:T(8,128)(4,1)} %get-tuple-element.210) | copy-start | bytes 12292
  18.5 2.0 %copy-start.4 = (f32[16,16,16]{2,1,0:T(8,128)S(1)}, f32[16,16,16]{2,1,0:T(8,128)}, u32[]{:S(2)}) copy-start(f32[16,16,16]{2,1,0:T(8,128)} %get-tuple-element.214) | copy-start | bytes 49156
  20.0 3.9 %copy-start.2 = (f32[16,16,4,128]{3,2,1,0:T(4,128)}, f32[16,16,4,128]{3,2,1,0:T(4,128)S(1)}, u32[]{:S(2)}) copy-start(f32[16,16,4,128]{3,2,1,0:T(4,128)S(1)} %reshape.401) | copy-start | bytes 1572868
  23.9 4.5 %copy-start.6 = (f32[16,4,16]{2,1,0:T(4,128)}, f32[16,4,16]{2,1,0:T(4,128)S(1)}, u32[]{:S(2)}) copy-start(f32[16,4,16]{2,1,0:T(4,128)S(1)} %get-tuple-element.217) | copy-start | bytes 12292
  23.9 4.5 %copy-start.8 = (pred[16,16,16]{2,1,0:T(8,128)(4,1)S(1)}, pred[16,16,16]{2,1,0:T(8,128)(4,1)}, u32[]{:S(2)}) copy-start(pred[16,16,16]{2,1,0:T(8,128)(4,1)} %get-tuple-element.213) | copy-start | bytes 12292
  23.9 4.6 %copy-start.13 = (f32[128]{0:T(128)S(1)}, f32[128]{0:T(128)}, u32[]{:S(2)}) copy-start(f32[128]{0:T(128)} %param.29) | copy-start | bytes 1540
  24.0 4.8 %copy-start.3 = (f32[16,16,4,128]{3,2,1,0:T(4,128)S(1)}, f32[16,16,4,128]{3,2,1,0:T(4,128)}, u32[]{:S(2)}) copy-start(f32[16,16,4,128]{3,2,1,0:T(4,128)} %copy-done.2) | copy-start | bytes 1572868
  27.6 54.2 %reduce-scatter.2.cloned.1.call-start = ((), (), s32[]{:S(2)}) async-start(), calls=%async_computation.1 | async-start | bytes 393216 | tf_op jit(solution)/shard_map/reduce_scatter | solution.py:227
  28.7 17.5 %copy-start.7 = (f32[16,4,16]{2,1,0:T(4,128)S(1)}, f32[16,4,16]{2,1,0:T(4,128)}, u32[]{:S(2)}) copy-start(f32[16,4,16]{2,1,0:T(4,128)} %copy-done.6) | copy-start | bytes 12292
  28.7 32.7 %copy-start.5 = (bf16[256,128]{1,0:T(8,128)(2,1)S(1)}, bf16[256,128]{1,0:T(8,128)(2,1)}, u32[]{:S(2)}) copy-start(bf16[256,128]{1,0:T(8,128)(2,1)} %slice.32) | copy-start | bytes 196612
Sparse Core Ops, SparseCore 0:
  27.7 31.9 all-gather.4
  72.9 8.7 reduce-scatter.1
where the time goes:
time: 89.2 us; the launch traced here: 88.6 us
  blocking collectives  29.3 us (33%)
  matrix products  17.5 us (20%)
  between operations  13.9 us (16%)
  other arithmetic  12.6 us (14%)
  waiting for transfers between devices  9.01 us (10%)
  local copies, waits for them, and re-layouts  6.23 us (7%)
    all_gather x2, blocking collectives, joined(): lax.all_gather(a.astype(kind), axis)  29.3 us
    reduce_scatter x1, waiting for transfers between devices, shards(): lax.psum_scatter(head_part.astype(jnp.bfloat16), 'tp', scatter_dimension=...  8.96 us
    add x3, other arithmetic, join_blocks(): earlier[2] * left_factor[..., None] + later[2] * right_factor[..., None]  4.34 us
    dot_general x1, matrix products, shards(): jnp.einsum('skgpl,slkd->skgpd', weights.astype(jnp.bfloat16).reshape(seq_...  3.62 us
    dot_general x1, matrix products, shards(): jnp.einsum('spkgd,slkd->skgpl', queries, merged_keys, preferred_element_t...  3.09 us
    dot_general x1, matrix products, shards(): summed = jnp.dot(normed, joined_weight, preferred_element_type=jnp.float32)  2.91 us
    dot_general x4, matrix products, ancestors(): jnp.einsum('sij,sjk->sik', reachable, reachable, precision=HIGHEST)  2.54 us
    dot_general x1, matrix products, shards(): jnp.dot(attended, output_weight, preferred_element_type=jnp.float32)  2.06 us
  transfers between devices with their start and end apart: 2, of which 1 were waited for; matrix products, arithmetic and copies ran while one was open for 6% of the time, Pallas kernels for 0%

commit v1 on v0

--- a/solution.py
+++ b/solution.py
@@ -1,6 +1,11 @@
+import functools
+import math
+
 import jax
 import jax.numpy as jnp
 from jax import lax
+from jax.experimental import pallas as pl
+from jax.experimental.pallas import tpu as pltpu
 from jax.sharding import PartitionSpec as P
 
 EPSILON = 1e-06
@@ -227,6 +232,503 @@
     return lax.psum_scatter(head_part.astype(jnp.bfloat16), "tp", scatter_dimension=2, tiled=True)
 
 
+LOG2E = math.log2(math.e)
+MASKED = 2.0**100
+NT = (((1,), (1,)), ((), ()))
+
+
+def in_vmem(shape, dtype):
+    return pltpu.VMEM(shape, dtype)
+
+
+def held(array):
+    return pltpu.with_memory_space_constraint(array, pltpu.VMEM)
+
+
+def partner_of(place, step):
+    return jnp.bitwise_xor(place, step)
+
+
+def attend_kernel(
+    kv_size,
+    lengths,
+    tokens,
+    norm_gain,
+    query_weight,
+    key_weight,
+    value_weight,
+    forget_rows,
+    query_gain,
+    key_gain,
+    cache_keys,
+    cache_values,
+    cache_logcum,
+    *refs,
+):
+    packed = refs[:kv_size]
+    own_queries, own_keys, own_values, own_gates = refs[kv_size : kv_size + 4]
+    (
+        token_buf,
+        weight_buf,
+        key_buf,
+        value_buf,
+        normed_buf,
+        summed_buf,
+        query_buf,
+        new_key_buf,
+        new_value_buf,
+        token_sem,
+        weight_sem,
+        cache_sem,
+    ) = refs[kv_size + 4 :]
+    place = lax.axis_index("kv")
+    rows, width = tokens.shape
+    query_cols = query_weight.shape[1]
+    head_size = key_weight.shape[1]
+    heads = query_cols // head_size
+    seq_count, block_len = cache_keys.shape[0], cache_keys.shape[1]
+    nodes = rows // seq_count
+    group = seq_count // kv_size
+    row_parts = token_sem.shape[0]
+    row_part = rows // row_parts
+    depth_parts = weight_sem.shape[0]
+    depth = width // depth_parts
+
+    def token_copy(part):
+        span = pl.ds(part * row_part, row_part)
+        return pltpu.make_async_copy(tokens.at[span], token_buf.at[span], token_sem.at[part])
+
+    def weight_copies(part):
+        span = pl.ds(part * depth, depth)
+        return [
+            pltpu.make_async_copy(
+                query_weight.at[span],
+                weight_buf.at[span, pl.ds(0, query_cols)],
+                weight_sem.at[part, 0],
+            ),
+            pltpu.make_async_copy(
+                key_weight.at[span],
+                weight_buf.at[span, pl.ds(query_cols, head_size)],
+                weight_sem.at[part, 1],
+            ),
+            pltpu.make_async_copy(
+                value_weight.at[span],
+                weight_buf.at[span, pl.ds(query_cols + head_size, head_size)],
+                weight_sem.at[part, 2],
+            ),
+        ]
+
+    def cache_copies(step):
+        span = pl.ds(partner_of(place, step) * group, group)
+        return [
+            pltpu.make_async_copy(cache_keys.at[span], key_buf.at[step], cache_sem.at[step, 0]),
+            pltpu.make_async_copy(cache_values.at[span], value_buf.at[step], cache_sem.at[step, 1]),
+        ]
+
+    order = list(range(kv_size - 1, -1, -1))
+    for part in range(row_parts):
+        token_copy(part).start()
+    for part in range(depth_parts):
+        for copy in weight_copies(part):
+            copy.start()
+    for step in order:
+        for copy in cache_copies(step):
+            copy.start()
+
+    gain = norm_gain[...]
+    for part in range(row_parts):
+        token_copy(part).wait()
+        for first in range(part * row_part, (part + 1) * row_part, nodes):
+            widened = token_buf[pl.ds(first, nodes), :].astype(jnp.float32)
+            mean = jnp.mean(widened * widened, axis=1, keepdims=True)
+            normed_buf[pl.ds(first, nodes), :] = (
+                widened * lax.rsqrt(mean + EPSILON) * gain
+            ).astype(jnp.bfloat16)
+
+    for part in range(depth_parts):
+        for copy in weight_copies(part):
+            copy.wait()
+        span = pl.ds(part * depth, depth)
+        product = jnp.dot(
+            normed_buf[:, span], weight_buf[span, :], preferred_element_type=jnp.float32
+        )
+        if part == 0:
+            summed_buf[...] = product
+        else:
+            summed_buf[...] += product
+
+    own_rows = pl.ds(pl.multiple_of(place * (group * nodes), group * nodes), group * nodes)
+    own_gates[...] = lax.dot_general(
+        forget_rows[...], normed_buf[own_rows, :], NT, preferred_element_type=jnp.float32
+    )
+
+    def head_norm(vectors, gain_vec):
+        mean = jnp.mean(vectors * vectors, axis=1, keepdims=True)
+        return (vectors * lax.rsqrt(mean + EPSILON) * gain_vec).astype(jnp.bfloat16)
+
+    for head in range(heads):
+        normal = head_norm(
+            summed_buf[:, head * head_size : (head + 1) * head_size], query_gain[...]
+        )
+        query_buf[:, head * nodes : (head + 1) * nodes, :] = normal.reshape(
+            seq_count, nodes, head_size
+        )
+    new_key_buf[...] = head_norm(
+        summed_buf[:, query_cols : query_cols + head_size], key_gain[...]
+    )
+    new_value_buf[...] = summed_buf[:, query_cols + head_size :].astype(jnp.bfloat16)
+    own_queries[...] = query_buf[pl.ds(place * group, group)]
+    own_keys[...] = new_key_buf[own_rows, :]
+    own_values[...] = new_value_buf[own_rows, :]
+
+    scale = head_size ** (-0.5) * LOG2E
+    column = lax.broadcasted_iota(jnp.int32, (heads, block_len), 1)
+    lane = lax.broadcasted_iota(jnp.int32, (heads * nodes, head_size), 1)
+    for step in order:
+        for copy in cache_copies(step):
+            copy.wait()
+        stats = jnp.zeros((heads * nodes, head_size), jnp.float32)
+        for item in range(group):
+            seq = partner_of(place, step) * group + item
+            raw = lax.dot_general(
+                query_buf[seq], key_buf[step, item], NT, preferred_element_type=jnp.float32
+            )
+            valid = lengths[seq] - place * block_len
+            decay = jnp.where(column < valid, cache_logcum[seq] * LOG2E, MASKED)
+            decay = jnp.concatenate(
+                [
+                    jnp.broadcast_to(decay[head : head + 1, :], (nodes, block_len))
+                    for head in range(heads)
+                ],
+                axis=0,
+            )
+            scores = raw * scale - decay
+            top = jnp.max(scores, axis=1, keepdims=True).astype(jnp.bfloat16).astype(jnp.float32)
+            weights = jnp.exp2(scores - top)
+            total = jnp.sum(weights, axis=1, keepdims=True)
+            values = jnp.dot(
+                weights.astype(jnp.bfloat16),
+                value_buf[step, item],
+                preferred_element_type=jnp.float32,
+            )
+            first = item * heads * nodes
+            packed[step][first : first + heads * nodes, :] = values.astype(jnp.bfloat16)
+            stats = jnp.where(lane == 2 * item, top, stats)
+            stats = jnp.where(lane == 2 * item + 1, total, stats)
+        packed[step][group * heads * nodes :, :] = stats.astype(jnp.bfloat16)
+
+
+def tree_kernel(
+    kv_size,
+    tp_size,
+    accepted,
+    forget_bias,
+    parents,
+    queries,
+    keys_new,
+    values_new,
+    gates,
+    pending_keys,
+    pending_values,
+    pending_logcum,
+    tree_acc,
+    tree_stats,
+    key_buf,
+    value_buf,
+):
+    place = lax.axis_index("kv")
+    side = lax.axis_index("tp")
+    group, head_rows, head_size = queries.shape
+    most_taken, heads, seq_count = pending_logcum.shape
+    nodes = head_rows // heads
+    tree_rows = group * nodes
+    size = 2 * tree_rows
+    exact = dict(preferred_element_type=jnp.float32, precision=HIGHEST)
+
+    key_buf[...] = jnp.zeros_like(key_buf)
+    value_buf[...] = jnp.zeros_like(value_buf)
+    key_buf[:tree_rows, :] = keys_new[...].astype(jnp.float32)
+    value_buf[:tree_rows, :] = values_new[...].astype(jnp.float32)
+    for item in range(group):
+        rows = slice(tree_rows + item * most_taken, tree_rows + (item + 1) * most_taken)
+        key_buf[rows, :] = pending_keys[place * group + item].astype(jnp.float32)
+        value_buf[rows, :] = pending_values[place * group + item].astype(jnp.float32)
+
+    lane = lax.broadcasted_iota(jnp.int32, (1, size), 1)
+    in_tree = jnp.where(lane < tree_rows, 1, 0)
+    tree_item, tree_node = lane // nodes, lane % nodes
+    late = lane - tree_rows
+    late_item, late_node = late // most_taken, late % most_taken
+    in_late = jnp.where((late >= 0) & (late_item < group), 1, 0)
+    item_of = jnp.where(late < 0, tree_item, late_item)
+    taken = jnp.zeros((1, size), jnp.int32)
+    for item in range(group):
+        taken = jnp.where(item_of == item, accepted[place * group + item], taken)
+
+    node_row = lax.broadcasted_iota(jnp.int32, (parents.shape[1], size), 0)
+    spread = jnp.dot(
+        parents[...].astype(jnp.float32),
+        (node_row == tree_node).astype(jnp.float32),
+        preferred_element_type=jnp.float32,
+    )
+    seq_row = lax.broadcasted_iota(jnp.int32, (seq_count, size), 0)
+    own_seq = (seq_row == place * group + jnp.where(in_tree + in_late > 0, item_of, -seq_count)).astype(
+        jnp.float32
+    )
+    parent = jnp.sum(own_seq * spread, axis=0, keepdims=True).astype(jnp.int32)
+    square_row = lax.broadcasted_iota(jnp.int32, (size, size), 0)
+    square_lane = lax.broadcasted_iota(jnp.int32, (size, size), 1)
+    identity = (square_row == square_lane).astype(jnp.float32)
+    linked = square_row == jnp.where((late < 0) & (parent >= 0), tree_item * nodes + parent, -1)
+    reach = linked.astype(jnp.float32) + identity
+    for doubling in range((nodes - 1).bit_length()):
+        low = reach.astype(jnp.bfloat16)
+        reach = jnp.minimum(jnp.dot(low, low, preferred_element_type=jnp.float32), 1.0)
+    low = reach.astype(jnp.bfloat16)
+    ancestry = lax.dot_general(
+        identity.astype(jnp.bfloat16), low, NT, preferred_element_type=jnp.float32
+    )
+
+    raw_gates = gates[:heads, :]
+    for other in range(1, tp_size):
+        raw_gates = jnp.where(side == other, gates[other * heads : (other + 1) * heads, :], raw_gates)
+    bias = jnp.concatenate(
+        [jnp.full((1, tree_rows), forget_bias[side * heads + head]) for head in range(heads)], axis=0
+    )
+    logits = raw_gates + bias
+    log_gates = jnp.minimum(logits, 0.0) - jnp.log1p(jnp.exp(-jnp.abs(logits)))
+    decay = jnp.dot(log_gates, reach[:tree_rows, :], **exact)
+    decay = decay * in_tree.astype(jnp.float32)
+    picked = jnp.where(late < 0, taken - 1, late_node)
+    for node in range(most_taken):
+        chosen = own_seq * (picked == node).astype(jnp.float32)
+        decay = decay + jnp.dot(pending_logcum[node], chosen, **exact)
+    decay = decay * LOG2E
+
+    head_decay = jnp.concatenate(
+        [jnp.broadcast_to(decay[head : head + 1, :], (nodes, size)) for head in range(heads)], axis=0
+    )
+    row = lax.broadcasted_iota(jnp.int32, (head_rows, size), 0)
+    keys = key_buf[...].astype(jnp.bfloat16)
+    values = value_buf[...].astype(jnp.bfloat16)
+    scale = head_size ** (-0.5) * LOG2E
+    for item in range(group):
+        raw = lax.dot_general(queries[item], keys, NT, preferred_element_type=jnp.float32)
+        own_decay = jnp.sum(
+            jnp.where(lane == item * nodes + row % nodes, head_decay, 0.0), axis=1, keepdims=True
+        )
+        scores = raw * scale + own_decay - head_decay
+        reached = jnp.concatenate([ancestry[item * nodes : (item + 1) * nodes, :]] * heads, axis=0)
+        offered = jnp.where(late_item == item, jnp.where(late_node < taken, in_late, 0), 0)
+        seen = reached * in_tree.astype(jnp.float32) + offered.astype(jnp.float32) > 0.5
+        top = jnp.max(jnp.where(seen, scores, NEG_LARGE), axis=1, keepdims=True)
+        weights = jnp.where(seen, jnp.exp2(scores - top), 0.0)
+        total = jnp.sum(weights, axis=1, keepdims=True)
+        rows = slice(item * head_rows, (item + 1) * head_rows)
+        tree_acc[rows, :] = jnp.dot(
+            weights.astype(jnp.bfloat16), values, preferred_element_type=jnp.float32
+        )
+        stat_lane = lax.broadcasted_iota(jnp.int32, (head_rows, head_size), 1)
+        tree_stats[rows, :] = jnp.where(
+            stat_lane == 0, top, jnp.where(stat_lane == 1, total, own_decay)
+        )
+
+
+def merge_kernel(kv_size, tree_acc, tree_stats, *refs):
+    packed, chunk = refs[:kv_size], refs[kv_size]
+    head_size = tree_acc.shape[1]
+    heads = chunk.shape[1] // head_size
+    nodes_all = chunk.shape[0]
+    group = (packed[0].shape[0] * heads) // (nodes_all * heads) - 1
+    group = tree_acc.shape[0] // (packed[0].shape[0] - tree_acc.shape[0])
+    head_rows = tree_acc.shape[0] // group
+    nodes = head_rows // heads
+    stats = [p[group * head_rows :, :].astype(jnp.float32) for p in packed]
+    for item in range(group):
+        rows = slice(item * head_rows, (item + 1) * head_rows)
+        own_decay = tree_stats[rows, 2:3]
+        tree_top = tree_stats[rows, 0:1]
+        tops = [s[:, 2 * item : 2 * item + 1] + own_decay for s in stats]
+        top = functools.reduce(jnp.maximum, tops, tree_top)
+        factor = jnp.exp2(tree_top - top)
+        bottom = tree_stats[rows, 1:2] * factor
+        upper = tree_acc[rows, :] * factor
+        for source in range(kv_size):
+            factor = jnp.exp2(tops[source] - top)
+            bottom = bottom + stats[source][:, 2 * item + 1 : 2 * item + 2] * factor
+            upper = upper + packed[source][rows, :].astype(jnp.float32) * factor
+        attended = (upper / bottom).astype(jnp.bfloat16)
+        for head in range(heads):
+            chunk[item * nodes : (item + 1) * nodes, head * head_size : (head + 1) * head_size] = (
+                attended[head * nodes : (head + 1) * nodes, :]
+            )
+
+
+def project_kernel(kv_size, weight, *refs):
+    chunks, (kept, sent) = refs[:kv_size], refs[kv_size:]
+    place = lax.axis_index("kv")
+    side = lax.axis_index("tp")
+    rows = chunks[0].shape[0]
+    cols = kept.shape[1]
+    for out, half in ((sent, 1 - side), (kept, side)):
+        part = weight[:, pl.ds(pl.multiple_of(half * cols, cols), cols)]
+        for step in range(kv_size):
+            first = pl.multiple_of(partner_of(place, step) * rows, rows)
+            out[pl.ds(first, rows), :] = jnp.dot(
+                chunks[step][...], part, preferred_element_type=jnp.float32
+            ).astype(jnp.bfloat16)
+
+
+def exchange(array, axis, size, step):
+    return lax.ppermute(array, axis, [(i, i ^ step) for i in range(size)])
+
+
+def fast_shards(
+    tokens,
+    norm_gain,
+    query_weight,
+    key_weight,
+    value_weight,
+    forget_weight,
+    forget_bias,
+    query_gain,
+    key_gain,
+    output_weight,
+    cache_keys,
+    cache_values,
+    cache_logcum,
+    pending_keys,
+    pending_values,
+    pending_logcum,
+    lengths,
+    accepted,
+    parents,
+):
+    kv_size, tp_size = lax.axis_size("kv"), lax.axis_size("tp")
+    seq_count, nodes, width = tokens.shape
+    query_cols = query_weight.shape[1]
+    head_size = query_gain.shape[0]
+    heads = query_cols // head_size
+    block_len = cache_keys.shape[1]
+    most_taken = pending_keys.shape[1]
+    rows = seq_count * nodes
+    group = seq_count // kv_size
+    head_rows = heads * nodes
+    bf16, f32 = jnp.bfloat16, jnp.float32
+    hbm = pl.BlockSpec(memory_space=pltpu.HBM)
+    vmem = pl.BlockSpec(memory_space=pltpu.VMEM)
+    smem = pl.BlockSpec(memory_space=pltpu.SMEM)
+    row_parts, depth_parts = 4, 4
+
+    results = pl.pallas_call(
+        functools.partial(attend_kernel, kv_size),
+        name="attend",
+        out_shape=[in_vmem(((group + 1) * head_rows, head_size), bf16) for _ in range(kv_size)]
+        + [
+            in_vmem((group, head_rows, head_size), bf16),
+            in_vmem((group * nodes, head_size), bf16),
+            in_vmem((group * nodes, head_size), bf16),
+            in_vmem((forget_weight.shape[1], group * nodes), f32),
+        ],
+        in_specs=[smem, hbm, vmem, hbm, hbm, hbm, vmem, vmem, vmem, hbm, hbm, vmem],
+        out_specs=[vmem] * (kv_size + 4),
+        scratch_shapes=[
+            pltpu.VMEM((rows, width), bf16),
+            pltpu.VMEM((width, query_cols + 2 * head_size), bf16),
+            pltpu.VMEM((kv_size, group, block_len, head_size), bf16),
+            pltpu.VMEM((kv_size, group, block_len, head_size), bf16),
+            pltpu.VMEM((rows, width), bf16),
+            pltpu.VMEM((rows, query_cols + 2 * head_size), f32),
+            pltpu.VMEM((seq_count, head_rows, head_size), bf16),
+            pltpu.VMEM((rows, head_size), bf16),
+            pltpu.VMEM((rows, head_size), bf16),
+            pltpu.SemaphoreType.DMA((row_parts,)),
+            pltpu.SemaphoreType.DMA((depth_parts, 3)),
+            pltpu.SemaphoreType.DMA((kv_size, 2)),
+        ],
+    )(
+        lengths,
+        tokens.reshape(rows, width),
+        norm_gain.reshape(1, width),
+        query_weight,
+        key_weight,
+        value_weight,
+        forget_weight.T,
+        query_gain.reshape(1, head_size),
+        key_gain.reshape(1, head_size),
+        cache_keys.reshape(seq_count, block_len, head_size),
+        cache_values.reshape(seq_count, block_len, head_size),
+        jnp.swapaxes(cache_logcum, 1, 2),
+    )
+    packed, (own_queries, own_keys, own_values, own_gates) = results[:kv_size], results[kv_size:]
+    moved = {s: exchange(packed[s], "kv", kv_size, s) for s in range(kv_size - 1, 0, -1)}
+    tree_acc, tree_stats = pl.pallas_call(
+        functools.partial(tree_kernel, kv_size, tp_size),
+        name="tree",
+        out_shape=[
+            in_vmem((group * head_rows, head_size), f32),
+            in_vmem((group * head_rows, head_size), f32),
+        ],
+        in_specs=[smem, smem] + [vmem] * 8,
+        out_specs=[vmem, vmem],
+        scratch_shapes=[pltpu.VMEM((2 * group * nodes, head_size), f32)] * 2,
+        cost_estimate=pl.CostEstimate(flops=4_000_000_000, bytes_accessed=1_000_000, transcendentals=0),
+    )(
+        accepted,
+        forget_bias,
+        parents,
+        held(own_queries),
+        held(own_keys),
+        held(own_values),
+        held(own_gates),
+        pending_keys.reshape(seq_count, most_taken, head_size),
+        pending_values.reshape(seq_count, most_taken, head_size),
+        jnp.transpose(pending_logcum, (1, 2, 0)),
+    )
+    chunk = pl.pallas_call(
+        functools.partial(merge_kernel, kv_size),
+        name="merge",
+        out_shape=in_vmem((group * nodes, query_cols), bf16),
+        in_specs=[vmem] * (kv_size + 2),
+        out_specs=vmem,
+    )(
+        held(tree_acc),
+        held(tree_stats),
+        held(packed[0]),
+        *[held(moved[s]) for s in range(1, kv_size)],
+    )
+    chunks = [chunk] + [exchange(chunk, "kv", kv_size, s) for s in range(1, kv_size)]
+    cols = output_weight.shape[1] // tp_size
+    kept, sent = pl.pallas_call(
+        functools.partial(project_kernel, kv_size),
+        name="project",
+        out_shape=[in_vmem((rows, cols), bf16), in_vmem((rows, cols), bf16)],
+        in_specs=[vmem] * (kv_size + 1),
+        out_specs=[vmem, vmem],
+    )(held(output_weight), *[held(c) for c in chunks])
+    received = exchange(sent, "tp", tp_size, 1)
+    summed = (kept.astype(f32) + received.astype(f32)).astype(bf16)
+    return summed.reshape(seq_count, nodes, cols)
+
+
+def fits_fast(mesh, shapes):
+    kv_size = mesh.shape["kv"]
+    seq_count = shapes["tokens"][0] // mesh.shape["dp"]
+    one_key_head = shapes["cache_keys"][2] == mesh.shape["tp"]
+    small = kv_size <= 4 and kv_size & (kv_size - 1) == 0
+    return small and one_key_head and mesh.shape["tp"] == 2 and seq_count % kv_size == 0
+
+
+def chosen_shards(mesh):
+    def run(*args):
+        shapes = {"tokens": args[0].shape, "cache_keys": args[10].shape}
+        shapes["tokens"] = (shapes["tokens"][0] * mesh.shape["dp"],)
+        shapes["cache_keys"] = (0, 0, shapes["cache_keys"][2] * mesh.shape["tp"])
+        return (fast_shards if fits_fast(mesh, shapes) else shards)(*args)
+
+    return run
+
+
 def solution(mesh):
     placed = (
         P("dp", None, None),
@@ -250,5 +752,5 @@
         P("dp", None),
     )
     return jax.shard_map(
-        shards, mesh=mesh, in_specs=placed, out_specs=P("dp", None, ("kv", "tp")), check_vma=False
-    )
+        chosen_shards(mesh), mesh=mesh, in_specs=placed, out_specs=P("dp", None, ("kv", "tp")), check_vma=False
+    )

time: 89.2 us -> 35 us (0.39)
  blocking collectives: 29.3 us -> 0 us
  matrix products: 17.5 us -> 0 us
  Pallas kernels: 0 us -> 14.5 us
  between operations: 13.9 us -> 0.04 us
  other arithmetic: 12.6 us -> 0.69 us
  starting transfers between devices: 0.08 us -> 10.3 us
  local copies, waits for them, and re-layouts: 6.23 us -> 0.01 us
    all_gather x2 -> x0, blocking collectives: 29.3 us -> none  [joined(): lax.all_gather(a.astype(kind), axis)]
    dot_general x14 -> x0, matrix products: 17.5 us -> none  [the longest x1 3.62 us: shards(): jnp.einsum('skgpl,slkd->skgpd', weights.astype(jnp.bfloat16).reshape(seq_...]
    pallas_call x0 -> x4, Pallas kernels: none -> 14.5 us  [the longest x1 9.56 us: fast_shards(): pl.pallas_call(functools.partial(attend_kernel, kv_size), name='attend',...]
    ppermute x0 -> x7, starting transfers between devices: none -> 10.3 us  [exchange(): return lax.ppermute(array, axis, [(i, i ^ step) for i in range(size)])]
    ppermute x0 -> x7, waiting for transfers between devices: none -> 9.26 us  [exchange(): return lax.ppermute(array, axis, [(i, i ^ step) for i in range(size)])]
    reduce_scatter x1 -> x0, waiting for transfers between devices: 8.96 us -> none  [shards(): lax.psum_scatter(head_part.astype(jnp.bfloat16), 'tp', scatter_dimension=...]
    add x9 -> x0, other arithmetic: 5.34 us -> none  [the longest x3 4.34 us: join_blocks(): earlier[2] * left_factor[..., None] + later[2] * right_factor[..., None]]
    reduce_sum x5 -> x0, other arithmetic: 3.48 us -> none  [the longest x1 1.49 us: shards(): jnp.mean(widened * widened, axis=-1, keepdims=True) + EPSILON]
  transfers between devices with their start and end apart: 2 -> 7, of which waited for: 1 -> 4; matrix products, arithmetic and copies ran while one was open for 6% -> 0% of each run, Pallas kernels for 0% -> 7%
where the time goes in v1:
time: 35 us; the launch traced here: 34.8 us
  Pallas kernels  14.5 us (41%)
  starting transfers between devices  10.3 us (29%)
  waiting for transfers between devices  9.26 us (26%)
  other arithmetic  0.69 us (2%)
    ppermute x7, starting transfers between devices, exchange(): return lax.ppermute(array, axis, [(i, i ^ step) for i in range(size)])  10.3 us
    pallas_call x1, Pallas kernels, fast_shards(): pl.pallas_call(functools.partial(attend_kernel, kv_size), name='attend',...  9.56 us
    ppermute x7, waiting for transfers between devices, exchange(): return lax.ppermute(array, axis, [(i, i ^ step) for i in range(size)])  9.26 us
    pallas_call x1, Pallas kernels, fast_shards(): pl.pallas_call(functools.partial(tree_kernel, kv_size, tp_size), name='tr...  2.57 us
    pallas_call x1, Pallas kernels, fast_shards(): pl.pallas_call(functools.partial(merge_kernel, kv_size), name='merge', ou...  1.93 us
  transfers between devices with their start and end apart: 7, of which 4 were waited for; matrix products, arithmetic and copies ran while one was open for 0% of the time, Pallas kernels for 7%

profile of v1, /device:TPU:0, one launch (start us, length us, event | category | flops | bytes accessed | tf_op | source)
XLA Modules:
  0.0 34.8 jit_solution(14434501321969225431)
XLA Ops:
  0.0 9.6 %attend.1 = (bf16[320,128]{1,0:T(8,128)(2,1)S(1)}, bf16[320,128]{1,0:T(8,128)(2,1)S(1)}, bf16[320,128]{1,0:T(8,128)(2,1)S(1)}, bf16[320,128]{1,0:T(8,128)(2,1)S(...) custom-call(s32[16]{0:T(128)} %lengths.1, ...), custom_call_target="tpu_custom_call" | custom-call | tf_op jit(solution)/shard_map/attend/pallas_call | solution.py:623
  9.6 3.1 %collective-permute-start = (bf16[320,128]{1,0:T(8,128)(2,1)S(1)}, bf16[320,128]{1,0:T(8,128)(2,1)S(1)}, u32[]{:S(2)}, u32[]{:S(2)}) collective-permute-start(bf16[320,128]{1,0:T(8,128)(2,1)S(1)} %get-tuple-element.24), channel_id=1, source_target_pairs={{0,2},{2,0},{4,6},{6,4},{1,3},{3,1},{5,7},{7,5},{8,10},{10,8},{12,... | collective-permute-start | bytes 245768 | tf_op jit(solution)/shard_map/ppermute | solution.py:583
  12.7 2.6 %collective-permute-start.1 = (bf16[320,128]{1,0:T(8,128)(2,1)S(1)}, bf16[320,128]{1,0:T(8,128)(2,1)S(1)}, u32[]{:S(2)}, u32[]{:S(2)}) collective-permute-start(bf16[320,128]{1,0:T(8,128)(2,1)S(1)} %get-tuple-element.25), channel_id=1, source_target_pairs={{0,4},{2,6},{4,0},{6,2},{1,5},{3,7},{5,1},{7,3},{8,12},{10,14},{12... | collective-permute-start | bytes 245768 | tf_op jit(solution)/shard_map/ppermute | solution.py:583
  15.3 0.0 collective-permute-start.2
  15.3 0.0 copy-start
  15.3 2.6 %tree.1 = (f32[256,128]{1,0:T(8,128)S(1)}, f32[256,128]{1,0:T(8,128)S(1)}) custom-call(s32[16]{0:T(128)} %accepted.1, f32[8]{0:T(128)} %forget_bias.1, s32[16,16]{1,0:T(8,128)} %parents.1, bf16[4,64,128]{2,1,0:T(8,128)(2,1)S(1)} %get-tuple-element.17.queries, bf16[64,128]{1,0:T(8,128)(2,1)S(1)} %get-tuple-element.18.keys_new, ...), custom_call_target="tpu_custom_call" | custom-call | flops 4000000000 | bytes 1000000 | tf_op jit(solution)/shard_map/tree/pallas_call | solution.py:665
  17.9 0.0 collective-permute-done.refs_1_
  17.9 4.0 %collective-permute-done.1.refs_2_ = bf16[320,128]{1,0:T(8,128)(2,1)S(1)} collective-permute-done((bf16[320,128]{1,0:T(8,128)(2,1)S(1)}, bf16[320,128]{1,0:T(8,128)(2,1)S(1)}, u32[]{:S(2)}, u32[]{:S(2)}) %collective-permute-start.1) | collective-permute-done | bytes 81952 | tf_op jit(solution)/shard_map/ppermute | solution.py:583
  21.9 0.0 collective-permute-done.2.refs_3_
  21.9 1.9 %merge.1.refs_0_ = bf16[64,512]{1,0:T(8,128)(2,1)S(1)} custom-call(f32[256,128]{1,0:T(8,128)S(1)} %get-tuple-element.21.tree_acc, f32[256,128]{1,0:T(8,128)S(1)} %get-tuple-element.22.tree_stats, bf16[320,128]{1,0:T(8,128)(2,1)S(1)} %get-tuple-element.23.refs_0_, bf16[320,128]{1,0:T(8,128)(2,1)S(1)} %collective-permute-done.refs_1_, ...), custom_call_target="tpu_custom_call" | custom-call | tf_op jit(solution)/shard_map/merge/pallas_call | solution.py:688
  23.8 2.5 %collective-permute-start.5 = (bf16[64,512]{1,0:T(8,128)(2,1)S(1)}, bf16[64,512]{1,0:T(8,128)(2,1)S(1)}, u32[]{:S(2)}, u32[]{:S(2)}) collective-permute-start(bf16[64,512]{1,0:T(8,128)(2,1)S(1)} %merge.1.refs_0_), channel_id=1, source_target_pairs={{0,6},{2,4},{4,2},{6,0},{1,7},{3,5},{5,3},{7,1},{8,14},{10,12},{12... | collective-permute-start | bytes 196616 | tf_op jit(solution)/shard_map/ppermute | solution.py:583
  26.4 0.4 %collective-permute-start.4 = (bf16[64,512]{1,0:T(8,128)(2,1)S(1)}, bf16[64,512]{1,0:T(8,128)(2,1)S(1)}, u32[]{:S(2)}, u32[]{:S(2)}) collective-permute-start(bf16[64,512]{1,0:T(8,128)(2,1)S(1)} %merge.1.refs_0_), channel_id=1, source_target_pairs={{0,4},{2,6},{4,0},{6,2},{1,5},{3,7},{5,1},{7,3},{8,12},{10,14},{12... | collective-permute-start | bytes 196616 | tf_op jit(solution)/shard_map/ppermute | solution.py:583
  26.8 1.5 %collective-permute-start.3 = (bf16[64,512]{1,0:T(8,128)(2,1)S(1)}, bf16[64,512]{1,0:T(8,128)(2,1)S(1)}, u32[]{:S(2)}, u32[]{:S(2)}) collective-permute-start(bf16[64,512]{1,0:T(8,128)(2,1)S(1)} %merge.1.refs_0_), channel_id=1, source_target_pairs={{0,2},{2,0},{4,6},{6,4},{1,3},{3,1},{5,7},{7,5},{8,10},{10,8},{12,... | collective-permute-start | bytes 196616 | tf_op jit(solution)/shard_map/ppermute | solution.py:583
  28.3 2.1 %collective-permute-done.5.refs_3_ = bf16[64,512]{1,0:T(8,128)(2,1)S(1)} collective-permute-done((bf16[64,512]{1,0:T(8,128)(2,1)S(1)}, bf16[64,512]{1,0:T(8,128)(2,1)S(1)}, u32[]{:S(2)}, u32[]{:S(2)}) %collective-permute-start.5) | collective-permute-done | bytes 65568 | tf_op jit(solution)/shard_map/ppermute | solution.py:583
  30.3 1.9 %collective-permute-done.4.refs_2_ = bf16[64,512]{1,0:T(8,128)(2,1)S(1)} collective-permute-done((bf16[64,512]{1,0:T(8,128)(2,1)S(1)}, bf16[64,512]{1,0:T(8,128)(2,1)S(1)}, u32[]{:S(2)}, u32[]{:S(2)}) %collective-permute-start.4) | collective-permute-done | bytes 65568 | tf_op jit(solution)/shard_map/ppermute | solution.py:583
  32.2 0.0 collective-permute-done.3.refs_1_
  32.2 0.0 copy-done
  32.2 0.5 %project.1 = (bf16[256,256]{1,0:T(8,128)(2,1)S(1)}, bf16[256,256]{1,0:T(8,128)(2,1)S(1)}) custom-call(bf16[512,512]{1,0:T(8,128)(2,1)S(1)} %copy-done, bf16[64,512]{1,0:T(8,128)(2,1)S(1)} %merge.1.refs_0_, bf16[64,512]{1,0:T(8,128)(2,1)S(1)} %collective-permute-done.3.refs_1_, bf16[64,512]{1,0:T(8,128)(2,1)S(1)} %collective-permute-done.4.refs_2_, ...), custom_call_target="tpu_custom_call" | custom-call | tf_op jit(solution)/shard_map/project/pallas_call | solution.py:702
  32.7 0.1 collective-permute-start.6
  32.8 1.3 %collective-permute-done.6 = bf16[256,256]{1,0:T(8,128)(2,1)S(1)} collective-permute-done((bf16[256,256]{1,0:T(8,128)(2,1)S(1)}, bf16[256,256]{1,0:T(8,128)(2,1)S(1)}, u32[]{:S(2)}, u32[]{:S(2)}) %collective-permute-start.6) | collective-permute-done | bytes 131104 | tf_op jit(solution)/shard_map/ppermute | solution.py:583
  34.1 0.7 %add_convert_fusion = bf16[256,256]{1,0:T(8,128)(2,1)} fusion(bf16[256,256]{1,0:T(8,128)(2,1)S(1)} %collective-permute-done.6, bf16[256,256]{1,0:T(8,128)(2,1)S(1)} %get-tuple-element.27), kind=kLoop, calls=%fused_computation | loop fusion | flops 262144 | bytes 393216 | tf_op jit(solution)/shard_map/convert_element_type | solution.py:710
Async XLA Ops:
  9.6 8.3 %collective-permute-start = (bf16[320,128]{1,0:T(8,128)(2,1)S(1)}, bf16[320,128]{1,0:T(8,128)(2,1)S(1)}, u32[]{:S(2)}, u32[]{:S(2)}) collective-permute-start(bf16[320,128]{1,0:T(8,128)(2,1)S(1)} %get-tuple-element.24), channel_id=1, source_target_pairs={{0,2},{2,0},{4,6},{6,4},{1,3},{3,1},{5,7},{7,5},{8,10},{10,8},{12,... | collective-permute-start | bytes 245768 | tf_op jit(solution)/shard_map/ppermute | solution.py:583
  12.7 9.2 %collective-permute-start.1 = (bf16[320,128]{1,0:T(8,128)(2,1)S(1)}, bf16[320,128]{1,0:T(8,128)(2,1)S(1)}, u32[]{:S(2)}, u32[]{:S(2)}) collective-permute-start(bf16[320,128]{1,0:T(8,128)(2,1)S(1)} %get-tuple-element.25), channel_id=1, source_target_pairs={{0,4},{2,6},{4,0},{6,2},{1,5},{3,7},{5,1},{7,3},{8,12},{10,14},{12... | collective-permute-start | bytes 245768 | tf_op jit(solution)/shard_map/ppermute | solution.py:583
  15.3 6.6 %collective-permute-start.2 = (bf16[320,128]{1,0:T(8,128)(2,1)S(1)}, bf16[320,128]{1,0:T(8,128)(2,1)S(1)}, u32[]{:S(2)}, u32[]{:S(2)}) collective-permute-start(bf16[320,128]{1,0:T(8,128)(2,1)S(1)} %get-tuple-element.26), channel_id=1, source_target_pairs={{0,6},{2,4},{4,2},{6,0},{1,7},{3,5},{5,3},{7,1},{8,14},{10,12},{12... | collective-permute-start | bytes 245768 | tf_op jit(solution)/shard_map/ppermute | solution.py:583
  15.3 16.9 %copy-start = (bf16[512,512]{1,0:T(8,128)(2,1)S(1)}, bf16[512,512]{1,0:T(8,128)(2,1)}, u32[]{:S(2)}) copy-start(bf16[512,512]{1,0:T(8,128)(2,1)} %weight.1) | copy-start | bytes 1572868
  23.8 6.5 %collective-permute-start.5 = (bf16[64,512]{1,0:T(8,128)(2,1)S(1)}, bf16[64,512]{1,0:T(8,128)(2,1)S(1)}, u32[]{:S(2)}, u32[]{:S(2)}) collective-permute-start(bf16[64,512]{1,0:T(8,128)(2,1)S(1)} %merge.1.refs_0_), channel_id=1, source_target_pairs={{0,6},{2,4},{4,2},{6,0},{1,7},{3,5},{5,3},{7,1},{8,14},{10,12},{12... | collective-permute-start | bytes 196616 | tf_op jit(solution)/shard_map/ppermute | solution.py:583
  26.4 5.8 %collective-permute-start.4 = (bf16[64,512]{1,0:T(8,128)(2,1)S(1)}, bf16[64,512]{1,0:T(8,128)(2,1)S(1)}, u32[]{:S(2)}, u32[]{:S(2)}) collective-permute-start(bf16[64,512]{1,0:T(8,128)(2,1)S(1)} %merge.1.refs_0_), channel_id=1, source_target_pairs={{0,4},{2,6},{4,0},{6,2},{1,5},{3,7},{5,1},{7,3},{8,12},{10,14},{12... | collective-permute-start | bytes 196616 | tf_op jit(solution)/shard_map/ppermute | solution.py:583
  26.8 5.4 %collective-permute-start.3 = (bf16[64,512]{1,0:T(8,128)(2,1)S(1)}, bf16[64,512]{1,0:T(8,128)(2,1)S(1)}, u32[]{:S(2)}, u32[]{:S(2)}) collective-permute-start(bf16[64,512]{1,0:T(8,128)(2,1)S(1)} %merge.1.refs_0_), channel_id=1, source_target_pairs={{0,2},{2,0},{4,6},{6,4},{1,3},{3,1},{5,7},{7,5},{8,10},{10,8},{12,... | collective-permute-start | bytes 196616 | tf_op jit(solution)/shard_map/ppermute | solution.py:583
  32.7 1.4 %collective-permute-start.6 = (bf16[256,256]{1,0:T(8,128)(2,1)S(1)}, bf16[256,256]{1,0:T(8,128)(2,1)S(1)}, u32[]{:S(2)}, u32[]{:S(2)}) collective-permute-start(bf16[256,256]{1,0:T(8,128)(2,1)S(1)} %get-tuple-element.28), channel_id=1, source_target_pairs={{0,1},{1,0},{2,3},{3,2},{4,5},{5,4},{6,7},{7,6},{8,9},{9,8},{10,11... | collective-permute-start | bytes 393224 | tf_op jit(solution)/shard_map/ppermute | solution.py:583

commit v2 on v1

--- a/solution.py
+++ b/solution.py
@@ -46,7 +46,7 @@
     reachable = (parents[..., None] == indices).astype(jnp.float32) + jnp.eye(
         node_count, dtype=jnp.float32
     )
-    for doubling in range((node_count - 1).bit_length()):
+    for _ in range((node_count - 1).bit_length()):
         reachable = jnp.minimum(
             jnp.einsum("sij,sjk->sik", reachable, reachable, precision=HIGHEST), 1.0
         )
@@ -234,6 +234,8 @@
 
 LOG2E = math.log2(math.e)
 MASKED = 2.0**100
+STAT_ROWS = 16
+GRANT = 16 * 2**20
 NT = (((1,), (1,)), ((), ()))
 
 
@@ -249,7 +251,66 @@
     return jnp.bitwise_xor(place, step)
 
 
-def attend_kernel(
+def tile_rows(rows, nodes):
+    return jnp.concatenate(
+        [jnp.broadcast_to(rows[i : i + 1, :], (nodes, rows.shape[1])) for i in range(rows.shape[0])],
+        axis=0,
+    )
+
+
+def stacked(columns, head_rows, lanes):
+    lane = lax.broadcasted_iota(jnp.int32, (head_rows, lanes), 1)
+    stats = jnp.zeros((head_rows, lanes), jnp.float32)
+    for place, column in enumerate(columns):
+        stats = jnp.where(lane == place, column, stats)
+    return stats.T
+
+
+def partials(queries, keys, values, decays, nodes, packed, extra=None):
+    head_rows, head_size = queries[0].shape
+    scale = head_size ** (-0.5) * LOG2E
+    group = len(queries)
+    raw = [
+        lax.dot_general(q, k, NT, preferred_element_type=jnp.float32)
+        for q, k in zip(queries, keys, strict=True)
+    ]
+    scores = [r * scale - tile_rows(d, nodes) for r, d in zip(raw, decays, strict=True)]
+    tops = [jnp.max(s, axis=1, keepdims=True) for s in scores]
+    if extra is not None:
+        tree_scores, tree_values = extra
+        tops = [
+            jnp.maximum(t, jnp.max(s, axis=1, keepdims=True))
+            for t, s in zip(tops, tree_scores, strict=True)
+        ]
+    tops = [t.astype(jnp.bfloat16).astype(jnp.float32) for t in tops]
+    weights = [jnp.exp2(s - t) for s, t in zip(scores, tops, strict=True)]
+    totals = [jnp.sum(w, axis=1, keepdims=True) for w in weights]
+    sums = [
+        jnp.dot(w.astype(jnp.bfloat16), v, preferred_element_type=jnp.float32)
+        for w, v in zip(weights, values, strict=True)
+    ]
+    if extra is not None:
+        weights = [jnp.exp2(s - t) for s, t in zip(tree_scores, tops, strict=True)]
+        totals = [
+            t + jnp.sum(w, axis=1, keepdims=True) for t, w in zip(totals, weights, strict=True)
+        ]
+        sums = [
+            s + jnp.dot(w.astype(jnp.bfloat16), tree_values, preferred_element_type=jnp.float32)
+            for s, w in zip(sums, weights, strict=True)
+        ]
+    for item in range(group):
+        first = item * head_rows
+        packed[first : first + head_rows, :] = sums[item].astype(jnp.bfloat16)
+    high = [t.astype(jnp.bfloat16).astype(jnp.float32) for t in totals]
+    low = [t - h for t, h in zip(totals, high, strict=True)]
+    stats = stacked(tops + high + low, head_rows, head_size)
+    packed[group * head_rows :, :head_rows] = stats[:STAT_ROWS, :].astype(jnp.bfloat16)
+    packed[group * head_rows :, head_rows:] = jnp.zeros(
+        (STAT_ROWS, head_size - head_rows), jnp.bfloat16
+    )
+
+
+def first_kernel(
     kv_size,
     lengths,
     tokens,
@@ -257,30 +318,34 @@
     query_weight,
     key_weight,
     value_weight,
-    forget_rows,
     query_gain,
     key_gain,
     cache_keys,
     cache_values,
     cache_logcum,
-    *refs,
+    packed,
+    normed,
+    queries,
+    new_keys,
+    new_values,
+    key_buf,
+    value_buf,
+    decay_buf,
+    length_buf,
+    token_buf,
+    gain_buf,
+    query_gain_buf,
+    key_gain_buf,
+    query_weight_buf,
+    key_weight_buf,
+    value_weight_buf,
+    logcum_buf,
+    summed_buf,
+    small_sem,
+    token_sem,
+    weight_sem,
+    cache_sem,
 ):
-    packed = refs[:kv_size]
-    own_queries, own_keys, own_values, own_gates = refs[kv_size : kv_size + 4]
-    (
-        token_buf,
-        weight_buf,
-        key_buf,
-        value_buf,
-        normed_buf,
-        summed_buf,
-        query_buf,
-        new_key_buf,
-        new_value_buf,
-        token_sem,
-        weight_sem,
-        cache_sem,
-    ) = refs[kv_size + 4 :]
     place = lax.axis_index("kv")
     rows, width = tokens.shape
     query_cols = query_weight.shape[1]
@@ -294,73 +359,90 @@
     depth_parts = weight_sem.shape[0]
     depth = width // depth_parts
 
-    def token_copy(part):
-        span = pl.ds(part * row_part, row_part)
-        return pltpu.make_async_copy(tokens.at[span], token_buf.at[span], token_sem.at[part])
-
-    def weight_copies(part):
-        span = pl.ds(part * depth, depth)
+    def spans(source, target, sem, count, parts):
+        part = count // parts
         return [
             pltpu.make_async_copy(
-                query_weight.at[span],
-                weight_buf.at[span, pl.ds(0, query_cols)],
-                weight_sem.at[part, 0],
-            ),
-            pltpu.make_async_copy(
-                key_weight.at[span],
-                weight_buf.at[span, pl.ds(query_cols, head_size)],
-                weight_sem.at[part, 1],
-            ),
-            pltpu.make_async_copy(
-                value_weight.at[span],
-                weight_buf.at[span, pl.ds(query_cols + head_size, head_size)],
-                weight_sem.at[part, 2],
-            ),
+                source.at[pl.ds(i * part, part)], target.at[pl.ds(i * part, part)], sem(i)
+            )
+            for i in range(parts)
         ]
 
-    def cache_copies(step):
+    small = [
+        pltpu.make_async_copy(source, target, small_sem.at[i])
+        for i, (source, target) in enumerate(
+            (
+                (lengths, length_buf),
+                (norm_gain, gain_buf),
+                (query_gain, query_gain_buf),
+                (key_gain, key_gain_buf),
+                (cache_logcum, logcum_buf),
+            )
+        )
+    ]
+    token_copies = spans(tokens, token_buf, lambda i: token_sem.at[i], rows, row_parts)
+    weight_copies = list(
+        zip(
+            spans(query_weight, query_weight_buf, lambda i: weight_sem.at[i, 0], width, depth_parts),
+            spans(key_weight, key_weight_buf, lambda i: weight_sem.at[i, 1], width, depth_parts),
+            spans(value_weight, value_weight_buf, lambda i: weight_sem.at[i, 2], width, depth_parts),
+            strict=True,
+        )
+    )
+    cache_copies = []
+    for step in range(kv_size):
         span = pl.ds(partner_of(place, step) * group, group)
-        return [
-            pltpu.make_async_copy(cache_keys.at[span], key_buf.at[step], cache_sem.at[step, 0]),
-            pltpu.make_async_copy(cache_values.at[span], value_buf.at[step], cache_sem.at[step, 1]),
-        ]
-
-    order = list(range(kv_size - 1, -1, -1))
+        cache_copies.append(
+            (
+                pltpu.make_async_copy(cache_keys.at[span], key_buf.at[step], cache_sem.at[step, 0]),
+                pltpu.make_async_copy(cache_values.at[span], value_buf.at[step], cache_sem.at[step, 1]),
+            )
+        )
+    small[1].start()
+    for copy in token_copies:
+        copy.start()
+    for copies in weight_copies:
+        for copy in copies:
+            copy.start()
+    for i in (0, 2, 3, 4):
+        small[i].start()
+    for step in range(kv_size - 1, -1, -1):
+        for copy in cache_copies[step]:
+            copy.start()
+
+    small[1].wait()
+    gain = gain_buf[...]
     for part in range(row_parts):
-        token_copy(part).start()
-    for part in range(depth_parts):
-        for copy in weight_copies(part):
-            copy.start()
-    for step in order:
-        for copy in cache_copies(step):
-            copy.start()
-
-    gain = norm_gain[...]
-    for part in range(row_parts):
-        token_copy(part).wait()
+        token_copies[part].wait()
         for first in range(part * row_part, (part + 1) * row_part, nodes):
             widened = token_buf[pl.ds(first, nodes), :].astype(jnp.float32)
             mean = jnp.mean(widened * widened, axis=1, keepdims=True)
-            normed_buf[pl.ds(first, nodes), :] = (
+            normed[pl.ds(first, nodes), :] = (
                 widened * lax.rsqrt(mean + EPSILON) * gain
             ).astype(jnp.bfloat16)
 
     for part in range(depth_parts):
-        for copy in weight_copies(part):
+        for copy in weight_copies[part]:
             copy.wait()
         span = pl.ds(part * depth, depth)
-        product = jnp.dot(
-            normed_buf[:, span], weight_buf[span, :], preferred_element_type=jnp.float32
-        )
-        if part == 0:
-            summed_buf[...] = product
-        else:
-            summed_buf[...] += product
-
-    own_rows = pl.ds(pl.multiple_of(place * (group * nodes), group * nodes), group * nodes)
-    own_gates[...] = lax.dot_general(
-        forget_rows[...], normed_buf[own_rows, :], NT, preferred_element_type=jnp.float32
-    )
+        left = normed[:, span]
+        both = jnp.concatenate([key_weight_buf[span, :], value_weight_buf[span, :]], axis=1)
+        for target, right in (
+            (pl.ds(0, query_cols), query_weight_buf[span, :]),
+            (pl.ds(query_cols, 2 * head_size), both),
+        ):
+            product = jnp.dot(left, right, preferred_element_type=jnp.float32)
+            if part == 0:
+                summed_buf[:, target] = product
+            else:
+                summed_buf[:, target] += product
+    for i in (0, 2, 3, 4):
+        small[i].wait()
+
+    column = lax.broadcasted_iota(jnp.int32, (heads, block_len), 1)
+    for seq in range(seq_count):
+        valid = length_buf[seq] - place * block_len
+        decay_buf[seq] = jnp.where(column < valid, logcum_buf[seq] * LOG2E, MASKED)
 
     def head_norm(vectors, gain_vec):
         mean = jnp.mean(vectors * vectors, axis=1, keepdims=True)
@@ -368,91 +450,83 @@
 
     for head in range(heads):
         normal = head_norm(
-            summed_buf[:, head * head_size : (head + 1) * head_size], query_gain[...]
+            summed_buf[:, head * head_size : (head + 1) * head_size], query_gain_buf[...]
         )
-        query_buf[:, head * nodes : (head + 1) * nodes, :] = normal.reshape(
+        queries[:, head * nodes : (head + 1) * nodes, :] = normal.reshape(
             seq_count, nodes, head_size
         )
-    new_key_buf[...] = head_norm(
-        summed_buf[:, query_cols : query_cols + head_size], key_gain[...]
-    )
-    new_value_buf[...] = summed_buf[:, query_cols + head_size :].astype(jnp.bfloat16)
-    own_queries[...] = query_buf[pl.ds(place * group, group)]
-    own_keys[...] = new_key_buf[own_rows, :]
-    own_values[...] = new_value_buf[own_rows, :]
-
-    scale = head_size ** (-0.5) * LOG2E
-    column = lax.broadcasted_iota(jnp.int32, (heads, block_len), 1)
-    lane = lax.broadcasted_iota(jnp.int32, (heads * nodes, head_size), 1)
-    for step in order:
-        for copy in cache_copies(step):
+    new_keys[...] = head_norm(
+        summed_buf[:, query_cols : query_cols + head_size], key_gain_buf[...]
+    )
+    new_values[...] = summed_buf[:, query_cols + head_size :].astype(jnp.bfloat16)
+    for step in range(kv_size - 1, -1, -1):
+        for copy in cache_copies[step]:
             copy.wait()
-        stats = jnp.zeros((heads * nodes, head_size), jnp.float32)
-        for item in range(group):
-            seq = partner_of(place, step) * group + item
-            raw = lax.dot_general(
-                query_buf[seq], key_buf[step, item], NT, preferred_element_type=jnp.float32
-            )
-            valid = lengths[seq] - place * block_len
-            decay = jnp.where(column < valid, cache_logcum[seq] * LOG2E, MASKED)
-            decay = jnp.concatenate(
-                [
-                    jnp.broadcast_to(decay[head : head + 1, :], (nodes, block_len))
-                    for head in range(heads)
-                ],
-                axis=0,
-            )
-            scores = raw * scale - decay
-            top = jnp.max(scores, axis=1, keepdims=True).astype(jnp.bfloat16).astype(jnp.float32)
-            weights = jnp.exp2(scores - top)
-            total = jnp.sum(weights, axis=1, keepdims=True)
-            values = jnp.dot(
-                weights.astype(jnp.bfloat16),
-                value_buf[step, item],
-                preferred_element_type=jnp.float32,
-            )
-            first = item * heads * nodes
-            packed[step][first : first + heads * nodes, :] = values.astype(jnp.bfloat16)
-            stats = jnp.where(lane == 2 * item, top, stats)
-            stats = jnp.where(lane == 2 * item + 1, total, stats)
-        packed[step][group * heads * nodes :, :] = stats.astype(jnp.bfloat16)
-
-
-def tree_kernel(
-    kv_size,
+    step_partials(kv_size - 1, place, nodes, queries, key_buf, value_buf, decay_buf, packed)
+
+
+def step_partials(step, place, nodes, queries, keys, values, decays, packed, extra=None):
+    group = keys.shape[1]
+    seqs = [partner_of(place, step) * group + item for item in range(group)]
+    partials(
+        [queries[seq] for seq in seqs],
+        [keys[step, item] for item in range(group)],
+        [values[step, item] for item in range(group)],
+        [decays[seq] for seq in seqs],
+        nodes,
+        packed,
+        extra,
+    )
+
+
+def next_kernel(step, queries, keys, values, decays, packed):
+    nodes = queries.shape[1] // decays.shape[1]
+    step_partials(step, lax.axis_index("kv"), nodes, queries, keys, values, decays, packed)
+
+
+def own_kernel(
     tp_size,
     accepted,
     forget_bias,
     parents,
-    queries,
-    keys_new,
-    values_new,
-    gates,
+    forget_rows,
     pending_keys,
     pending_values,
     pending_logcum,
-    tree_acc,
-    tree_stats,
+    normed,
+    queries,
+    new_keys,
+    new_values,
+    keys,
+    values,
+    decays,
+    packed,
+    terms,
     key_buf,
     value_buf,
 ):
     place = lax.axis_index("kv")
     side = lax.axis_index("tp")
-    group, head_rows, head_size = queries.shape
+    group = keys.shape[1]
+    head_rows, head_size = queries.shape[1], queries.shape[2]
     most_taken, heads, seq_count = pending_logcum.shape
     nodes = head_rows // heads
     tree_rows = group * nodes
     size = 2 * tree_rows
     exact = dict(preferred_element_type=jnp.float32, precision=HIGHEST)
+    own_rows = pl.ds(pl.multiple_of(place * tree_rows, tree_rows), tree_rows)
 
     key_buf[...] = jnp.zeros_like(key_buf)
     value_buf[...] = jnp.zeros_like(value_buf)
-    key_buf[:tree_rows, :] = keys_new[...].astype(jnp.float32)
-    value_buf[:tree_rows, :] = values_new[...].astype(jnp.float32)
+    key_buf[:tree_rows, :] = new_keys[own_rows, :].astype(jnp.float32)
+    value_buf[:tree_rows, :] = new_values[own_rows, :].astype(jnp.float32)
     for item in range(group):
         rows = slice(tree_rows + item * most_taken, tree_rows + (item + 1) * most_taken)
         key_buf[rows, :] = pending_keys[place * group + item].astype(jnp.float32)
         value_buf[rows, :] = pending_values[place * group + item].astype(jnp.float32)
+    gates = lax.dot_general(
+        forget_rows[...], normed[own_rows, :], NT, preferred_element_type=jnp.float32
+    )
 
     lane = lax.broadcasted_iota(jnp.int32, (1, size), 1)
     in_tree = jnp.where(lane < tree_rows, 1, 0)
@@ -481,7 +555,7 @@
     identity = (square_row == square_lane).astype(jnp.float32)
     linked = square_row == jnp.where((late < 0) & (parent >= 0), tree_item * nodes + parent, -1)
     reach = linked.astype(jnp.float32) + identity
-    for doubling in range((nodes - 1).bit_length()):
+    for _ in range((nodes - 1).bit_length()):
         low = reach.astype(jnp.bfloat16)
         reach = jnp.minimum(jnp.dot(low, low, preferred_element_type=jnp.float32), 1.0)
     low = reach.astype(jnp.bfloat16)
@@ -505,59 +579,62 @@
         decay = decay + jnp.dot(pending_logcum[node], chosen, **exact)
     decay = decay * LOG2E
 
-    head_decay = jnp.concatenate(
-        [jnp.broadcast_to(decay[head : head + 1, :], (nodes, size)) for head in range(heads)], axis=0
-    )
+    head_decay = tile_rows(decay, nodes)
     row = lax.broadcasted_iota(jnp.int32, (head_rows, size), 0)
-    keys = key_buf[...].astype(jnp.bfloat16)
-    values = value_buf[...].astype(jnp.bfloat16)
+    tree_keys = key_buf[...].astype(jnp.bfloat16)
     scale = head_size ** (-0.5) * LOG2E
+    tree_scores, own_terms = [], []
     for item in range(group):
-        raw = lax.dot_general(queries[item], keys, NT, preferred_element_type=jnp.float32)
-        own_decay = jnp.sum(
-            jnp.where(lane == item * nodes + row % nodes, head_decay, 0.0), axis=1, keepdims=True
+        raw = lax.dot_general(
+            queries[place * group + item], tree_keys, NT, preferred_element_type=jnp.float32
         )
-        scores = raw * scale + own_decay - head_decay
+        own_terms.append(
+            jnp.sum(
+                jnp.where(lane == item * nodes + row % nodes, head_decay, 0.0),
+                axis=1,
+                keepdims=True,
+            )
+        )
         reached = jnp.concatenate([ancestry[item * nodes : (item + 1) * nodes, :]] * heads, axis=0)
         offered = jnp.where(late_item == item, jnp.where(late_node < taken, in_late, 0), 0)
         seen = reached * in_tree.astype(jnp.float32) + offered.astype(jnp.float32) > 0.5
-        top = jnp.max(jnp.where(seen, scores, NEG_LARGE), axis=1, keepdims=True)
-        weights = jnp.where(seen, jnp.exp2(scores - top), 0.0)
-        total = jnp.sum(weights, axis=1, keepdims=True)
-        rows = slice(item * head_rows, (item + 1) * head_rows)
-        tree_acc[rows, :] = jnp.dot(
-            weights.astype(jnp.bfloat16), values, preferred_element_type=jnp.float32
-        )
-        stat_lane = lax.broadcasted_iota(jnp.int32, (head_rows, head_size), 1)
-        tree_stats[rows, :] = jnp.where(
-            stat_lane == 0, top, jnp.where(stat_lane == 1, total, own_decay)
-        )
-
-
-def merge_kernel(kv_size, tree_acc, tree_stats, *refs):
+        tree_scores.append(jnp.where(seen, raw * scale - head_decay, -MASKED))
+    terms[...] = stacked(own_terms, head_rows, head_size)[: terms.shape[0], :]
+    extra = (tree_scores, value_buf[...].astype(jnp.bfloat16))
+    step_partials(0, place, nodes, queries, keys, values, decays, packed, extra)
+
+
+def merge_kernel(kv_size, terms, *refs):
     packed, chunk = refs[:kv_size], refs[kv_size]
-    head_size = tree_acc.shape[1]
+    head_size = packed[0].shape[1]
     heads = chunk.shape[1] // head_size
-    nodes_all = chunk.shape[0]
-    group = (packed[0].shape[0] * heads) // (nodes_all * heads) - 1
-    group = tree_acc.shape[0] // (packed[0].shape[0] - tree_acc.shape[0])
-    head_rows = tree_acc.shape[0] // group
+    head_rows = terms.shape[1]
     nodes = head_rows // heads
-    stats = [p[group * head_rows :, :].astype(jnp.float32) for p in packed]
+    group = chunk.shape[0] // nodes
+    base = group * head_rows
+    term = terms[:group, :]
+    stats = [p[base:, :head_rows].astype(jnp.float32) for p in packed]
+    tops = [s[:group] + term for s in stats]
+    top = functools.reduce(jnp.maximum, tops)
+    factors = [jnp.exp2(t - top) for t in tops]
+    bottom = sum(
+        (s[group : 2 * group] + s[2 * group : 3 * group]) * f
+        for s, f in zip(stats, factors, strict=True)
+    )
+    factors = [f / bottom for f in factors]
+    row = lax.broadcasted_iota(jnp.int32, (head_rows, head_rows), 0)
+    lane = lax.broadcasted_iota(jnp.int32, (head_rows, head_rows), 1)
     for item in range(group):
         rows = slice(item * head_rows, (item + 1) * head_rows)
-        own_decay = tree_stats[rows, 2:3]
-        tree_top = tree_stats[rows, 0:1]
-        tops = [s[:, 2 * item : 2 * item + 1] + own_decay for s in stats]
-        top = functools.reduce(jnp.maximum, tops, tree_top)
-        factor = jnp.exp2(tree_top - top)
-        bottom = tree_stats[rows, 1:2] * factor
-        upper = tree_acc[rows, :] * factor
+        attended = jnp.zeros((head_rows, head_size), jnp.float32)
         for source in range(kv_size):
-            factor = jnp.exp2(tops[source] - top)
-            bottom = bottom + stats[source][:, 2 * item + 1 : 2 * item + 2] * factor
-            upper = upper + packed[source][rows, :].astype(jnp.float32) * factor
-        attended = (upper / bottom).astype(jnp.bfloat16)
+            spread = jnp.where(row == lane, factors[source][item : item + 1, :], 0.0)
+            high = spread.astype(jnp.bfloat16)
+            low = (spread - high.astype(jnp.float32)).astype(jnp.bfloat16)
+            held_rows = packed[source][rows, :]
+            attended += jnp.dot(high, held_rows, preferred_element_type=jnp.float32)
+            attended += jnp.dot(low, held_rows, preferred_element_type=jnp.float32)
+        attended = attended.astype(jnp.bfloat16)
         for head in range(heads):
             chunk[item * nodes : (item + 1) * nodes, head * head_size : (head + 1) * head_size] = (
                 attended[head * nodes : (head + 1) * nodes, :]
@@ -619,57 +696,77 @@
     vmem = pl.BlockSpec(memory_space=pltpu.VMEM)
     smem = pl.BlockSpec(memory_space=pltpu.SMEM)
     row_parts, depth_parts = 4, 4
-
-    results = pl.pallas_call(
-        functools.partial(attend_kernel, kv_size),
-        name="attend",
-        out_shape=[in_vmem(((group + 1) * head_rows, head_size), bf16) for _ in range(kv_size)]
-        + [
-            in_vmem((group, head_rows, head_size), bf16),
-            in_vmem((group * nodes, head_size), bf16),
-            in_vmem((group * nodes, head_size), bf16),
-            in_vmem((forget_weight.shape[1], group * nodes), f32),
+    packed_shape = in_vmem((group * head_rows + STAT_ROWS, head_size), bf16)
+
+    farthest, normed, queries, new_keys, new_values, keys, values, decays = pl.pallas_call(
+        functools.partial(first_kernel, kv_size),
+        compiler_params=pltpu.CompilerParams(vmem_limit_bytes=GRANT),
+        name="first",
+        out_shape=[
+            packed_shape,
+            in_vmem((rows, width), bf16),
+            in_vmem((seq_count, head_rows, head_size), bf16),
+            in_vmem((rows, head_size), bf16),
+            in_vmem((rows, head_size), bf16),
+            in_vmem((kv_size, group, block_len, head_size), bf16),
+            in_vmem((kv_size, group, block_len, head_size), bf16),
+            in_vmem((seq_count, heads, block_len), f32),
         ],
-        in_specs=[smem, hbm, vmem, hbm, hbm, hbm, vmem, vmem, vmem, hbm, hbm, vmem],
-        out_specs=[vmem] * (kv_size + 4),
+        in_specs=[hbm] * 11,
+        out_specs=[vmem] * 8,
         scratch_shapes=[
+            pltpu.SMEM((seq_count,), jnp.int32),
             pltpu.VMEM((rows, width), bf16),
-            pltpu.VMEM((width, query_cols + 2 * head_size), bf16),
-            pltpu.VMEM((kv_size, group, block_len, head_size), bf16),
-            pltpu.VMEM((kv_size, group, block_len, head_size), bf16),
-            pltpu.VMEM((rows, width), bf16),
+            pltpu.VMEM((1, width), f32),
+            pltpu.VMEM((1, head_size), f32),
+            pltpu.VMEM((1, head_size), f32),
+            pltpu.VMEM((width, query_cols), bf16),
+            pltpu.VMEM((width, head_size), bf16),
+            pltpu.VMEM((width, head_size), bf16),
+            pltpu.VMEM((seq_count, heads, block_len), f32),
             pltpu.VMEM((rows, query_cols + 2 * head_size), f32),
-            pltpu.VMEM((seq_count, head_rows, head_size), bf16),
-            pltpu.VMEM((rows, head_size), bf16),
-            pltpu.VMEM((rows, head_size), bf16),
+            pltpu.SemaphoreType.DMA((5,)),
             pltpu.SemaphoreType.DMA((row_parts,)),
             pltpu.SemaphoreType.DMA((depth_parts, 3)),
             pltpu.SemaphoreType.DMA((kv_size, 2)),
         ],
     )(
-        lengths,
-        tokens.reshape(rows, width),
-        norm_gain.reshape(1, width),
-        query_weight,
-        key_weight,
-        value_weight,
-        forget_weight.T,
-        query_gain.reshape(1, head_size),
-        key_gain.reshape(1, head_size),
-        cache_keys.reshape(seq_count, block_len, head_size),
-        cache_values.reshape(seq_count, block_len, head_size),
-        jnp.swapaxes(cache_logcum, 1, 2),
-    )
-    packed, (own_queries, own_keys, own_values, own_gates) = results[:kv_size], results[kv_size:]
-    moved = {s: exchange(packed[s], "kv", kv_size, s) for s in range(kv_size - 1, 0, -1)}
-    tree_acc, tree_stats = pl.pallas_call(
-        functools.partial(tree_kernel, kv_size, tp_size),
-        name="tree",
-        out_shape=[
-            in_vmem((group * head_rows, head_size), f32),
-            in_vmem((group * head_rows, head_size), f32),
-        ],
-        in_specs=[smem, smem] + [vmem] * 8,
+        *[
+            pltpu.with_memory_space_constraint(a, pltpu.HBM)
+            for a in (
+                lengths,
+                tokens.reshape(rows, width),
+                norm_gain.reshape(1, width),
+                query_weight,
+                key_weight,
+                value_weight,
+                query_gain.reshape(1, head_size),
+                key_gain.reshape(1, head_size),
+                cache_keys.reshape(seq_count, block_len, head_size),
+                cache_values.reshape(seq_count, block_len, head_size),
+                jnp.swapaxes(cache_logcum, 1, 2),
+            )
+        ]
+    )
+    shared = [held(a) for a in (queries, keys, values, decays)]
+    packed = {kv_size - 1: farthest}
+    for step in range(kv_size - 2, 0, -1):
+        packed[step] = pl.pallas_call(
+            functools.partial(next_kernel, step),
+            compiler_params=pltpu.CompilerParams(vmem_limit_bytes=GRANT),
+        out_shape=packed_shape,
+            in_specs=[vmem] * 4,
+            out_specs=vmem,
+        )(*shared)
+    moved = {}
+    for step in range(kv_size - 1, 0, -1):
+        moved[step] = exchange(packed[step], "kv", kv_size, step)
+    own, terms = pl.pallas_call(
+        functools.partial(own_kernel, tp_size),
+        compiler_params=pltpu.CompilerParams(vmem_limit_bytes=GRANT),
+        name="own",
+        out_shape=[packed_shape, in_vmem((8, head_rows), f32)],
+        in_specs=[smem, smem] + [vmem] * 12,
         out_specs=[vmem, vmem],
         scratch_shapes=[pltpu.VMEM((2 * group * nodes, head_size), f32)] * 2,
         cost_estimate=pl.CostEstimate(flops=4_000_000_000, bytes_accessed=1_000_000, transcendentals=0),
@@ -677,35 +774,36 @@
         accepted,
         forget_bias,
         parents,
-        held(own_queries),
-        held(own_keys),
-        held(own_values),
-        held(own_gates),
+        forget_weight.T,
         pending_keys.reshape(seq_count, most_taken, head_size),
         pending_values.reshape(seq_count, most_taken, head_size),
         jnp.transpose(pending_logcum, (1, 2, 0)),
+        held(normed),
+        shared[0],
+        held(new_keys),
+        held(new_values),
+        *shared[1:],
     )
     chunk = pl.pallas_call(
         functools.partial(merge_kernel, kv_size),
+        compiler_params=pltpu.CompilerParams(vmem_limit_bytes=GRANT),
         name="merge",
         out_shape=in_vmem((group * nodes, query_cols), bf16),
-        in_specs=[vmem] * (kv_size + 2),
+        in_specs=[vmem] * (kv_size + 1),
         out_specs=vmem,
-    )(
-        held(tree_acc),
-        held(tree_stats),
-        held(packed[0]),
-        *[held(moved[s]) for s in range(1, kv_size)],
-    )
-    chunks = [chunk] + [exchange(chunk, "kv", kv_size, s) for s in range(1, kv_size)]
+    )(held(terms), held(own), *[held(moved[s]) for s in range(1, kv_size)])
+    chunks = {0: chunk}
+    for step in range(kv_size - 1, 0, -1):
+        chunks[step] = exchange(chunk, "kv", kv_size, step)
     cols = output_weight.shape[1] // tp_size
     kept, sent = pl.pallas_call(
         functools.partial(project_kernel, kv_size),
+        compiler_params=pltpu.CompilerParams(vmem_limit_bytes=GRANT),
         name="project",
         out_shape=[in_vmem((rows, cols), bf16), in_vmem((rows, cols), bf16)],
         in_specs=[vmem] * (kv_size + 1),
         out_specs=[vmem, vmem],
-    )(held(output_weight), *[held(c) for c in chunks])
+    )(held(output_weight), *[held(chunks[c]) for c in range(kv_size)])
     received = exchange(sent, "tp", tp_size, 1)
     summed = (kept.astype(f32) + received.astype(f32)).astype(bf16)
     return summed.reshape(seq_count, nodes, cols)
@@ -724,7 +822,9 @@
         shapes = {"tokens": args[0].shape, "cache_keys": args[10].shape}
         shapes["tokens"] = (shapes["tokens"][0] * mesh.shape["dp"],)
         shapes["cache_keys"] = (0, 0, shapes["cache_keys"][2] * mesh.shape["tp"])
-        return (fast_shards if fits_fast(mesh, shapes) else shards)(*args)
+        if not fits_fast(mesh, shapes):
+            return shards(*args)
+        return fast_shards(*args)
 
     return run
 

time: 35 us -> 28.9 us (0.83)
  Pallas kernels: 14.5 us -> 8.82 us
  waiting for transfers between devices: 9.26 us -> 8.78 us
    pallas_call x4 -> x6, Pallas kernels: 14.5 us -> 8.82 us  [the longest x1 5.19 us: fast_shards(): pl.pallas_call(functools.partial(first_kernel, kv_size), compiler_params=...]
    ppermute x7, waiting for transfers between devices: 9.26 us -> 8.78 us  [exchange(): return lax.ppermute(array, axis, [(i, i ^ step) for i in range(size)])]
  transfers between devices with their start and end apart: 7 -> 7, of which waited for: 4 -> 5; matrix products, arithmetic and copies ran while one was open for 0% -> 0% of each run, Pallas kernels for 7% -> 8%
where the time goes in v2:
time: 28.9 us; the launch traced here: 28.7 us
  starting transfers between devices  10.2 us (35%)
  Pallas kernels  8.82 us (31%)
  waiting for transfers between devices  8.78 us (30%)
  other arithmetic  0.69 us (2%)
    ppermute x7, starting transfers between devices, exchange(): return lax.ppermute(array, axis, [(i, i ^ step) for i in range(size)])  10.2 us
    ppermute x7, waiting for transfers between devices, exchange(): return lax.ppermute(array, axis, [(i, i ^ step) for i in range(size)])  8.78 us
    pallas_call x1, Pallas kernels, fast_shards(): pl.pallas_call(functools.partial(first_kernel, kv_size), compiler_params=...  5.19 us
    pallas_call x1, Pallas kernels, fast_shards(): pl.pallas_call(functools.partial(own_kernel, tp_size), compiler_params=pl...  1.94 us
    pallas_call x2, Pallas kernels, fast_shards(): pl.pallas_call(functools.partial(next_kernel, step), compiler_params=pltp...  0.9 us
    convert_element_type x1, other arithmetic, fast_shards(): summed = (kept.astype(f32) + received.astype(f32)).astype(bf16)  0.69 us
  transfers between devices with their start and end apart: 7, of which 5 were waited for; matrix products, arithmetic and copies ran while one was open for 0% of the time, Pallas kernels for 8%

profile of v2, /device:TPU:0, one launch (start us, length us, event | category | flops | bytes accessed | tf_op | source)
XLA Modules:
  0.0 28.7 jit_solution(8357726730612963150)
XLA Ops:
  0.0 5.2 %first.1 = (bf16[272,128]{1,0:T(8,128)(2,1)S(1)}, bf16[256,2048]{1,0:T(8,128)(2,1)S(1)}, bf16[16,64,128]{2,1,0:T(8,128)(2,1)S(1)}, bf16[256,128]{1,0:T(8,128)(2,...) custom-call(s32[16]{0:T(128)} %lengths.1, ...), custom_call_target="tpu_custom_call" | custom-call | tf_op jit(solution)/shard_map/first/pallas_call | solution.py:701
  5.2 0.0 copy-start.1
  5.2 0.0 copy-start.2
  5.2 0.0 copy-start.3
  5.2 0.0 copy-start.4
  5.2 0.0 copy-start.5
  5.3 0.0 copy-start.6
  5.3 0.0 copy-start.7
  5.3 0.5 %shard_map.181 = bf16[272,128]{1,0:T(8,128)(2,1)S(1)} custom-call(bf16[16,64,128]{2,1,0:T(8,128)(2,1)S(1)} %get-tuple-element.18.queries, bf16[4,4,256,128]{3,2,1,0:T(8,128)(2,1)S(1)} %get-tuple-element.21.keys, bf16[4,4,256,128]{3,2,1,0:T(8,128)(2,1)S(1)} %get-tuple-element.22.values, f32[16,4,256]{2,1,0:T(4,128)S(1)} %get-tuple-element.23.decays), custom_call_target="tpu_custom_call" | custom-call | tf_op jit(solution)/shard_map/pallas_call | solution.py:754
  5.7 3.1 %collective-permute-start = (bf16[272,128]{1,0:T(8,128)(2,1)S(1)}, bf16[272,128]{1,0:T(8,128)(2,1)S(1)}, u32[]{:S(2)}, u32[]{:S(2)}) collective-permute-start(bf16[272,128]{1,0:T(8,128)(2,1)S(1)} %shard_map.181), channel_id=1, source_target_pairs={{0,2},{2,0},{4,6},{6,4},{1,3},{3,1},{5,7},{7,5},{8,10},{10,8},{12,... | collective-permute-start | bytes 208904 | tf_op jit(solution)/shard_map/ppermute | solution.py:660
  8.8 0.4 %shard_map.182 = bf16[272,128]{1,0:T(8,128)(2,1)S(1)} custom-call(bf16[16,64,128]{2,1,0:T(8,128)(2,1)S(1)} %get-tuple-element.18.queries, bf16[4,4,256,128]{3,2,1,0:T(8,128)(2,1)S(1)} %get-tuple-element.21.keys, bf16[4,4,256,128]{3,2,1,0:T(8,128)(2,1)S(1)} %get-tuple-element.22.values, f32[16,4,256]{2,1,0:T(4,128)S(1)} %get-tuple-element.23.decays), custom_call_target="tpu_custom_call" | custom-call | tf_op jit(solution)/shard_map/pallas_call | solution.py:754
  9.3 2.7 %collective-permute-start.1 = (bf16[272,128]{1,0:T(8,128)(2,1)S(1)}, bf16[272,128]{1,0:T(8,128)(2,1)S(1)}, u32[]{:S(2)}, u32[]{:S(2)}) collective-permute-start(bf16[272,128]{1,0:T(8,128)(2,1)S(1)} %shard_map.182), channel_id=1, source_target_pairs={{0,4},{2,6},{4,0},{6,2},{1,5},{3,7},{5,1},{7,3},{8,12},{10,14},{12... | collective-permute-start | bytes 208904 | tf_op jit(solution)/shard_map/ppermute | solution.py:660
  12.0 0.0 collective-permute-start.2
  12.0 0.0 copy-done.1
  12.0 0.0 copy-done.2
  12.0 0.0 copy-done.3
  12.0 0.0 copy-start
  12.0 1.9 %own.1 = (bf16[272,128]{1,0:T(8,128)(2,1)S(1)}, f32[8,64]{1,0:T(8,128)S(1)}) custom-call(s32[16]{0:T(128)S(1)} %copy-done.6, f32[8]{0:T(128)S(1)} %copy-done.7, s32[16,16]{1,0:T(8,128)S(1)} %copy-done.4, bf16[8,2048]{1,0:T(8,128)(2,1)S(1)} %bitcast.12, bf16[16,4,128]{2,1,0:T(4,128)(2,1)S(1)} %bitcast.13, bf16[16,4,128]{2,1,0:T(4,128)(2,1)S(1)} %bitcast.14, ...), custom_call_target="tpu_custom_call" | custom-call | flops 4000000000 | bytes 1000000 | tf_op jit(solution)/shard_map/own/pallas_call | solution.py:764
  14.0 0.0 collective-permute-done.refs_1_
  14.0 2.8 %collective-permute-done.1.refs_2_ = bf16[272,128]{1,0:T(8,128)(2,1)S(1)} collective-permute-done((bf16[272,128]{1,0:T(8,128)(2,1)S(1)}, bf16[272,128]{1,0:T(8,128)(2,1)S(1)}, u32[]{:S(2)}, u32[]{:S(2)}) %collective-permute-start.1) | collective-permute-done | bytes 69664 | tf_op jit(solution)/shard_map/ppermute | solution.py:660
  16.8 1.4 %collective-permute-done.2.refs_3_ = bf16[272,128]{1,0:T(8,128)(2,1)S(1)} collective-permute-done((bf16[272,128]{1,0:T(8,128)(2,1)S(1)}, bf16[272,128]{1,0:T(8,128)(2,1)S(1)}, u32[]{:S(2)}, u32[]{:S(2)}) %collective-permute-start.2) | collective-permute-done | bytes 69664 | tf_op jit(solution)/shard_map/ppermute | solution.py:660
  18.2 0.3 %merge.1.refs_0_ = bf16[64,512]{1,0:T(8,128)(2,1)S(1)} custom-call(f32[8,64]{1,0:T(8,128)S(1)} %get-tuple-element.24.terms, bf16[272,128]{1,0:T(8,128)(2,1)S(1)} %get-tuple-element.25.refs_0_, bf16[272,128]{1,0:T(8,128)(2,1)S(1)} %collective-permute-done.refs_1_, bf16[272,128]{1,0:T(8,128)(2,1)S(1)} %collective-permute-done.1.refs_2_, ...), custom_call_target="tpu_custom_call" | custom-call | tf_op jit(solution)/shard_map/merge/pallas_call | solution.py:787
  18.5 1.9 %collective-permute-start.5 = (bf16[64,512]{1,0:T(8,128)(2,1)S(1)}, bf16[64,512]{1,0:T(8,128)(2,1)S(1)}, u32[]{:S(2)}, u32[]{:S(2)}) collective-permute-start(bf16[64,512]{1,0:T(8,128)(2,1)S(1)} %merge.1.refs_0_), channel_id=1, source_target_pairs={{0,6},{2,4},{4,2},{6,0},{1,7},{3,5},{5,3},{7,1},{8,14},{10,12},{12... | collective-permute-start | bytes 196616 | tf_op jit(solution)/shard_map/ppermute | solution.py:660
  20.4 0.3 %collective-permute-start.4 = (bf16[64,512]{1,0:T(8,128)(2,1)S(1)}, bf16[64,512]{1,0:T(8,128)(2,1)S(1)}, u32[]{:S(2)}, u32[]{:S(2)}) collective-permute-start(bf16[64,512]{1,0:T(8,128)(2,1)S(1)} %merge.1.refs_0_), channel_id=1, source_target_pairs={{0,4},{2,6},{4,0},{6,2},{1,5},{3,7},{5,1},{7,3},{8,12},{10,14},{12... | collective-permute-start | bytes 196616 | tf_op jit(solution)/shard_map/ppermute | solution.py:660
  20.7 2.2 %collective-permute-start.3 = (bf16[64,512]{1,0:T(8,128)(2,1)S(1)}, bf16[64,512]{1,0:T(8,128)(2,1)S(1)}, u32[]{:S(2)}, u32[]{:S(2)}) collective-permute-start(bf16[64,512]{1,0:T(8,128)(2,1)S(1)} %merge.1.refs_0_), channel_id=1, source_target_pairs={{0,2},{2,0},{4,6},{6,4},{1,3},{3,1},{5,7},{7,5},{8,10},{10,8},{12,... | collective-permute-start | bytes 196616 | tf_op jit(solution)/shard_map/ppermute | solution.py:660
  22.9 1.7 %collective-permute-done.5.refs_3_ = bf16[64,512]{1,0:T(8,128)(2,1)S(1)} collective-permute-done((bf16[64,512]{1,0:T(8,128)(2,1)S(1)}, bf16[64,512]{1,0:T(8,128)(2,1)S(1)}, u32[]{:S(2)}, u32[]{:S(2)}) %collective-permute-start.5) | collective-permute-done | bytes 65568 | tf_op jit(solution)/shard_map/ppermute | solution.py:660
  24.6 1.6 %collective-permute-done.4.refs_2_ = bf16[64,512]{1,0:T(8,128)(2,1)S(1)} collective-permute-done((bf16[64,512]{1,0:T(8,128)(2,1)S(1)}, bf16[64,512]{1,0:T(8,128)(2,1)S(1)}, u32[]{:S(2)}, u32[]{:S(2)}) %collective-permute-start.4) | collective-permute-done | bytes 65568 | tf_op jit(solution)/shard_map/ppermute | solution.py:660
  26.1 0.0 collective-permute-done.3.refs_1_
  26.1 0.5 %project.1 = (bf16[256,256]{1,0:T(8,128)(2,1)S(1)}, bf16[256,256]{1,0:T(8,128)(2,1)S(1)}) custom-call(bf16[512,512]{1,0:T(8,128)(2,1)S(1)} %copy-done, bf16[64,512]{1,0:T(8,128)(2,1)S(1)} %merge.1.refs_0_, bf16[64,512]{1,0:T(8,128)(2,1)S(1)} %collective-permute-done.3.refs_1_, bf16[64,512]{1,0:T(8,128)(2,1)S(1)} %collective-permute-done.4.refs_2_, ...), custom_call_target="tpu_custom_call" | custom-call | tf_op jit(solution)/shard_map/project/pallas_call | solution.py:799
  26.6 0.1 collective-permute-start.6
  26.7 1.3 %collective-permute-done.6 = bf16[256,256]{1,0:T(8,128)(2,1)S(1)} collective-permute-done((bf16[256,256]{1,0:T(8,128)(2,1)S(1)}, bf16[256,256]{1,0:T(8,128)(2,1)S(1)}, u32[]{:S(2)}, u32[]{:S(2)}) %collective-permute-start.6) | collective-permute-done | bytes 131104 | tf_op jit(solution)/shard_map/ppermute | solution.py:660
  28.0 0.7 %add_convert_fusion = bf16[256,256]{1,0:T(8,128)(2,1)} fusion(bf16[256,256]{1,0:T(8,128)(2,1)S(1)} %collective-permute-done.6, bf16[256,256]{1,0:T(8,128)(2,1)S(1)} %get-tuple-element.27), kind=kLoop, calls=%fused_computation | loop fusion | flops 262144 | bytes 393216 | tf_op jit(solution)/shard_map/convert_element_type | solution.py:808
  (5 shorter events, 0.0 us)
Async XLA Ops:
  5.2 6.8 %copy-start.1 = (bf16[2048,8]{0,1:T(8,128)(2,1)S(1)}, bf16[2048,8]{0,1:T(8,128)(2,1)}, u32[]{:S(2)}) copy-start(bf16[2048,8]{0,1:T(8,128)(2,1)} %param.24) | copy-start | bytes 98308
  5.2 6.7 %copy-start.2 = (bf16[16,4,1,128]{3,1,2,0:T(4,128)(2,1)S(1)}, bf16[16,4,1,128]{3,1,2,0:T(4,128)(2,1)}, u32[]{:S(2)}) copy-start(bf16[16,4,1,128]{3,1,2,0:T(4,128)(2,1)} %param.32) | copy-start | bytes 49156
  5.2 6.7 %copy-start.3 = (bf16[16,4,1,128]{3,1,2,0:T(4,128)(2,1)S(1)}, bf16[16,4,1,128]{3,1,2,0:T(4,128)(2,1)}, u32[]{:S(2)}) copy-start(bf16[16,4,1,128]{3,1,2,0:T(4,128)(2,1)} %param.33) | copy-start | bytes 49156
  5.2 6.7 %copy-start.4 = (s32[16,16]{1,0:T(8,128)S(1)}, s32[16,16]{1,0:T(8,128)}, u32[]{:S(2)}) copy-start(s32[16,16]{1,0:T(8,128)} %parents.1) | copy-start | bytes 3076
  5.2 6.7 %copy-start.5 = (f32[16,4,4]{0,2,1:T(4,128)S(1)}, f32[16,4,4]{0,2,1:T(4,128)}, u32[]{:S(2)}) copy-start(f32[16,4,4]{0,2,1:T(4,128)} %param.34) | copy-start | bytes 3076
  5.3 6.7 %copy-start.6 = (s32[16]{0:T(128)S(1)}, s32[16]{0:T(128)}, u32[]{:S(2)}) copy-start(s32[16]{0:T(128)} %accepted.1) | copy-start | bytes 196
  5.3 6.7 %copy-start.7 = (f32[8]{0:T(128)S(1)}, f32[8]{0:T(128)}, u32[]{:S(2)}) copy-start(f32[8]{0:T(128)} %forget_bias.1) | copy-start | bytes 100
  5.7 8.2 %collective-permute-start = (bf16[272,128]{1,0:T(8,128)(2,1)S(1)}, bf16[272,128]{1,0:T(8,128)(2,1)S(1)}, u32[]{:S(2)}, u32[]{:S(2)}) collective-permute-start(bf16[272,128]{1,0:T(8,128)(2,1)S(1)} %shard_map.181), channel_id=1, source_target_pairs={{0,2},{2,0},{4,6},{6,4},{1,3},{3,1},{5,7},{7,5},{8,10},{10,8},{12,... | collective-permute-start | bytes 208904 | tf_op jit(solution)/shard_map/ppermute | solution.py:660
  9.3 7.5 %collective-permute-start.1 = (bf16[272,128]{1,0:T(8,128)(2,1)S(1)}, bf16[272,128]{1,0:T(8,128)(2,1)S(1)}, u32[]{:S(2)}, u32[]{:S(2)}) collective-permute-start(bf16[272,128]{1,0:T(8,128)(2,1)S(1)} %shard_map.182), channel_id=1, source_target_pairs={{0,4},{2,6},{4,0},{6,2},{1,5},{3,7},{5,1},{7,3},{8,12},{10,14},{12... | collective-permute-start | bytes 208904 | tf_op jit(solution)/shard_map/ppermute | solution.py:660
  12.0 6.2 %collective-permute-start.2 = (bf16[272,128]{1,0:T(8,128)(2,1)S(1)}, bf16[272,128]{1,0:T(8,128)(2,1)S(1)}, u32[]{:S(2)}, u32[]{:S(2)}) collective-permute-start(bf16[272,128]{1,0:T(8,128)(2,1)S(1)} %get-tuple-element.26), channel_id=1, source_target_pairs={{0,6},{2,4},{4,2},{6,0},{1,7},{3,5},{5,3},{7,1},{8,14},{10,12},{12... | collective-permute-start | bytes 208904 | tf_op jit(solution)/shard_map/ppermute | solution.py:660
  12.0 14.1 %copy-start = (bf16[512,512]{1,0:T(8,128)(2,1)S(1)}, bf16[512,512]{1,0:T(8,128)(2,1)}, u32[]{:S(2)}) copy-start(bf16[512,512]{1,0:T(8,128)(2,1)} %weight.1) | copy-start | bytes 1572868
  18.5 6.1 %collective-permute-start.5 = (bf16[64,512]{1,0:T(8,128)(2,1)S(1)}, bf16[64,512]{1,0:T(8,128)(2,1)S(1)}, u32[]{:S(2)}, u32[]{:S(2)}) collective-permute-start(bf16[64,512]{1,0:T(8,128)(2,1)S(1)} %merge.1.refs_0_), channel_id=1, source_target_pairs={{0,6},{2,4},{4,2},{6,0},{1,7},{3,5},{5,3},{7,1},{8,14},{10,12},{12... | collective-permute-start | bytes 196616 | tf_op jit(solution)/shard_map/ppermute | solution.py:660
  20.4 5.7 %collective-permute-start.4 = (bf16[64,512]{1,0:T(8,128)(2,1)S(1)}, bf16[64,512]{1,0:T(8,128)(2,1)S(1)}, u32[]{:S(2)}, u32[]{:S(2)}) collective-permute-start(bf16[64,512]{1,0:T(8,128)(2,1)S(1)} %merge.1.refs_0_), channel_id=1, source_target_pairs={{0,4},{2,6},{4,0},{6,2},{1,5},{3,7},{5,1},{7,3},{8,12},{10,14},{12... | collective-permute-start | bytes 196616 | tf_op jit(solution)/shard_map/ppermute | solution.py:660
  20.7 5.4 %collective-permute-start.3 = (bf16[64,512]{1,0:T(8,128)(2,1)S(1)}, bf16[64,512]{1,0:T(8,128)(2,1)S(1)}, u32[]{:S(2)}, u32[]{:S(2)}) collective-permute-start(bf16[64,512]{1,0:T(8,128)(2,1)S(1)} %merge.1.refs_0_), channel_id=1, source_target_pairs={{0,2},{2,0},{4,6},{6,4},{1,3},{3,1},{5,7},{7,5},{8,10},{10,8},{12,... | collective-permute-start | bytes 196616 | tf_op jit(solution)/shard_map/ppermute | solution.py:660
  26.6 1.4 %collective-permute-start.6 = (bf16[256,256]{1,0:T(8,128)(2,1)S(1)}, bf16[256,256]{1,0:T(8,128)(2,1)S(1)}, u32[]{:S(2)}, u32[]{:S(2)}) collective-permute-start(bf16[256,256]{1,0:T(8,128)(2,1)S(1)} %get-tuple-element.28), channel_id=1, source_target_pairs={{0,1},{1,0},{2,3},{3,2},{4,5},{5,4},{6,7},{7,6},{8,9},{9,8},{10,11... | collective-permute-start | bytes 393224 | tf_op jit(solution)/shard_map/ppermute | solution.py:660

commit v3 on v2

--- a/solution.py
+++ b/solution.py
@@ -310,24 +310,24 @@
     )
 
 
+def unit(vectors, gain_vec):
+    mean = jnp.mean(vectors * vectors, axis=1, keepdims=True)
+    return (vectors * lax.rsqrt(mean + EPSILON) * gain_vec).astype(jnp.bfloat16)
+
+
 def first_kernel(
     kv_size,
     lengths,
     tokens,
     norm_gain,
     query_weight,
-    key_weight,
-    value_weight,
     query_gain,
-    key_gain,
     cache_keys,
     cache_values,
     cache_logcum,
     packed,
     normed,
     queries,
-    new_keys,
-    new_values,
     key_buf,
     value_buf,
     decay_buf,
@@ -335,10 +335,7 @@
     token_buf,
     gain_buf,
     query_gain_buf,
-    key_gain_buf,
     query_weight_buf,
-    key_weight_buf,
-    value_weight_buf,
     logcum_buf,
     summed_buf,
     small_sem,
@@ -349,7 +346,7 @@
     place = lax.axis_index("kv")
     rows, width = tokens.shape
     query_cols = query_weight.shape[1]
-    head_size = key_weight.shape[1]
+    head_size = query_gain.shape[1]
     heads = query_cols // head_size
     seq_count, block_len = cache_keys.shape[0], cache_keys.shape[1]
     nodes = rows // seq_count
@@ -375,20 +372,12 @@
                 (lengths, length_buf),
                 (norm_gain, gain_buf),
                 (query_gain, query_gain_buf),
-                (key_gain, key_gain_buf),
                 (cache_logcum, logcum_buf),
             )
         )
     ]
     token_copies = spans(tokens, token_buf, lambda i: token_sem.at[i], rows, row_parts)
-    weight_copies = list(
-        zip(
-            spans(query_weight, query_weight_buf, lambda i: weight_sem.at[i, 0], width, depth_parts),
-            spans(key_weight, key_weight_buf, lambda i: weight_sem.at[i, 1], width, depth_parts),
-            spans(value_weight, value_weight_buf, lambda i: weight_sem.at[i, 2], width, depth_parts),
-            strict=True,
-        )
-    )
+    weight_copies = spans(query_weight, query_weight_buf, lambda i: weight_sem.at[i], width, depth_parts)
     cache_copies = []
     for step in range(kv_size):
         span = pl.ds(partner_of(place, step) * group, group)
@@ -401,10 +390,9 @@
     small[1].start()
     for copy in token_copies:
         copy.start()
-    for copies in weight_copies:
-        for copy in copies:
-            copy.start()
-    for i in (0, 2, 3, 4):
+    for copy in weight_copies:
+        copy.start()
+    for i in (0, 2, 3):
         small[i].start()
     for step in range(kv_size - 1, -1, -1):
         for copy in cache_copies[step]:
@@ -422,21 +410,16 @@
             ).astype(jnp.bfloat16)
 
     for part in range(depth_parts):
-        for copy in weight_copies[part]:
-            copy.wait()
+        weight_copies[part].wait()
         span = pl.ds(part * depth, depth)
-        left = normed[:, span]
-        both = jnp.concatenate([key_weight_buf[span, :], value_weight_buf[span, :]], axis=1)
-        for target, right in (
-            (pl.ds(0, query_cols), query_weight_buf[span, :]),
-            (pl.ds(query_cols, 2 * head_size), both),
-        ):
-            product = jnp.dot(left, right, preferred_element_type=jnp.float32)
-            if part == 0:
-                summed_buf[:, target] = product
-            else:
-                summed_buf[:, target] += product
-    for i in (0, 2, 3, 4):
+        product = jnp.dot(
+            normed[:, span], query_weight_buf[span, :], preferred_element_type=jnp.float32
+        )
+        if part == 0:
+            summed_buf[...] = product
+        else:
+            summed_buf[...] += product
+    for i in (0, 2, 3):
         small[i].wait()
 
     column = lax.broadcasted_iota(jnp.int32, (heads, block_len), 1)
@@ -444,21 +427,13 @@
         valid = length_buf[seq] - place * block_len
         decay_buf[seq] = jnp.where(column < valid, logcum_buf[seq] * LOG2E, MASKED)
 
-    def head_norm(vectors, gain_vec):
-        mean = jnp.mean(vectors * vectors, axis=1, keepdims=True)
-        return (vectors * lax.rsqrt(mean + EPSILON) * gain_vec).astype(jnp.bfloat16)
-
     for head in range(heads):
-        normal = head_norm(
+        normal = unit(
             summed_buf[:, head * head_size : (head + 1) * head_size], query_gain_buf[...]
         )
         queries[:, head * nodes : (head + 1) * nodes, :] = normal.reshape(
             seq_count, nodes, head_size
         )
-    new_keys[...] = head_norm(
-        summed_buf[:, query_cols : query_cols + head_size], key_gain_buf[...]
-    )
-    new_values[...] = summed_buf[:, query_cols + head_size :].astype(jnp.bfloat16)
     for step in range(kv_size - 1, -1, -1):
         for copy in cache_copies[step]:
             copy.wait()
@@ -493,10 +468,11 @@
     pending_keys,
     pending_values,
     pending_logcum,
+    key_weight,
+    value_weight,
+    key_gain,
     normed,
     queries,
-    new_keys,
-    new_values,
     keys,
     values,
     decays,
@@ -518,8 +494,13 @@
 
     key_buf[...] = jnp.zeros_like(key_buf)
     value_buf[...] = jnp.zeros_like(value_buf)
-    key_buf[:tree_rows, :] = new_keys[own_rows, :].astype(jnp.float32)
-    value_buf[:tree_rows, :] = new_values[own_rows, :].astype(jnp.float32)
+    summed = jnp.dot(
+        normed[own_rows, :],
+        jnp.concatenate([key_weight[...], value_weight[...]], axis=1),
+        preferred_element_type=jnp.float32,
+    )
+    key_buf[:tree_rows, :] = unit(summed[:, :head_size], key_gain[...]).astype(jnp.float32)
+    value_buf[:tree_rows, :] = summed[:, head_size:]
     for item in range(group):
         rows = slice(tree_rows + item * most_taken, tree_rows + (item + 1) * most_taken)
         key_buf[rows, :] = pending_keys[place * group + item].astype(jnp.float32)
@@ -698,7 +679,7 @@
     row_parts, depth_parts = 4, 4
     packed_shape = in_vmem((group * head_rows + STAT_ROWS, head_size), bf16)
 
-    farthest, normed, queries, new_keys, new_values, keys, values, decays = pl.pallas_call(
+    farthest, normed, queries, keys, values, decays = pl.pallas_call(
         functools.partial(first_kernel, kv_size),
         compiler_params=pltpu.CompilerParams(vmem_limit_bytes=GRANT),
         name="first",
@@ -706,28 +687,23 @@
             packed_shape,
             in_vmem((rows, width), bf16),
             in_vmem((seq_count, head_rows, head_size), bf16),
-            in_vmem((rows, head_size), bf16),
-            in_vmem((rows, head_size), bf16),
             in_vmem((kv_size, group, block_len, head_size), bf16),
             in_vmem((kv_size, group, block_len, head_size), bf16),
             in_vmem((seq_count, heads, block_len), f32),
         ],
-        in_specs=[hbm] * 11,
-        out_specs=[vmem] * 8,
+        in_specs=[hbm] * 8,
+        out_specs=[vmem] * 6,
         scratch_shapes=[
             pltpu.SMEM((seq_count,), jnp.int32),
             pltpu.VMEM((rows, width), bf16),
             pltpu.VMEM((1, width), f32),
             pltpu.VMEM((1, head_size), f32),
-            pltpu.VMEM((1, head_size), f32),
             pltpu.VMEM((width, query_cols), bf16),
-            pltpu.VMEM((width, head_size), bf16),
-            pltpu.VMEM((width, head_size), bf16),
             pltpu.VMEM((seq_count, heads, block_len), f32),
-            pltpu.VMEM((rows, query_cols + 2 * head_size), f32),
-            pltpu.SemaphoreType.DMA((5,)),
+            pltpu.VMEM((rows, query_cols), f32),
+            pltpu.SemaphoreType.DMA((4,)),
             pltpu.SemaphoreType.DMA((row_parts,)),
-            pltpu.SemaphoreType.DMA((depth_parts, 3)),
+            pltpu.SemaphoreType.DMA((depth_parts,)),
             pltpu.SemaphoreType.DMA((kv_size, 2)),
         ],
     )(
@@ -738,10 +714,7 @@
                 tokens.reshape(rows, width),
                 norm_gain.reshape(1, width),
                 query_weight,
-                key_weight,
-                value_weight,
                 query_gain.reshape(1, head_size),
-                key_gain.reshape(1, head_size),
                 cache_keys.reshape(seq_count, block_len, head_size),
                 cache_values.reshape(seq_count, block_len, head_size),
                 jnp.swapaxes(cache_logcum, 1, 2),
@@ -766,7 +739,7 @@
         compiler_params=pltpu.CompilerParams(vmem_limit_bytes=GRANT),
         name="own",
         out_shape=[packed_shape, in_vmem((8, head_rows), f32)],
-        in_specs=[smem, smem] + [vmem] * 12,
+        in_specs=[smem, smem] + [vmem] * 13,
         out_specs=[vmem, vmem],
         scratch_shapes=[pltpu.VMEM((2 * group * nodes, head_size), f32)] * 2,
         cost_estimate=pl.CostEstimate(flops=4_000_000_000, bytes_accessed=1_000_000, transcendentals=0),
@@ -778,11 +751,11 @@
         pending_keys.reshape(seq_count, most_taken, head_size),
         pending_values.reshape(seq_count, most_taken, head_size),
         jnp.transpose(pending_logcum, (1, 2, 0)),
+        held(key_weight),
+        held(value_weight),
+        key_gain.reshape(1, head_size),
         held(normed),
-        shared[0],
-        held(new_keys),
-        held(new_values),
-        *shared[1:],
+        *shared,
     )
     chunk = pl.pallas_call(
         functools.partial(merge_kernel, kv_size),

time: 28.9 us -> 27.9 us (0.965)
  Pallas kernels: 8.82 us -> 7.92 us
    pallas_call x1, Pallas kernels: 5.19 us -> 4.13 us  [fast_shards(): pl.pallas_call(functools.partial(first_kernel, kv_size), compiler_params=...]
  transfers between devices with their start and end apart: 7 -> 7, of which waited for: 5 -> 5; matrix products, arithmetic and copies ran while one was open for 0% -> 0% of each run, Pallas kernels for 8% -> 9%
where the time goes in v3:
time: 27.9 us; the launch traced here: 27.7 us
  starting transfers between devices  10.2 us (37%)
  waiting for transfers between devices  8.6 us (31%)
  Pallas kernels  7.92 us (28%)
  other arithmetic  0.69 us (2%)
    ppermute x7, starting transfers between devices, exchange(): return lax.ppermute(array, axis, [(i, i ^ step) for i in range(size)])  10.2 us
    ppermute x7, waiting for transfers between devices, exchange(): return lax.ppermute(array, axis, [(i, i ^ step) for i in range(size)])  8.6 us
    pallas_call x1, Pallas kernels, fast_shards(): pl.pallas_call(functools.partial(first_kernel, kv_size), compiler_params=...  4.13 us
    pallas_call x1, Pallas kernels, fast_shards(): pl.pallas_call(functools.partial(own_kernel, tp_size), compiler_params=pl...  2.11 us
    pallas_call x2, Pallas kernels, fast_shards(): pl.pallas_call(functools.partial(next_kernel, step), compiler_params=pltp...  0.9 us
    convert_element_type x1, other arithmetic, fast_shards(): summed = (kept.astype(f32) + received.astype(f32)).astype(bf16)  0.69 us
  transfers between devices with their start and end apart: 7, of which 5 were waited for; matrix products, arithmetic and copies ran while one was open for 0% of the time, Pallas kernels for 9%

profile of v3, /device:TPU:0, one launch (start us, length us, event | category | flops | bytes accessed | tf_op | source)
XLA Modules:
  0.0 27.7 jit_solution(14737363612839971042)
XLA Ops:
  0.0 4.1 %first.1 = (bf16[272,128]{1,0:T(8,128)(2,1)S(1)}, bf16[256,2048]{1,0:T(8,128)(2,1)S(1)}, bf16[16,64,128]{2,1,0:T(8,128)(2,1)S(1)}, bf16[4,4,256,128]{3,2,1,0:T(8...) custom-call(s32[16]{0:T(128)} %lengths.1, bf16[256,2048]{1,0:T(8,128)(2,1)} %bitcast.17, ...), custom_call_target="tpu_custom_call" | custom-call | tf_op jit(solution)/shard_map/first/pallas_call | solution.py:682
  4.1 0.0 copy-start.1
  4.2 0.0 copy-start.2
  4.2 0.0 copy-start.3
  4.2 0.0 copy-start.4
  4.2 0.0 copy-start.5
  4.2 0.0 copy-start.6
  4.2 0.0 copy-start.7
  4.2 0.0 copy-start.8
  4.2 0.0 copy-start.9
  4.2 0.0 copy-start.10
  4.3 0.4 %shard_map.181 = bf16[272,128]{1,0:T(8,128)(2,1)S(1)} custom-call(bf16[16,64,128]{2,1,0:T(8,128)(2,1)S(1)} %get-tuple-element.16.queries, bf16[4,4,256,128]{3,2,1,0:T(8,128)(2,1)S(1)} %get-tuple-element.17.keys, bf16[4,4,256,128]{3,2,1,0:T(8,128)(2,1)S(1)} %get-tuple-element.18.values, f32[16,4,256]{2,1,0:T(4,128)S(1)} %get-tuple-element.19.decays), custom_call_target="tpu_custom_call" | custom-call | tf_op jit(solution)/shard_map/pallas_call | solution.py:727
  4.7 3.1 %collective-permute-start = (bf16[272,128]{1,0:T(8,128)(2,1)S(1)}, bf16[272,128]{1,0:T(8,128)(2,1)S(1)}, u32[]{:S(2)}, u32[]{:S(2)}) collective-permute-start(bf16[272,128]{1,0:T(8,128)(2,1)S(1)} %shard_map.181), channel_id=1, source_target_pairs={{0,2},{2,0},{4,6},{6,4},{1,3},{3,1},{5,7},{7,5},{8,10},{10,8},{12,... | collective-permute-start | bytes 208904 | tf_op jit(solution)/shard_map/ppermute | solution.py:641
  7.8 0.4 %shard_map.182 = bf16[272,128]{1,0:T(8,128)(2,1)S(1)} custom-call(bf16[16,64,128]{2,1,0:T(8,128)(2,1)S(1)} %get-tuple-element.16.queries, bf16[4,4,256,128]{3,2,1,0:T(8,128)(2,1)S(1)} %get-tuple-element.17.keys, bf16[4,4,256,128]{3,2,1,0:T(8,128)(2,1)S(1)} %get-tuple-element.18.values, f32[16,4,256]{2,1,0:T(4,128)S(1)} %get-tuple-element.19.decays), custom_call_target="tpu_custom_call" | custom-call | tf_op jit(solution)/shard_map/pallas_call | solution.py:727
  8.3 2.6 %collective-permute-start.1 = (bf16[272,128]{1,0:T(8,128)(2,1)S(1)}, bf16[272,128]{1,0:T(8,128)(2,1)S(1)}, u32[]{:S(2)}, u32[]{:S(2)}) collective-permute-start(bf16[272,128]{1,0:T(8,128)(2,1)S(1)} %shard_map.182), channel_id=1, source_target_pairs={{0,4},{2,6},{4,0},{6,2},{1,5},{3,7},{5,1},{7,3},{8,12},{10,14},{12... | collective-permute-start | bytes 208904 | tf_op jit(solution)/shard_map/ppermute | solution.py:641
  10.9 0.0 collective-permute-start.2
  11.0 0.0 copy-start
  11.0 2.1 %own.1 = (bf16[272,128]{1,0:T(8,128)(2,1)S(1)}, f32[8,64]{1,0:T(8,128)S(1)}) custom-call(s32[16]{0:T(128)S(1)} %copy-done.8, f32[8]{0:T(128)S(1)} %copy-done.9, s32[16,16]{1,0:T(8,128)S(1)} %copy-done.6, bf16[8,2048]{1,0:T(8,128)(2,1)S(1)} %bitcast.12, bf16[16,4,128]{2,1,0:T(4,128)(2,1)S(1)} %bitcast.13, bf16[16,4,128]{2,1,0:T(4,128)(2,1)S(1)} %bitcast.14, ...), custom_call_target="tpu_custom_call" | custom-call | flops 4000000000 | bytes 1000000 | tf_op jit(solution)/shard_map/own/pallas_call | solution.py:737
  13.1 0.0 collective-permute-done.refs_1_
  13.1 2.6 %collective-permute-done.1.refs_2_ = bf16[272,128]{1,0:T(8,128)(2,1)S(1)} collective-permute-done((bf16[272,128]{1,0:T(8,128)(2,1)S(1)}, bf16[272,128]{1,0:T(8,128)(2,1)S(1)}, u32[]{:S(2)}, u32[]{:S(2)}) %collective-permute-start.1) | collective-permute-done | bytes 69664 | tf_op jit(solution)/shard_map/ppermute | solution.py:641
  15.8 1.4 %collective-permute-done.2.refs_3_ = bf16[272,128]{1,0:T(8,128)(2,1)S(1)} collective-permute-done((bf16[272,128]{1,0:T(8,128)(2,1)S(1)}, bf16[272,128]{1,0:T(8,128)(2,1)S(1)}, u32[]{:S(2)}, u32[]{:S(2)}) %collective-permute-start.2) | collective-permute-done | bytes 69664 | tf_op jit(solution)/shard_map/ppermute | solution.py:641
  17.1 0.3 %merge.1.refs_0_ = bf16[64,512]{1,0:T(8,128)(2,1)S(1)} custom-call(f32[8,64]{1,0:T(8,128)S(1)} %get-tuple-element.20.terms, bf16[272,128]{1,0:T(8,128)(2,1)S(1)} %get-tuple-element.21.refs_0_, bf16[272,128]{1,0:T(8,128)(2,1)S(1)} %collective-permute-done.refs_1_, bf16[272,128]{1,0:T(8,128)(2,1)S(1)} %collective-permute-done.1.refs_2_, ...), custom_call_target="tpu_custom_call" | custom-call | tf_op jit(solution)/shard_map/merge/pallas_call | solution.py:760
  17.4 2.0 %collective-permute-start.5 = (bf16[64,512]{1,0:T(8,128)(2,1)S(1)}, bf16[64,512]{1,0:T(8,128)(2,1)S(1)}, u32[]{:S(2)}, u32[]{:S(2)}) collective-permute-start(bf16[64,512]{1,0:T(8,128)(2,1)S(1)} %merge.1.refs_0_), channel_id=1, source_target_pairs={{0,6},{2,4},{4,2},{6,0},{1,7},{3,5},{5,3},{7,1},{8,14},{10,12},{12... | collective-permute-start | bytes 196616 | tf_op jit(solution)/shard_map/ppermute | solution.py:641
  19.4 0.3 %collective-permute-start.4 = (bf16[64,512]{1,0:T(8,128)(2,1)S(1)}, bf16[64,512]{1,0:T(8,128)(2,1)S(1)}, u32[]{:S(2)}, u32[]{:S(2)}) collective-permute-start(bf16[64,512]{1,0:T(8,128)(2,1)S(1)} %merge.1.refs_0_), channel_id=1, source_target_pairs={{0,4},{2,6},{4,0},{6,2},{1,5},{3,7},{5,1},{7,3},{8,12},{10,14},{12... | collective-permute-start | bytes 196616 | tf_op jit(solution)/shard_map/ppermute | solution.py:641
  19.7 2.1 %collective-permute-start.3 = (bf16[64,512]{1,0:T(8,128)(2,1)S(1)}, bf16[64,512]{1,0:T(8,128)(2,1)S(1)}, u32[]{:S(2)}, u32[]{:S(2)}) collective-permute-start(bf16[64,512]{1,0:T(8,128)(2,1)S(1)} %merge.1.refs_0_), channel_id=1, source_target_pairs={{0,2},{2,0},{4,6},{6,4},{1,3},{3,1},{5,7},{7,5},{8,10},{10,8},{12,... | collective-permute-start | bytes 196616 | tf_op jit(solution)/shard_map/ppermute | solution.py:641
  21.8 1.7 %collective-permute-done.5.refs_3_ = bf16[64,512]{1,0:T(8,128)(2,1)S(1)} collective-permute-done((bf16[64,512]{1,0:T(8,128)(2,1)S(1)}, bf16[64,512]{1,0:T(8,128)(2,1)S(1)}, u32[]{:S(2)}, u32[]{:S(2)}) %collective-permute-start.5) | collective-permute-done | bytes 65568 | tf_op jit(solution)/shard_map/ppermute | solution.py:641
  23.5 1.6 %collective-permute-done.4.refs_2_ = bf16[64,512]{1,0:T(8,128)(2,1)S(1)} collective-permute-done((bf16[64,512]{1,0:T(8,128)(2,1)S(1)}, bf16[64,512]{1,0:T(8,128)(2,1)S(1)}, u32[]{:S(2)}, u32[]{:S(2)}) %collective-permute-start.4) | collective-permute-done | bytes 65568 | tf_op jit(solution)/shard_map/ppermute | solution.py:641
  25.1 0.0 collective-permute-done.3.refs_1_
  25.1 0.5 %project.1 = (bf16[256,256]{1,0:T(8,128)(2,1)S(1)}, bf16[256,256]{1,0:T(8,128)(2,1)S(1)}) custom-call(bf16[512,512]{1,0:T(8,128)(2,1)S(1)} %copy-done, bf16[64,512]{1,0:T(8,128)(2,1)S(1)} %merge.1.refs_0_, bf16[64,512]{1,0:T(8,128)(2,1)S(1)} %collective-permute-done.3.refs_1_, bf16[64,512]{1,0:T(8,128)(2,1)S(1)} %collective-permute-done.4.refs_2_, ...), custom_call_target="tpu_custom_call" | custom-call | tf_op jit(solution)/shard_map/project/pallas_call | solution.py:772
  25.6 0.1 collective-permute-start.6
  25.7 1.3 %collective-permute-done.6 = bf16[256,256]{1,0:T(8,128)(2,1)S(1)} collective-permute-done((bf16[256,256]{1,0:T(8,128)(2,1)S(1)}, bf16[256,256]{1,0:T(8,128)(2,1)S(1)}, u32[]{:S(2)}, u32[]{:S(2)}) %collective-permute-start.6) | collective-permute-done | bytes 131104 | tf_op jit(solution)/shard_map/ppermute | solution.py:641
  27.0 0.7 %add_convert_fusion = bf16[256,256]{1,0:T(8,128)(2,1)} fusion(bf16[256,256]{1,0:T(8,128)(2,1)S(1)} %collective-permute-done.6, bf16[256,256]{1,0:T(8,128)(2,1)S(1)} %get-tuple-element.23), kind=kLoop, calls=%fused_computation | loop fusion | flops 262144 | bytes 393216 | tf_op jit(solution)/shard_map/convert_element_type | solution.py:781
  (11 shorter events, 0.0 us)
Async XLA Ops:
  4.1 6.8 %copy-start.1 = (bf16[2048,128]{1,0:T(8,128)(2,1)S(1)}, bf16[2048,128]{1,0:T(8,128)(2,1)}, u32[]{:S(2)}) copy-start(bf16[2048,128]{1,0:T(8,128)(2,1)} %key_weight.1) | copy-start | bytes 1572868
  4.2 6.8 %copy-start.2 = (bf16[2048,128]{1,0:T(8,128)(2,1)S(1)}, bf16[2048,128]{1,0:T(8,128)(2,1)}, u32[]{:S(2)}) copy-start(bf16[2048,128]{1,0:T(8,128)(2,1)} %value_weight.1) | copy-start | bytes 1572868
  4.2 6.8 %copy-start.3 = (bf16[2048,8]{0,1:T(8,128)(2,1)S(1)}, bf16[2048,8]{0,1:T(8,128)(2,1)}, u32[]{:S(2)}) copy-start(bf16[2048,8]{0,1:T(8,128)(2,1)} %param.24) | copy-start | bytes 98308
  4.2 6.8 %copy-start.4 = (bf16[16,4,1,128]{3,1,2,0:T(4,128)(2,1)S(1)}, bf16[16,4,1,128]{3,1,2,0:T(4,128)(2,1)}, u32[]{:S(2)}) copy-start(bf16[16,4,1,128]{3,1,2,0:T(4,128)(2,1)} %param.32) | copy-start | bytes 49156
  4.2 6.7 %copy-start.5 = (bf16[16,4,1,128]{3,1,2,0:T(4,128)(2,1)S(1)}, bf16[16,4,1,128]{3,1,2,0:T(4,128)(2,1)}, u32[]{:S(2)}) copy-start(bf16[16,4,1,128]{3,1,2,0:T(4,128)(2,1)} %param.33) | copy-start | bytes 49156
  4.2 6.7 %copy-start.6 = (s32[16,16]{1,0:T(8,128)S(1)}, s32[16,16]{1,0:T(8,128)}, u32[]{:S(2)}) copy-start(s32[16,16]{1,0:T(8,128)} %parents.1) | copy-start | bytes 3076
  4.2 6.7 %copy-start.7 = (f32[16,4,4]{0,2,1:T(4,128)S(1)}, f32[16,4,4]{0,2,1:T(4,128)}, u32[]{:S(2)}) copy-start(f32[16,4,4]{0,2,1:T(4,128)} %param.34) | copy-start | bytes 3076
  4.2 6.7 %copy-start.8 = (s32[16]{0:T(128)S(1)}, s32[16]{0:T(128)}, u32[]{:S(2)}) copy-start(s32[16]{0:T(128)} %accepted.1) | copy-start | bytes 196
  4.2 6.7 %copy-start.9 = (f32[8]{0:T(128)S(1)}, f32[8]{0:T(128)}, u32[]{:S(2)}) copy-start(f32[8]{0:T(128)} %forget_bias.1) | copy-start | bytes 100
  4.2 6.7 %copy-start.10 = (f32[128]{0:T(128)S(1)}, f32[128]{0:T(128)}, u32[]{:S(2)}) copy-start(f32[128]{0:T(128)} %param.27) | copy-start | bytes 1540
  4.7 8.4 %collective-permute-start = (bf16[272,128]{1,0:T(8,128)(2,1)S(1)}, bf16[272,128]{1,0:T(8,128)(2,1)S(1)}, u32[]{:S(2)}, u32[]{:S(2)}) collective-permute-start(bf16[272,128]{1,0:T(8,128)(2,1)S(1)} %shard_map.181), channel_id=1, source_target_pairs={{0,2},{2,0},{4,6},{6,4},{1,3},{3,1},{5,7},{7,5},{8,10},{10,8},{12,... | collective-permute-start | bytes 208904 | tf_op jit(solution)/shard_map/ppermute | solution.py:641
  8.3 7.5 %collective-permute-start.1 = (bf16[272,128]{1,0:T(8,128)(2,1)S(1)}, bf16[272,128]{1,0:T(8,128)(2,1)S(1)}, u32[]{:S(2)}, u32[]{:S(2)}) collective-permute-start(bf16[272,128]{1,0:T(8,128)(2,1)S(1)} %shard_map.182), channel_id=1, source_target_pairs={{0,4},{2,6},{4,0},{6,2},{1,5},{3,7},{5,1},{7,3},{8,12},{10,14},{12... | collective-permute-start | bytes 208904 | tf_op jit(solution)/shard_map/ppermute | solution.py:641
  10.9 6.2 %collective-permute-start.2 = (bf16[272,128]{1,0:T(8,128)(2,1)S(1)}, bf16[272,128]{1,0:T(8,128)(2,1)S(1)}, u32[]{:S(2)}, u32[]{:S(2)}) collective-permute-start(bf16[272,128]{1,0:T(8,128)(2,1)S(1)} %get-tuple-element.22), channel_id=1, source_target_pairs={{0,6},{2,4},{4,2},{6,0},{1,7},{3,5},{5,3},{7,1},{8,14},{10,12},{12... | collective-permute-start | bytes 208904 | tf_op jit(solution)/shard_map/ppermute | solution.py:641
  11.0 14.1 %copy-start = (bf16[512,512]{1,0:T(8,128)(2,1)S(1)}, bf16[512,512]{1,0:T(8,128)(2,1)}, u32[]{:S(2)}) copy-start(bf16[512,512]{1,0:T(8,128)(2,1)} %weight.1) | copy-start | bytes 1572868
  17.4 6.1 %collective-permute-start.5 = (bf16[64,512]{1,0:T(8,128)(2,1)S(1)}, bf16[64,512]{1,0:T(8,128)(2,1)S(1)}, u32[]{:S(2)}, u32[]{:S(2)}) collective-permute-start(bf16[64,512]{1,0:T(8,128)(2,1)S(1)} %merge.1.refs_0_), channel_id=1, source_target_pairs={{0,6},{2,4},{4,2},{6,0},{1,7},{3,5},{5,3},{7,1},{8,14},{10,12},{12... | collective-permute-start | bytes 196616 | tf_op jit(solution)/shard_map/ppermute | solution.py:641
  19.4 5.7 %collective-permute-start.4 = (bf16[64,512]{1,0:T(8,128)(2,1)S(1)}, bf16[64,512]{1,0:T(8,128)(2,1)S(1)}, u32[]{:S(2)}, u32[]{:S(2)}) collective-permute-start(bf16[64,512]{1,0:T(8,128)(2,1)S(1)} %merge.1.refs_0_), channel_id=1, source_target_pairs={{0,4},{2,6},{4,0},{6,2},{1,5},{3,7},{5,1},{7,3},{8,12},{10,14},{12... | collective-permute-start | bytes 196616 | tf_op jit(solution)/shard_map/ppermute | solution.py:641
  19.7 5.4 %collective-permute-start.3 = (bf16[64,512]{1,0:T(8,128)(2,1)S(1)}, bf16[64,512]{1,0:T(8,128)(2,1)S(1)}, u32[]{:S(2)}, u32[]{:S(2)}) collective-permute-start(bf16[64,512]{1,0:T(8,128)(2,1)S(1)} %merge.1.refs_0_), channel_id=1, source_target_pairs={{0,2},{2,0},{4,6},{6,4},{1,3},{3,1},{5,7},{7,5},{8,10},{10,8},{12,... | collective-permute-start | bytes 196616 | tf_op jit(solution)/shard_map/ppermute | solution.py:641
  25.6 1.4 %collective-permute-start.6 = (bf16[256,256]{1,0:T(8,128)(2,1)S(1)}, bf16[256,256]{1,0:T(8,128)(2,1)S(1)}, u32[]{:S(2)}, u32[]{:S(2)}) collective-permute-start(bf16[256,256]{1,0:T(8,128)(2,1)S(1)} %get-tuple-element.24), channel_id=1, source_target_pairs={{0,1},{1,0},{2,3},{3,2},{4,5},{5,4},{6,7},{7,6},{8,9},{9,8},{10,11... | collective-permute-start | bytes 393224 | tf_op jit(solution)/shard_map/ppermute | solution.py:641

commit v4 on v3

--- a/solution.py
+++ b/solution.py
@@ -236,6 +236,8 @@
 MASKED = 2.0**100
 STAT_ROWS = 16
 GRANT = 16 * 2**20
+GO_ORDER = (2, 3, 1)
+BACK_ORDER = (3, 2, 1)
 NT = (((1,), (1,)), ((), ()))
 
 
@@ -315,6 +317,27 @@
     return (vectors * lax.rsqrt(mean + EPSILON) * gain_vec).astype(jnp.bfloat16)
 
 
+def normalized(tokens, first, count, nodes, gain, normed):
+    for start in range(0, count, nodes):
+        widened = tokens[pl.ds(first + start, nodes), :].astype(jnp.float32)
+        mean = jnp.mean(widened * widened, axis=1, keepdims=True)
+        normed[pl.ds(start, nodes), :] = (
+            widened * lax.rsqrt(mean + EPSILON) * gain
+        ).astype(jnp.bfloat16)
+
+
+def queries_of(summed, gain, nodes):
+    head_size = gain.shape[1]
+    heads = summed.shape[1] // head_size
+    normal = [
+        unit(summed[:, head * head_size : (head + 1) * head_size], gain) for head in range(heads)
+    ]
+    return [
+        jnp.concatenate([n[first : first + nodes, :] for n in normal], axis=0)
+        for first in range(0, summed.shape[0], nodes)
+    ]
+
+
 def first_kernel(
     kv_size,
     lengths,
@@ -326,141 +349,129 @@
     cache_values,
     cache_logcum,
     packed,
-    normed,
-    queries,
-    key_buf,
-    value_buf,
+    second_queries,
+    weight_buf,
     decay_buf,
     length_buf,
     token_buf,
     gain_buf,
     query_gain_buf,
-    query_weight_buf,
+    key_buf,
+    value_buf,
     logcum_buf,
-    summed_buf,
+    normed,
     small_sem,
-    token_sem,
     weight_sem,
-    cache_sem,
 ):
     place = lax.axis_index("kv")
     rows, width = tokens.shape
-    query_cols = query_weight.shape[1]
-    head_size = query_gain.shape[1]
-    heads = query_cols // head_size
     seq_count, block_len = cache_keys.shape[0], cache_keys.shape[1]
+    heads = cache_logcum.shape[1]
     nodes = rows // seq_count
     group = seq_count // kv_size
-    row_parts = token_sem.shape[0]
-    row_part = rows // row_parts
+    count = group * nodes
     depth_parts = weight_sem.shape[0]
     depth = width // depth_parts
-
-    def spans(source, target, sem, count, parts):
-        part = count // parts
-        return [
-            pltpu.make_async_copy(
-                source.at[pl.ds(i * part, part)], target.at[pl.ds(i * part, part)], sem(i)
-            )
-            for i in range(parts)
-        ]
-
+    owner = partner_of(place, GO_ORDER[0])
+
+    second = partner_of(place, GO_ORDER[1])
+    cache_span = pl.ds(owner * group, group)
     small = [
         pltpu.make_async_copy(source, target, small_sem.at[i])
         for i, (source, target) in enumerate(
             (
+                (norm_gain, gain_buf),
+                (tokens.at[pl.ds(pl.multiple_of(owner * count, count), count)], token_buf.at[0]),
+                (tokens.at[pl.ds(pl.multiple_of(second * count, count), count)], token_buf.at[1]),
+                (cache_logcum, logcum_buf),
                 (lengths, length_buf),
-                (norm_gain, gain_buf),
                 (query_gain, query_gain_buf),
-                (cache_logcum, logcum_buf),
+                (cache_keys.at[cache_span], key_buf),
+                (cache_values.at[cache_span], value_buf),
             )
         )
     ]
-    token_copies = spans(tokens, token_buf, lambda i: token_sem.at[i], rows, row_parts)
-    weight_copies = spans(query_weight, query_weight_buf, lambda i: weight_sem.at[i], width, depth_parts)
-    cache_copies = []
-    for step in range(kv_size):
-        span = pl.ds(partner_of(place, step) * group, group)
-        cache_copies.append(
-            (
-                pltpu.make_async_copy(cache_keys.at[span], key_buf.at[step], cache_sem.at[step, 0]),
-                pltpu.make_async_copy(cache_values.at[span], value_buf.at[step], cache_sem.at[step, 1]),
-            )
+    weight_copies = [
+        pltpu.make_async_copy(
+            query_weight.at[pl.ds(i * depth, depth)],
+            weight_buf.at[pl.ds(i * depth, depth)],
+            weight_sem.at[i],
         )
-    small[1].start()
-    for copy in token_copies:
+        for i in range(depth_parts)
+    ]
+    for copy in small[:3] + weight_copies + small[3:]:
         copy.start()
-    for copy in weight_copies:
-        copy.start()
-    for i in (0, 2, 3):
-        small[i].start()
-    for step in range(kv_size - 1, -1, -1):
-        for copy in cache_copies[step]:
-            copy.start()
-
-    small[1].wait()
-    gain = gain_buf[...]
-    for part in range(row_parts):
-        token_copies[part].wait()
-        for first in range(part * row_part, (part + 1) * row_part, nodes):
-            widened = token_buf[pl.ds(first, nodes), :].astype(jnp.float32)
-            mean = jnp.mean(widened * widened, axis=1, keepdims=True)
-            normed[pl.ds(first, nodes), :] = (
-                widened * lax.rsqrt(mean + EPSILON) * gain
-            ).astype(jnp.bfloat16)
-
+
+    small[0].wait()
+    for item in range(2):
+        small[1 + item].wait()
+        normalized(token_buf.at[item], 0, count, nodes, gain_buf[...], normed.at[pl.ds(item * count, count)])
+    summed = None
     for part in range(depth_parts):
         weight_copies[part].wait()
         span = pl.ds(part * depth, depth)
-        product = jnp.dot(
-            normed[:, span], query_weight_buf[span, :], preferred_element_type=jnp.float32
-        )
-        if part == 0:
-            summed_buf[...] = product
-        else:
-            summed_buf[...] += product
-    for i in (0, 2, 3):
-        small[i].wait()
-
+        product = jnp.dot(normed[:, span], weight_buf[span, :], preferred_element_type=jnp.float32)
+        summed = product if part == 0 else summed + product
+    for copy in small[3:]:
+        copy.wait()
     column = lax.broadcasted_iota(jnp.int32, (heads, block_len), 1)
     for seq in range(seq_count):
         valid = length_buf[seq] - place * block_len
         decay_buf[seq] = jnp.where(column < valid, logcum_buf[seq] * LOG2E, MASKED)
-
-    for head in range(heads):
-        normal = unit(
-            summed_buf[:, head * head_size : (head + 1) * head_size], query_gain_buf[...]
-        )
-        queries[:, head * nodes : (head + 1) * nodes, :] = normal.reshape(
-            seq_count, nodes, head_size
-        )
-    for step in range(kv_size - 1, -1, -1):
-        for copy in cache_copies[step]:
-            copy.wait()
-    step_partials(kv_size - 1, place, nodes, queries, key_buf, value_buf, decay_buf, packed)
-
-
-def step_partials(step, place, nodes, queries, keys, values, decays, packed, extra=None):
-    group = keys.shape[1]
-    seqs = [partner_of(place, step) * group + item for item in range(group)]
+    queries = queries_of(summed, query_gain_buf[...], nodes)
+    for item in range(group):
+        second_queries[item] = queries[group + item]
     partials(
-        [queries[seq] for seq in seqs],
-        [keys[step, item] for item in range(group)],
-        [values[step, item] for item in range(group)],
+        queries[:group],
+        [key_buf[item] for item in range(group)],
+        [value_buf[item] for item in range(group)],
+        [decay_buf[owner * group + item] for item in range(group)],
+        nodes,
+        packed,
+    )
+
+
+def step_partials(step, nodes, tokens, norm_gain, query_weight, query_gain, keys, values, decays, normed, packed, extra_of=None):
+    place = lax.axis_index("kv")
+    count = normed.shape[0]
+    group = count // nodes
+    owner = partner_of(place, step)
+    normalized(tokens, pl.multiple_of(owner * count, count), count, nodes, norm_gain[...], normed)
+    summed = jnp.dot(normed[...], query_weight[...], preferred_element_type=jnp.float32)
+    queries = queries_of(summed, query_gain[...], nodes)
+    seqs = [owner * group + item for item in range(group)]
+    partials(
+        queries,
+        [keys[seq] for seq in seqs],
+        [values[seq] for seq in seqs],
         [decays[seq] for seq in seqs],
         nodes,
         packed,
-        extra,
-    )
-
-
-def next_kernel(step, queries, keys, values, decays, packed):
-    nodes = queries.shape[1] // decays.shape[1]
-    step_partials(step, lax.axis_index("kv"), nodes, queries, keys, values, decays, packed)
+        None if extra_of is None else extra_of(queries),
+    )
+
+
+def next_kernel(step, nodes, *refs):
+    *operands, packed, normed = refs
+    step_partials(step, nodes, *operands, normed, packed)
+
+
+def second_kernel(step, nodes, queries, keys, values, decays, packed):
+    group = queries.shape[0]
+    seqs = [partner_of(lax.axis_index("kv"), step) * group + item for item in range(group)]
+    partials(
+        [queries[item] for item in range(group)],
+        [keys[seq] for seq in seqs],
+        [values[seq] for seq in seqs],
+        [decays[seq] for seq in seqs],
+        nodes,
+        packed,
+    )
 
 
 def own_kernel(
     tp_size,
+    nodes,
     accepted,
     forget_bias,
     parents,
@@ -471,8 +482,10 @@
     key_weight,
     value_weight,
     key_gain,
-    normed,
-    queries,
+    tokens,
+    norm_gain,
+    query_weight,
+    query_gain,
     keys,
     values,
     decays,
@@ -480,22 +493,75 @@
     terms,
     key_buf,
     value_buf,
+    normed,
+):
+    extra_of = functools.partial(
+        tree_block,
+        tp_size,
+        nodes,
+        accepted,
+        forget_bias,
+        parents,
+        forget_rows,
+        pending_keys,
+        pending_values,
+        pending_logcum,
+        key_weight,
+        value_weight,
+        key_gain,
+        terms,
+        key_buf,
+        value_buf,
+        normed,
+    )
+    step_partials(
+        0,
+        nodes,
+        tokens,
+        norm_gain,
+        query_weight,
+        query_gain,
+        keys,
+        values,
+        decays,
+        normed,
+        packed,
+        extra_of,
+    )
+
+
+def tree_block(
+    tp_size,
+    nodes,
+    accepted,
+    forget_bias,
+    parents,
+    forget_rows,
+    pending_keys,
+    pending_values,
+    pending_logcum,
+    key_weight,
+    value_weight,
+    key_gain,
+    terms,
+    key_buf,
+    value_buf,
+    normed,
+    queries,
 ):
     place = lax.axis_index("kv")
     side = lax.axis_index("tp")
-    group = keys.shape[1]
-    head_rows, head_size = queries.shape[1], queries.shape[2]
+    tree_rows = normed.shape[0]
+    group = tree_rows // nodes
     most_taken, heads, seq_count = pending_logcum.shape
-    nodes = head_rows // heads
-    tree_rows = group * nodes
+    head_rows, head_size = heads * nodes, key_gain.shape[1]
     size = 2 * tree_rows
     exact = dict(preferred_element_type=jnp.float32, precision=HIGHEST)
-    own_rows = pl.ds(pl.multiple_of(place * tree_rows, tree_rows), tree_rows)
 
     key_buf[...] = jnp.zeros_like(key_buf)
     value_buf[...] = jnp.zeros_like(value_buf)
     summed = jnp.dot(
-        normed[own_rows, :],
+        normed[...],
         jnp.concatenate([key_weight[...], value_weight[...]], axis=1),
         preferred_element_type=jnp.float32,
     )
@@ -506,7 +572,7 @@
         key_buf[rows, :] = pending_keys[place * group + item].astype(jnp.float32)
         value_buf[rows, :] = pending_values[place * group + item].astype(jnp.float32)
     gates = lax.dot_general(
-        forget_rows[...], normed[own_rows, :], NT, preferred_element_type=jnp.float32
+        forget_rows[...], normed[...], NT, preferred_element_type=jnp.float32
     )
 
     lane = lax.broadcasted_iota(jnp.int32, (1, size), 1)
@@ -567,7 +633,7 @@
     tree_scores, own_terms = [], []
     for item in range(group):
         raw = lax.dot_general(
-            queries[place * group + item], tree_keys, NT, preferred_element_type=jnp.float32
+            queries[item], tree_keys, NT, preferred_element_type=jnp.float32
         )
         own_terms.append(
             jnp.sum(
@@ -581,8 +647,7 @@
         seen = reached * in_tree.astype(jnp.float32) + offered.astype(jnp.float32) > 0.5
         tree_scores.append(jnp.where(seen, raw * scale - head_decay, -MASKED))
     terms[...] = stacked(own_terms, head_rows, head_size)[: terms.shape[0], :]
-    extra = (tree_scores, value_buf[...].astype(jnp.bfloat16))
-    step_partials(0, place, nodes, queries, keys, values, decays, packed, extra)
+    return tree_scores, value_buf[...].astype(jnp.bfloat16)
 
 
 def merge_kernel(kv_size, terms, *refs):
@@ -676,72 +741,88 @@
     hbm = pl.BlockSpec(memory_space=pltpu.HBM)
     vmem = pl.BlockSpec(memory_space=pltpu.VMEM)
     smem = pl.BlockSpec(memory_space=pltpu.SMEM)
-    row_parts, depth_parts = 4, 4
+    depth_parts = 4
+    count = group * nodes
     packed_shape = in_vmem((group * head_rows + STAT_ROWS, head_size), bf16)
-
-    farthest, normed, queries, keys, values, decays = pl.pallas_call(
+    token_matrix = tokens.reshape(rows, width)
+    norm_row = norm_gain.reshape(1, width)
+    query_row = query_gain.reshape(1, head_size)
+    key_array = cache_keys.reshape(seq_count, block_len, head_size)
+    value_array = cache_values.reshape(seq_count, block_len, head_size)
+
+    farthest, second_queries, query_matrix, decays = pl.pallas_call(
         functools.partial(first_kernel, kv_size),
         compiler_params=pltpu.CompilerParams(vmem_limit_bytes=GRANT),
         name="first",
         out_shape=[
             packed_shape,
-            in_vmem((rows, width), bf16),
-            in_vmem((seq_count, head_rows, head_size), bf16),
-            in_vmem((kv_size, group, block_len, head_size), bf16),
-            in_vmem((kv_size, group, block_len, head_size), bf16),
+            in_vmem((group, head_rows, head_size), bf16),
+            in_vmem((width, query_cols), bf16),
             in_vmem((seq_count, heads, block_len), f32),
         ],
         in_specs=[hbm] * 8,
-        out_specs=[vmem] * 6,
+        out_specs=[vmem] * 4,
         scratch_shapes=[
             pltpu.SMEM((seq_count,), jnp.int32),
-            pltpu.VMEM((rows, width), bf16),
+            pltpu.VMEM((2, count, width), bf16),
             pltpu.VMEM((1, width), f32),
             pltpu.VMEM((1, head_size), f32),
-            pltpu.VMEM((width, query_cols), bf16),
+            pltpu.VMEM((group, block_len, head_size), bf16),
+            pltpu.VMEM((group, block_len, head_size), bf16),
             pltpu.VMEM((seq_count, heads, block_len), f32),
-            pltpu.VMEM((rows, query_cols), f32),
-            pltpu.SemaphoreType.DMA((4,)),
-            pltpu.SemaphoreType.DMA((row_parts,)),
+            pltpu.VMEM((2 * count, width), bf16),
+            pltpu.SemaphoreType.DMA((8,)),
             pltpu.SemaphoreType.DMA((depth_parts,)),
-            pltpu.SemaphoreType.DMA((kv_size, 2)),
         ],
     )(
         *[
             pltpu.with_memory_space_constraint(a, pltpu.HBM)
             for a in (
                 lengths,
-                tokens.reshape(rows, width),
-                norm_gain.reshape(1, width),
+                token_matrix,
+                norm_row,
                 query_weight,
-                query_gain.reshape(1, head_size),
-                cache_keys.reshape(seq_count, block_len, head_size),
-                cache_values.reshape(seq_count, block_len, head_size),
+                query_row,
+                key_array,
+                value_array,
                 jnp.swapaxes(cache_logcum, 1, 2),
             )
         ]
     )
-    shared = [held(a) for a in (queries, keys, values, decays)]
-    packed = {kv_size - 1: farthest}
-    for step in range(kv_size - 2, 0, -1):
+    shared = [
+        held(a)
+        for a in (token_matrix, norm_row, query_matrix, query_row, key_array, value_array, decays)
+    ]
+    packed = {GO_ORDER[0]: farthest}
+    packed[GO_ORDER[1]] = pl.pallas_call(
+        functools.partial(second_kernel, GO_ORDER[1], nodes),
+        compiler_params=pltpu.CompilerParams(vmem_limit_bytes=GRANT),
+        name="second",
+        out_shape=packed_shape,
+        in_specs=[vmem] * 4,
+        out_specs=vmem,
+    )(held(second_queries), *shared[4:])
+    for step in GO_ORDER[2:]:
         packed[step] = pl.pallas_call(
-            functools.partial(next_kernel, step),
+            functools.partial(next_kernel, step, nodes),
             compiler_params=pltpu.CompilerParams(vmem_limit_bytes=GRANT),
-        out_shape=packed_shape,
-            in_specs=[vmem] * 4,
+            out_shape=packed_shape,
+            in_specs=[vmem] * 7,
             out_specs=vmem,
+            scratch_shapes=[pltpu.VMEM((count, width), bf16)],
         )(*shared)
     moved = {}
-    for step in range(kv_size - 1, 0, -1):
+    for step in GO_ORDER:
         moved[step] = exchange(packed[step], "kv", kv_size, step)
     own, terms = pl.pallas_call(
-        functools.partial(own_kernel, tp_size),
+        functools.partial(own_kernel, tp_size, nodes),
         compiler_params=pltpu.CompilerParams(vmem_limit_bytes=GRANT),
         name="own",
         out_shape=[packed_shape, in_vmem((8, head_rows), f32)],
-        in_specs=[smem, smem] + [vmem] * 13,
+        in_specs=[smem, smem] + [vmem] * 15,
         out_specs=[vmem, vmem],
-        scratch_shapes=[pltpu.VMEM((2 * group * nodes, head_size), f32)] * 2,
+        scratch_shapes=[pltpu.VMEM((2 * count, head_size), f32)] * 2
+        + [pltpu.VMEM((count, width), bf16)],
         cost_estimate=pl.CostEstimate(flops=4_000_000_000, bytes_accessed=1_000_000, transcendentals=0),
     )(
         accepted,
@@ -754,7 +835,6 @@
         held(key_weight),
         held(value_weight),
         key_gain.reshape(1, head_size),
-        held(normed),
         *shared,
     )
     chunk = pl.pallas_call(
@@ -766,7 +846,7 @@
         out_specs=vmem,
     )(held(terms), held(own), *[held(moved[s]) for s in range(1, kv_size)])
     chunks = {0: chunk}
-    for step in range(kv_size - 1, 0, -1):
+    for step in BACK_ORDER:
         chunks[step] = exchange(chunk, "kv", kv_size, step)
     cols = output_weight.shape[1] // tp_size
     kept, sent = pl.pallas_call(
@@ -786,7 +866,7 @@
     kv_size = mesh.shape["kv"]
     seq_count = shapes["tokens"][0] // mesh.shape["dp"]
     one_key_head = shapes["cache_keys"][2] == mesh.shape["tp"]
-    small = kv_size <= 4 and kv_size & (kv_size - 1) == 0
+    small = kv_size == 4
     return small and one_key_head and mesh.shape["tp"] == 2 and seq_count % kv_size == 0
 
 

time: 27.9 us -> 29.1 us (1.043)
  waiting for transfers between devices: 8.6 us -> 9.92 us
    ppermute x7, waiting for transfers between devices: 8.6 us -> 9.92 us  [exchange(): return lax.ppermute(array, axis, [(i, i ^ step) for i in range(size)])]
    pallas_call x1, Pallas kernels: 4.13 us -> 2.84 us  [fast_shards(): pl.pallas_call(functools.partial(first_kernel, kv_size), compiler_params=...]
    pallas_call x3, Pallas kernels: 3.01 us -> 4.08 us  [the longest x1 2.55 us: fast_shards(): pl.pallas_call(functools.partial(own_kernel, tp_size, nodes), compiler_pa...]
  transfers between devices with their start and end apart: 7 -> 7, of which waited for: 5 -> 6; matrix products, arithmetic and copies ran while one was open for 0% -> 0% of each run, Pallas kernels for 9% -> 10%
where the time goes in v4:
time: 29.1 us; the launch traced here: 28.9 us
  starting transfers between devices  10.3 us (35%)
  waiting for transfers between devices  9.92 us (34%)
  Pallas kernels  7.71 us (26%)
  other arithmetic  0.69 us (2%)
    ppermute x7, starting transfers between devices, exchange(): return lax.ppermute(array, axis, [(i, i ^ step) for i in range(size)])  10.3 us
    ppermute x7, waiting for transfers between devices, exchange(): return lax.ppermute(array, axis, [(i, i ^ step) for i in range(size)])  9.92 us
    pallas_call x1, Pallas kernels, fast_shards(): pl.pallas_call(functools.partial(first_kernel, kv_size), compiler_params=...  2.84 us
    pallas_call x1, Pallas kernels, fast_shards(): pl.pallas_call(functools.partial(own_kernel, tp_size, nodes), compiler_pa...  2.55 us
    pallas_call x1, Pallas kernels, fast_shards(): pl.pallas_call(functools.partial(next_kernel, step, nodes), compiler_para...  1.08 us
    convert_element_type x1, other arithmetic, fast_shards(): summed = (kept.astype(f32) + received.astype(f32)).astype(bf16)  0.69 us
  transfers between devices with their start and end apart: 7, of which 6 were waited for; matrix products, arithmetic and copies ran while one was open for 0% of the time, Pallas kernels for 10%

profile of v4, /device:TPU:0, one launch (start us, length us, event | category | flops | bytes accessed | tf_op | source)
XLA Modules:
  0.0 28.9 jit_solution(6455467440714082487)
XLA Ops:
  0.0 2.8 %first.1 = (bf16[272,128]{1,0:T(8,128)(2,1)S(1)}, bf16[4,64,128]{2,1,0:T(8,128)(2,1)S(1)}, bf16[2048,512]{1,0:T(8,128)(2,1)S(1)}, f32[16,4,256]{2,1,0:T(4,128)S(1)}) custom-call(s32[16]{0:T(128)} %lengths.1, bf16[256,2048]{1,0:T(8,128)(2,1)} %bitcast.20, f32[1,2048]{1,0:T(1,128)} %bitcast.23, bf16[2048,512]{1,0:T(8,128)(2,1)} %query_weight.1, ...), custom_call_target="tpu_custom_call" | custom-call | tf_op jit(solution)/shard_map/first/pallas_call | solution.py:753
  2.9 0.0 copy-done
  2.9 0.0 copy-done.1
  2.9 1.1 %shard_map.181 = bf16[272,128]{1,0:T(8,128)(2,1)S(1)} custom-call(bf16[256,2048]{1,0:T(8,128)(2,1)S(1)} %bitcast.21, f32[1,2048]{1,0:T(1,128)S(1)} %bitcast.24, bf16[2048,512]{1,0:T(8,128)(2,1)S(1)} %get-tuple-element.13.query_weight.refs_2_, f32[1,128]{1,0:T(1,128)S(1)} %bitcast.27, bf16[16,256,128]{2,1,0:T(8,128)(2,1)S(1)} %bitcast.13, ...), custom_call_target="tpu_custom_call" | custom-call | tf_op jit(solution)/shard_map/pallas_call | solution.py:806
  4.0 0.0 copy-start.8
  4.0 0.0 copy-start.9
  4.0 0.0 copy-start.10
  4.0 0.0 copy-start.11
  4.1 0.0 copy-start.12
  4.1 0.0 copy-start.13
  4.1 0.0 copy-start.14
  4.1 0.0 copy-start.15
  4.1 3.1 %collective-permute-start = (bf16[272,128]{1,0:T(8,128)(2,1)S(1)}, bf16[272,128]{1,0:T(8,128)(2,1)S(1)}, u32[]{:S(2)}, u32[]{:S(2)}) collective-permute-start(bf16[272,128]{1,0:T(8,128)(2,1)S(1)} %shard_map.181), channel_id=1, source_target_pairs={{0,2},{2,0},{4,6},{6,4},{1,3},{3,1},{5,7},{7,5},{8,10},{10,8},{12,... | collective-permute-start | bytes 208904 | tf_op jit(solution)/shard_map/ppermute | solution.py:706
  7.2 0.5 %second.1 = bf16[272,128]{1,0:T(8,128)(2,1)S(1)} custom-call(bf16[4,64,128]{2,1,0:T(8,128)(2,1)S(1)} %get-tuple-element.18.queries, bf16[16,256,128]{2,1,0:T(8,128)(2,1)S(1)} %bitcast.14, bf16[16,256,128]{2,1,0:T(8,128)(2,1)S(1)} %bitcast.18, f32[16,4,256]{2,1,0:T(4,128)S(1)} %get-tuple-element.14.decays.refs_6_), custom_call_target="tpu_custom_call" | custom-call | tf_op jit(solution)/shard_map/second/pallas_call | solution.py:797
  7.7 2.5 %collective-permute-start.2 = (bf16[272,128]{1,0:T(8,128)(2,1)S(1)}, bf16[272,128]{1,0:T(8,128)(2,1)S(1)}, u32[]{:S(2)}, u32[]{:S(2)}) collective-permute-start(bf16[272,128]{1,0:T(8,128)(2,1)S(1)} %second.1), channel_id=1, source_target_pairs={{0,6},{2,4},{4,2},{6,0},{1,7},{3,5},{5,3},{7,1},{8,14},{10,12},{12... | collective-permute-start | bytes 208904 | tf_op jit(solution)/shard_map/ppermute | solution.py:706
  10.2 0.2 collective-permute-start.1
  10.5 0.0 copy-start.3
  10.5 2.6 %own.1 = (bf16[272,128]{1,0:T(8,128)(2,1)S(1)}, f32[8,64]{1,0:T(8,128)S(1)}) custom-call(s32[16]{0:T(128)S(1)} %copy-done.13, f32[8]{0:T(128)S(1)} %copy-done.14, s32[16,16]{1,0:T(8,128)S(1)} %copy-done.11, bf16[8,2048]{1,0:T(8,128)(2,1)S(1)} %bitcast.29, bf16[16,4,128]{2,1,0:T(4,128)(2,1)S(1)} %bitcast.30, bf16[16,4,128]{2,1,0:T(4,128)(2,1)S(1)} %bitcast.31, ...), custom_call_target="tpu_custom_call" | custom-call | flops 4000000000 | bytes 1000000 | tf_op jit(solution)/shard_map/own/pallas_call | solution.py:817
  13.0 0.0 collective-permute-done.refs_1_
  13.0 1.6 %collective-permute-done.2.refs_3_ = bf16[272,128]{1,0:T(8,128)(2,1)S(1)} collective-permute-done((bf16[272,128]{1,0:T(8,128)(2,1)S(1)}, bf16[272,128]{1,0:T(8,128)(2,1)S(1)}, u32[]{:S(2)}, u32[]{:S(2)}) %collective-permute-start.2) | collective-permute-done | bytes 69664 | tf_op jit(solution)/shard_map/ppermute | solution.py:706
  14.6 2.4 %collective-permute-done.1.refs_2_ = bf16[272,128]{1,0:T(8,128)(2,1)S(1)} collective-permute-done((bf16[272,128]{1,0:T(8,128)(2,1)S(1)}, bf16[272,128]{1,0:T(8,128)(2,1)S(1)}, u32[]{:S(2)}, u32[]{:S(2)}) %collective-permute-start.1) | collective-permute-done | bytes 69664 | tf_op jit(solution)/shard_map/ppermute | solution.py:706
  17.0 0.3 %merge.1.refs_0_ = bf16[64,512]{1,0:T(8,128)(2,1)S(1)} custom-call(f32[8,64]{1,0:T(8,128)S(1)} %get-tuple-element.15.terms, bf16[272,128]{1,0:T(8,128)(2,1)S(1)} %get-tuple-element.16.refs_0_, bf16[272,128]{1,0:T(8,128)(2,1)S(1)} %collective-permute-done.refs_1_, bf16[272,128]{1,0:T(8,128)(2,1)S(1)} %collective-permute-done.1.refs_2_, ...), custom_call_target="tpu_custom_call" | custom-call | tf_op jit(solution)/shard_map/merge/pallas_call | solution.py:840
  17.3 0.0 collective-permute-start.3
  17.3 2.9 %collective-permute-start.4 = (bf16[64,512]{1,0:T(8,128)(2,1)S(1)}, bf16[64,512]{1,0:T(8,128)(2,1)S(1)}, u32[]{:S(2)}, u32[]{:S(2)}) collective-permute-start(bf16[64,512]{1,0:T(8,128)(2,1)S(1)} %merge.1.refs_0_), channel_id=1, source_target_pairs={{0,4},{2,6},{4,0},{6,2},{1,5},{3,7},{5,1},{7,3},{8,12},{10,14},{12... | collective-permute-start | bytes 196616 | tf_op jit(solution)/shard_map/ppermute | solution.py:706
  20.3 1.4 %collective-permute-start.5 = (bf16[64,512]{1,0:T(8,128)(2,1)S(1)}, bf16[64,512]{1,0:T(8,128)(2,1)S(1)}, u32[]{:S(2)}, u32[]{:S(2)}) collective-permute-start(bf16[64,512]{1,0:T(8,128)(2,1)S(1)} %merge.1.refs_0_), channel_id=1, source_target_pairs={{0,6},{2,4},{4,2},{6,0},{1,7},{3,5},{5,3},{7,1},{8,14},{10,12},{12... | collective-permute-start | bytes 196616 | tf_op jit(solution)/shard_map/ppermute | solution.py:706
  21.7 0.5 %collective-permute-done.3.refs_1_ = bf16[64,512]{1,0:T(8,128)(2,1)S(1)} collective-permute-done((bf16[64,512]{1,0:T(8,128)(2,1)S(1)}, bf16[64,512]{1,0:T(8,128)(2,1)S(1)}, u32[]{:S(2)}, u32[]{:S(2)}) %collective-permute-start.3) | collective-permute-done | bytes 65568 | tf_op jit(solution)/shard_map/ppermute | solution.py:706
  22.2 2.7 %collective-permute-done.4.refs_2_ = bf16[64,512]{1,0:T(8,128)(2,1)S(1)} collective-permute-done((bf16[64,512]{1,0:T(8,128)(2,1)S(1)}, bf16[64,512]{1,0:T(8,128)(2,1)S(1)}, u32[]{:S(2)}, u32[]{:S(2)}) %collective-permute-start.4) | collective-permute-done | bytes 65568 | tf_op jit(solution)/shard_map/ppermute | solution.py:706
  24.9 1.4 %collective-permute-done.5.refs_3_ = bf16[64,512]{1,0:T(8,128)(2,1)S(1)} collective-permute-done((bf16[64,512]{1,0:T(8,128)(2,1)S(1)}, bf16[64,512]{1,0:T(8,128)(2,1)S(1)}, u32[]{:S(2)}, u32[]{:S(2)}) %collective-permute-start.5) | collective-permute-done | bytes 65568 | tf_op jit(solution)/shard_map/ppermute | solution.py:706
  26.3 0.5 %project.1 = (bf16[256,256]{1,0:T(8,128)(2,1)S(1)}, bf16[256,256]{1,0:T(8,128)(2,1)S(1)}) custom-call(bf16[512,512]{1,0:T(8,128)(2,1)S(1)} %copy-done.3, bf16[64,512]{1,0:T(8,128)(2,1)S(1)} %merge.1.refs_0_, bf16[64,512]{1,0:T(8,128)(2,1)S(1)} %collective-permute-done.3.refs_1_, bf16[64,512]{1,0:T(8,128)(2,1)S(1)} %collective-permute-done.4.refs_2_, ...), custom_call_target="tpu_custom_call" | custom-call | tf_op jit(solution)/shard_map/project/pallas_call | solution.py:852
  26.8 0.1 collective-permute-start.6
  26.9 1.3 %collective-permute-done.6 = bf16[256,256]{1,0:T(8,128)(2,1)S(1)} collective-permute-done((bf16[256,256]{1,0:T(8,128)(2,1)S(1)}, bf16[256,256]{1,0:T(8,128)(2,1)S(1)}, u32[]{:S(2)}, u32[]{:S(2)}) %collective-permute-start.6) | collective-permute-done | bytes 131104 | tf_op jit(solution)/shard_map/ppermute | solution.py:706
  28.2 0.7 %add_convert_fusion = bf16[256,256]{1,0:T(8,128)(2,1)} fusion(bf16[256,256]{1,0:T(8,128)(2,1)S(1)} %collective-permute-done.6, bf16[256,256]{1,0:T(8,128)(2,1)S(1)} %get-tuple-element.19), kind=kLoop, calls=%fused_computation | loop fusion | flops 262144 | bytes 393216 | tf_op jit(solution)/shard_map/convert_element_type | solution.py:861
  (21 shorter events, 0.0 us)
Async XLA Ops:
  0.0 2.9 %copy-start = (bf16[16,256,1,128]{3,1,2,0:T(8,128)(2,1)S(1)}, bf16[16,256,1,128]{3,1,2,0:T(8,128)(2,1)}, u32[]{:S(2)}) copy-start(bf16[16,256,1,128]{3,1,2,0:T(8,128)(2,1)} %param.29) | copy-start | bytes 3145732
  0.0 2.9 %copy-start.1 = (bf16[16,256,1,128]{3,1,2,0:T(8,128)(2,1)S(1)}, bf16[16,256,1,128]{3,1,2,0:T(8,128)(2,1)}, u32[]{:S(2)}) copy-start(bf16[16,256,1,128]{3,1,2,0:T(8,128)(2,1)} %param.30) | copy-start | bytes 3145732
  0.0 2.9 %copy-start.2 = (bf16[16,16,2048]{2,1,0:T(8,128)(2,1)S(1)}, bf16[16,16,2048]{2,1,0:T(8,128)(2,1)}, u32[]{:S(2)}) copy-start(bf16[16,16,2048]{2,1,0:T(8,128)(2,1)} %param.19) | copy-start | bytes 3145732
  0.0 2.9 %copy-start.4 = (f32[2048]{0:T(1024)S(1)}, f32[2048]{0:T(1024)}, u32[]{:S(2)}) copy-start(f32[2048]{0:T(1024)} %param.20) | copy-start | bytes 24580
  0.0 2.9 %copy-start.5 = (f32[128]{0:T(128)S(1)}, f32[128]{0:T(128)}, u32[]{:S(2)}) copy-start(f32[128]{0:T(128)} %param.26) | copy-start | bytes 1540
  4.0 6.4 %copy-start.6 = (bf16[2048,128]{1,0:T(8,128)(2,1)S(1)}, bf16[2048,128]{1,0:T(8,128)(2,1)}, u32[]{:S(2)}) copy-start(bf16[2048,128]{1,0:T(8,128)(2,1)} %key_weight.1) | copy-start | bytes 1572868
  4.0 6.4 %copy-start.7 = (bf16[2048,128]{1,0:T(8,128)(2,1)S(1)}, bf16[2048,128]{1,0:T(8,128)(2,1)}, u32[]{:S(2)}) copy-start(bf16[2048,128]{1,0:T(8,128)(2,1)} %value_weight.1) | copy-start | bytes 1572868
  4.0 6.4 %copy-start.8 = (bf16[2048,8]{0,1:T(8,128)(2,1)S(1)}, bf16[2048,8]{0,1:T(8,128)(2,1)}, u32[]{:S(2)}) copy-start(bf16[2048,8]{0,1:T(8,128)(2,1)} %param.24) | copy-start | bytes 98308
  4.0 6.4 %copy-start.9 = (bf16[16,4,1,128]{3,1,2,0:T(4,128)(2,1)S(1)}, bf16[16,4,1,128]{3,1,2,0:T(4,128)(2,1)}, u32[]{:S(2)}) copy-start(bf16[16,4,1,128]{3,1,2,0:T(4,128)(2,1)} %param.32) | copy-start | bytes 49156
  4.0 6.4 %copy-start.10 = (bf16[16,4,1,128]{3,1,2,0:T(4,128)(2,1)S(1)}, bf16[16,4,1,128]{3,1,2,0:T(4,128)(2,1)}, u32[]{:S(2)}) copy-start(bf16[16,4,1,128]{3,1,2,0:T(4,128)(2,1)} %param.33) | copy-start | bytes 49156
  4.0 6.4 %copy-start.11 = (s32[16,16]{1,0:T(8,128)S(1)}, s32[16,16]{1,0:T(8,128)}, u32[]{:S(2)}) copy-start(s32[16,16]{1,0:T(8,128)} %parents.1) | copy-start | bytes 3076
  4.1 6.4 %copy-start.12 = (f32[16,4,4]{0,2,1:T(4,128)S(1)}, f32[16,4,4]{0,2,1:T(4,128)}, u32[]{:S(2)}) copy-start(f32[16,4,4]{0,2,1:T(4,128)} %param.34) | copy-start | bytes 3076
  4.1 6.4 %copy-start.13 = (s32[16]{0:T(128)S(1)}, s32[16]{0:T(128)}, u32[]{:S(2)}) copy-start(s32[16]{0:T(128)} %accepted.1) | copy-start | bytes 196
  4.1 6.4 %copy-start.14 = (f32[8]{0:T(128)S(1)}, f32[8]{0:T(128)}, u32[]{:S(2)}) copy-start(f32[8]{0:T(128)} %forget_bias.1) | copy-start | bytes 100
  4.1 6.4 %copy-start.15 = (f32[128]{0:T(128)S(1)}, f32[128]{0:T(128)}, u32[]{:S(2)}) copy-start(f32[128]{0:T(128)} %param.27) | copy-start | bytes 1540
  4.1 8.9 %collective-permute-start = (bf16[272,128]{1,0:T(8,128)(2,1)S(1)}, bf16[272,128]{1,0:T(8,128)(2,1)S(1)}, u32[]{:S(2)}, u32[]{:S(2)}) collective-permute-start(bf16[272,128]{1,0:T(8,128)(2,1)S(1)} %shard_map.181), channel_id=1, source_target_pairs={{0,2},{2,0},{4,6},{6,4},{1,3},{3,1},{5,7},{7,5},{8,10},{10,8},{12,... | collective-permute-start | bytes 208904 | tf_op jit(solution)/shard_map/ppermute | solution.py:706
  7.7 6.9 %collective-permute-start.2 = (bf16[272,128]{1,0:T(8,128)(2,1)S(1)}, bf16[272,128]{1,0:T(8,128)(2,1)S(1)}, u32[]{:S(2)}, u32[]{:S(2)}) collective-permute-start(bf16[272,128]{1,0:T(8,128)(2,1)S(1)} %second.1), channel_id=1, source_target_pairs={{0,6},{2,4},{4,2},{6,0},{1,7},{3,5},{5,3},{7,1},{8,14},{10,12},{12... | collective-permute-start | bytes 208904 | tf_op jit(solution)/shard_map/ppermute | solution.py:706
  10.2 6.8 %collective-permute-start.1 = (bf16[272,128]{1,0:T(8,128)(2,1)S(1)}, bf16[272,128]{1,0:T(8,128)(2,1)S(1)}, u32[]{:S(2)}, u32[]{:S(2)}) collective-permute-start(bf16[272,128]{1,0:T(8,128)(2,1)S(1)} %get-tuple-element.17), channel_id=1, source_target_pairs={{0,4},{2,6},{4,0},{6,2},{1,5},{3,7},{5,1},{7,3},{8,12},{10,14},{12... | collective-permute-start | bytes 208904 | tf_op jit(solution)/shard_map/ppermute | solution.py:706
  10.5 15.9 %copy-start.3 = (bf16[512,512]{1,0:T(8,128)(2,1)S(1)}, bf16[512,512]{1,0:T(8,128)(2,1)}, u32[]{:S(2)}) copy-start(bf16[512,512]{1,0:T(8,128)(2,1)} %weight.1) | copy-start | bytes 1572868
  17.3 4.9 %collective-permute-start.3 = (bf16[64,512]{1,0:T(8,128)(2,1)S(1)}, bf16[64,512]{1,0:T(8,128)(2,1)S(1)}, u32[]{:S(2)}, u32[]{:S(2)}) collective-permute-start(bf16[64,512]{1,0:T(8,128)(2,1)S(1)} %merge.1.refs_0_), channel_id=1, source_target_pairs={{0,2},{2,0},{4,6},{6,4},{1,3},{3,1},{5,7},{7,5},{8,10},{10,8},{12,... | collective-permute-start | bytes 196616 | tf_op jit(solution)/shard_map/ppermute | solution.py:706
  17.3 7.6 %collective-permute-start.4 = (bf16[64,512]{1,0:T(8,128)(2,1)S(1)}, bf16[64,512]{1,0:T(8,128)(2,1)S(1)}, u32[]{:S(2)}, u32[]{:S(2)}) collective-permute-start(bf16[64,512]{1,0:T(8,128)(2,1)S(1)} %merge.1.refs_0_), channel_id=1, source_target_pairs={{0,4},{2,6},{4,0},{6,2},{1,5},{3,7},{5,1},{7,3},{8,12},{10,14},{12... | collective-permute-start | bytes 196616 | tf_op jit(solution)/shard_map/ppermute | solution.py:706
  20.3 6.1 %collective-permute-start.5 = (bf16[64,512]{1,0:T(8,128)(2,1)S(1)}, bf16[64,512]{1,0:T(8,128)(2,1)S(1)}, u32[]{:S(2)}, u32[]{:S(2)}) collective-permute-start(bf16[64,512]{1,0:T(8,128)(2,1)S(1)} %merge.1.refs_0_), channel_id=1, source_target_pairs={{0,6},{2,4},{4,2},{6,0},{1,7},{3,5},{5,3},{7,1},{8,14},{10,12},{12... | collective-permute-start | bytes 196616 | tf_op jit(solution)/shard_map/ppermute | solution.py:706
  26.8 1.4 %collective-permute-start.6 = (bf16[256,256]{1,0:T(8,128)(2,1)S(1)}, bf16[256,256]{1,0:T(8,128)(2,1)S(1)}, u32[]{:S(2)}, u32[]{:S(2)}) collective-permute-start(bf16[256,256]{1,0:T(8,128)(2,1)S(1)} %get-tuple-element.20), channel_id=1, source_target_pairs={{0,1},{1,0},{2,3},{3,2},{4,5},{5,4},{6,7},{7,6},{8,9},{9,8},{10,11... | collective-permute-start | bytes 393224 | tf_op jit(solution)/shard_map/ppermute | solution.py:706

commit v5 on v4

--- a/solution.py
+++ b/solution.py
@@ -238,6 +238,7 @@
 GRANT = 16 * 2**20
 GO_ORDER = (2, 3, 1)
 BACK_ORDER = (3, 2, 1)
+EARLY, LATE = (0, 1, 3), (2,)
 NT = (((1,), (1,)), ((), ()))
 
 
@@ -687,19 +688,34 @@
             )
 
 
-def project_kernel(kv_size, weight, *refs):
-    chunks, (kept, sent) = refs[:kv_size], refs[kv_size:]
+def project_kernel(other, weight, *refs):
+    *chunks, out = refs
+    side = lax.axis_index("tp")
+    half = 1 - side if other else side
+    rows, cols = chunks[0].shape[0], out.shape[1]
+    part = weight[:, pl.ds(pl.multiple_of(half * cols, cols), cols)]
+    for i, chunk in enumerate(chunks):
+        out[i * rows : (i + 1) * rows, :] = jnp.dot(
+            chunk[...], part, preferred_element_type=jnp.float32
+        ).astype(jnp.bfloat16)
+
+
+def add_kernel(kept, early, late, out, buf, sem):
     place = lax.axis_index("kv")
-    side = lax.axis_index("tp")
-    rows = chunks[0].shape[0]
-    cols = kept.shape[1]
-    for out, half in ((sent, 1 - side), (kept, side)):
-        part = weight[:, pl.ds(pl.multiple_of(half * cols, cols), cols)]
-        for step in range(kv_size):
-            first = pl.multiple_of(partner_of(place, step) * rows, rows)
-            out[pl.ds(first, rows), :] = jnp.dot(
-                chunks[step][...], part, preferred_element_type=jnp.float32
-            ).astype(jnp.bfloat16)
+    rows = late.shape[0] // len(LATE)
+    copies = []
+    for i, step in enumerate(EARLY + LATE):
+        span = slice(i * rows, (i + 1) * rows)
+        first = (i - len(EARLY)) * rows
+        received = late[first : first + rows, :] if i >= len(EARLY) else early[span, :]
+        buf[span, :] = (kept[span, :].astype(jnp.float32) + received.astype(jnp.float32)).astype(
+            jnp.bfloat16
+        )
+        target = pl.ds(pl.multiple_of(partner_of(place, step) * rows, rows), rows)
+        copies.append(pltpu.make_async_copy(buf.at[pl.ds(i * rows, rows)], out.at[target], sem.at[i]))
+        copies[-1].start()
+    for copy in copies:
+        copy.wait()
 
 
 def exchange(array, axis, size, step):
@@ -849,16 +865,33 @@
     for step in BACK_ORDER:
         chunks[step] = exchange(chunk, "kv", kv_size, step)
     cols = output_weight.shape[1] // tp_size
-    kept, sent = pl.pallas_call(
-        functools.partial(project_kernel, kv_size),
+    weight = held(output_weight)
+
+    def project(steps, other):
+        return pl.pallas_call(
+            functools.partial(project_kernel, other),
+            compiler_params=pltpu.CompilerParams(vmem_limit_bytes=GRANT),
+            name="project",
+            out_shape=in_vmem((len(steps) * count, cols), bf16),
+            in_specs=[vmem] * (len(steps) + 1),
+            out_specs=vmem,
+            cost_estimate=pl.CostEstimate(flops=1_000_000_000, bytes_accessed=0, transcendentals=0),
+        )(weight, *[held(chunks[step]) for step in steps])
+
+    received = []
+    for steps in (EARLY, LATE):
+        sent = project(steps, True)
+        received.append(held(exchange(sent, "tp", tp_size, 1)))
+    kept = project(EARLY + LATE, False)
+    summed = pl.pallas_call(
+        add_kernel,
         compiler_params=pltpu.CompilerParams(vmem_limit_bytes=GRANT),
-        name="project",
-        out_shape=[in_vmem((rows, cols), bf16), in_vmem((rows, cols), bf16)],
-        in_specs=[vmem] * (kv_size + 1),
-        out_specs=[vmem, vmem],
-    )(held(output_weight), *[held(chunks[c]) for c in range(kv_size)])
-    received = exchange(sent, "tp", tp_size, 1)
-    summed = (kept.astype(f32) + received.astype(f32)).astype(bf16)
+        name="add",
+        out_shape=jax.ShapeDtypeStruct((rows, cols), bf16),
+        in_specs=[vmem] * 3,
+        out_specs=hbm,
+        scratch_shapes=[pltpu.VMEM((rows, cols), bf16), pltpu.SemaphoreType.DMA((kv_size,))],
+    )(held(kept), *received)
     return summed.reshape(seq_count, nodes, cols)
 
 

time: 29.1 us -> 29 us (level)
  Pallas kernels: 7.71 us -> 8.64 us
  starting transfers between devices: 10.3 us -> 9.48 us
  other arithmetic: 0.69 us -> 0 us
  waiting for transfers between devices: 9.92 us -> 10.4 us
    pallas_call x1 -> x4, Pallas kernels: 0.48 us -> 1.43 us  [the longest x3 0.73 us: project(): pl.pallas_call(functools.partial(project_kernel, other), compiler_params=...]
    ppermute x7 -> x8, starting transfers between devices: 10.3 us -> 9.48 us  [exchange(): return lax.ppermute(array, axis, [(i, i ^ step) for i in range(size)])]
    convert_element_type x1 -> x0, other arithmetic: 0.69 us -> none  [fast_shards(): summed = (kept.astype(f32) + received.astype(f32)).astype(bf16)]
    ppermute x7 -> x8, waiting for transfers between devices: 9.92 us -> 10.4 us  [exchange(): return lax.ppermute(array, axis, [(i, i ^ step) for i in range(size)])]
  transfers between devices with their start and end apart: 7 -> 8, of which waited for: 6 -> 6; matrix products, arithmetic and copies ran while one was open for 0% -> 0% of each run, Pallas kernels for 10% -> 13%
where the time goes in v5:
time: 29 us; the launch traced here: 28.9 us
  waiting for transfers between devices  10.4 us (36%)
  starting transfers between devices  9.48 us (33%)
  Pallas kernels  8.64 us (30%)
    ppermute x8, waiting for transfers between devices, exchange(): return lax.ppermute(array, axis, [(i, i ^ step) for i in range(size)])  10.4 us
    ppermute x8, starting transfers between devices, exchange(): return lax.ppermute(array, axis, [(i, i ^ step) for i in range(size)])  9.48 us
    pallas_call x1, Pallas kernels, fast_shards(): pl.pallas_call(functools.partial(first_kernel, kv_size), compiler_params=...  2.85 us
    pallas_call x1, Pallas kernels, fast_shards(): pl.pallas_call(functools.partial(own_kernel, tp_size, nodes), compiler_pa...  2.55 us
    pallas_call x1, Pallas kernels, fast_shards(): pl.pallas_call(functools.partial(next_kernel, step, nodes), compiler_para...  1.07 us
    pallas_call x3, Pallas kernels, project(): pl.pallas_call(functools.partial(project_kernel, other), compiler_params=...  0.73 us
    pallas_call x1, Pallas kernels, fast_shards(): pl.pallas_call(add_kernel, compiler_params=pltpu.CompilerParams(vmem_limi...  0.69 us
  transfers between devices with their start and end apart: 8, of which 6 were waited for; matrix products, arithmetic and copies ran while one was open for 0% of the time, Pallas kernels for 13%

profile of v5, /device:TPU:0, one launch (start us, length us, event | category | flops | bytes accessed | tf_op | source)
XLA Modules:
  0.0 28.9 jit_solution(4905475333560165843)
XLA Ops:
  0.0 2.8 %first.1 = (bf16[272,128]{1,0:T(8,128)(2,1)S(1)}, bf16[4,64,128]{2,1,0:T(8,128)(2,1)S(1)}, bf16[2048,512]{1,0:T(8,128)(2,1)S(1)}, f32[16,4,256]{2,1,0:T(4,128)S(1)}) custom-call(s32[16]{0:T(128)} %lengths.1, bf16[256,2048]{1,0:T(8,128)(2,1)} %bitcast.20, f32[1,2048]{1,0:T(1,128)} %bitcast.23, bf16[2048,512]{1,0:T(8,128)(2,1)} %query_weight.1, ...), custom_call_target="tpu_custom_call" | custom-call | tf_op jit(solution)/shard_map/first/pallas_call | solution.py:769
  2.9 1.1 %shard_map.181 = bf16[272,128]{1,0:T(8,128)(2,1)S(1)} custom-call(bf16[256,2048]{1,0:T(8,128)(2,1)S(1)} %bitcast.21, f32[1,2048]{1,0:T(1,128)S(1)} %bitcast.24, bf16[2048,512]{1,0:T(8,128)(2,1)S(1)} %get-tuple-element.11.query_weight.refs_2_, f32[1,128]{1,0:T(1,128)S(1)} %bitcast.27, bf16[16,256,128]{2,1,0:T(8,128)(2,1)S(1)} %bitcast.13, ...), custom_call_target="tpu_custom_call" | custom-call | tf_op jit(solution)/shard_map/pallas_call | solution.py:822
  4.0 0.0 copy-start.8
  4.0 0.0 copy-start.9
  4.0 0.0 copy-start.10
  4.0 0.0 copy-start.11
  4.0 0.0 copy-start.12
  4.1 0.0 copy-start.13
  4.1 0.0 copy-start.14
  4.1 0.0 copy-start.15
  4.1 3.1 %collective-permute-start = (bf16[272,128]{1,0:T(8,128)(2,1)S(1)}, bf16[272,128]{1,0:T(8,128)(2,1)S(1)}, u32[]{:S(2)}, u32[]{:S(2)}) collective-permute-start(bf16[272,128]{1,0:T(8,128)(2,1)S(1)} %shard_map.181), channel_id=1, source_target_pairs={{0,2},{2,0},{4,6},{6,4},{1,3},{3,1},{5,7},{7,5},{8,10},{10,8},{12,... | collective-permute-start | bytes 208904 | tf_op jit(solution)/shard_map/ppermute | solution.py:722
  7.2 0.4 %second.1 = bf16[272,128]{1,0:T(8,128)(2,1)S(1)} custom-call(bf16[4,64,128]{2,1,0:T(8,128)(2,1)S(1)} %get-tuple-element.16.queries, bf16[16,256,128]{2,1,0:T(8,128)(2,1)S(1)} %bitcast.14, bf16[16,256,128]{2,1,0:T(8,128)(2,1)S(1)} %bitcast.18, f32[16,4,256]{2,1,0:T(4,128)S(1)} %get-tuple-element.12.decays.refs_6_), custom_call_target="tpu_custom_call" | custom-call | tf_op jit(solution)/shard_map/second/pallas_call | solution.py:813
  7.7 2.5 %collective-permute-start.2 = (bf16[272,128]{1,0:T(8,128)(2,1)S(1)}, bf16[272,128]{1,0:T(8,128)(2,1)S(1)}, u32[]{:S(2)}, u32[]{:S(2)}) collective-permute-start(bf16[272,128]{1,0:T(8,128)(2,1)S(1)} %second.1), channel_id=1, source_target_pairs={{0,6},{2,4},{4,2},{6,0},{1,7},{3,5},{5,3},{7,1},{8,14},{10,12},{12... | collective-permute-start | bytes 208904 | tf_op jit(solution)/shard_map/ppermute | solution.py:722
  10.2 0.2 collective-permute-start.1
  10.5 0.0 copy-start.7
  10.5 2.6 %own.1 = (bf16[272,128]{1,0:T(8,128)(2,1)S(1)}, f32[8,64]{1,0:T(8,128)S(1)}) custom-call(s32[16]{0:T(128)S(1)} %copy-done.13, f32[8]{0:T(128)S(1)} %copy-done.14, s32[16,16]{1,0:T(8,128)S(1)} %copy-done.11, bf16[8,2048]{1,0:T(8,128)(2,1)S(1)} %bitcast.29, bf16[16,4,128]{2,1,0:T(4,128)(2,1)S(1)} %bitcast.30, bf16[16,4,128]{2,1,0:T(4,128)(2,1)S(1)} %bitcast.31, ...), custom_call_target="tpu_custom_call" | custom-call | flops 4000000000 | bytes 1000000 | tf_op jit(solution)/shard_map/own/pallas_call | solution.py:833
  13.0 1.6 %collective-permute-done.2.refs_3_ = bf16[272,128]{1,0:T(8,128)(2,1)S(1)} collective-permute-done((bf16[272,128]{1,0:T(8,128)(2,1)S(1)}, bf16[272,128]{1,0:T(8,128)(2,1)S(1)}, u32[]{:S(2)}, u32[]{:S(2)}) %collective-permute-start.2) | collective-permute-done | bytes 69664 | tf_op jit(solution)/shard_map/ppermute | solution.py:722
  14.6 2.4 %collective-permute-done.1.refs_2_ = bf16[272,128]{1,0:T(8,128)(2,1)S(1)} collective-permute-done((bf16[272,128]{1,0:T(8,128)(2,1)S(1)}, bf16[272,128]{1,0:T(8,128)(2,1)S(1)}, u32[]{:S(2)}, u32[]{:S(2)}) %collective-permute-start.1) | collective-permute-done | bytes 69664 | tf_op jit(solution)/shard_map/ppermute | solution.py:722
  17.0 0.3 %merge.1.refs_0_ = bf16[64,512]{1,0:T(8,128)(2,1)S(1)} custom-call(f32[8,64]{1,0:T(8,128)S(1)} %get-tuple-element.13.terms, bf16[272,128]{1,0:T(8,128)(2,1)S(1)} %get-tuple-element.14.refs_0_, bf16[272,128]{1,0:T(8,128)(2,1)S(1)} %collective-permute-done.refs_1_, bf16[272,128]{1,0:T(8,128)(2,1)S(1)} %collective-permute-done.1.refs_2_, ...), custom_call_target="tpu_custom_call" | custom-call | tf_op jit(solution)/shard_map/merge/pallas_call | solution.py:856
  17.3 0.0 collective-permute-start.3
  17.3 2.5 %collective-permute-start.4 = (bf16[64,512]{1,0:T(8,128)(2,1)S(1)}, bf16[64,512]{1,0:T(8,128)(2,1)S(1)}, u32[]{:S(2)}, u32[]{:S(2)}) collective-permute-start(bf16[64,512]{1,0:T(8,128)(2,1)S(1)} %merge.1.refs_0_), channel_id=1, source_target_pairs={{0,6},{2,4},{4,2},{6,0},{1,7},{3,5},{5,3},{7,1},{8,14},{10,12},{12... | collective-permute-start | bytes 196616 | tf_op jit(solution)/shard_map/ppermute | solution.py:722
  19.8 1.0 %collective-permute-start.5 = (bf16[64,512]{1,0:T(8,128)(2,1)S(1)}, bf16[64,512]{1,0:T(8,128)(2,1)S(1)}, u32[]{:S(2)}, u32[]{:S(2)}) collective-permute-start(bf16[64,512]{1,0:T(8,128)(2,1)S(1)} %merge.1.refs_0_), channel_id=1, source_target_pairs={{0,4},{2,6},{4,0},{6,2},{1,5},{3,7},{5,1},{7,3},{8,12},{10,14},{12... | collective-permute-start | bytes 196616 | tf_op jit(solution)/shard_map/ppermute | solution.py:722
  20.8 0.8 %collective-permute-done.3.refs_1_ = bf16[64,512]{1,0:T(8,128)(2,1)S(1)} collective-permute-done((bf16[64,512]{1,0:T(8,128)(2,1)S(1)}, bf16[64,512]{1,0:T(8,128)(2,1)S(1)}, u32[]{:S(2)}, u32[]{:S(2)}) %collective-permute-start.3) | collective-permute-done | bytes 65568 | tf_op jit(solution)/shard_map/ppermute | solution.py:722
  21.6 2.6 %collective-permute-done.4.refs_2_ = bf16[64,512]{1,0:T(8,128)(2,1)S(1)} collective-permute-done((bf16[64,512]{1,0:T(8,128)(2,1)S(1)}, bf16[64,512]{1,0:T(8,128)(2,1)S(1)}, u32[]{:S(2)}, u32[]{:S(2)}) %collective-permute-start.4) | collective-permute-done | bytes 65568 | tf_op jit(solution)/shard_map/ppermute | solution.py:722
  24.1 0.3 project.4
  24.4 0.1 collective-permute-start.6
  24.5 2.2 %collective-permute-done.5.refs_3_.refs_0_ = bf16[64,512]{1,0:T(8,128)(2,1)S(1)} collective-permute-done((bf16[64,512]{1,0:T(8,128)(2,1)S(1)}, bf16[64,512]{1,0:T(8,128)(2,1)S(1)}, u32[]{:S(2)}, u32[]{:S(2)}) %collective-permute-start.5) | collective-permute-done | bytes 65568 | tf_op jit(solution)/shard_map/ppermute | solution.py:722
  26.7 0.2 project.5
  26.9 0.1 collective-permute-start.7
  27.0 0.3 %project.3.kept = bf16[256,256]{1,0:T(8,128)(2,1)S(1)} custom-call(bf16[512,512]{1,0:T(8,128)(2,1)S(1)} %copy-done.7, bf16[64,512]{1,0:T(8,128)(2,1)S(1)} %merge.1.refs_0_, bf16[64,512]{1,0:T(8,128)(2,1)S(1)} %collective-permute-done.3.refs_1_, bf16[64,512]{1,0:T(8,128)(2,1)S(1)} %collective-permute-done.4.refs_2_, ...), custom_call_target="tpu_custom_call" | custom-call | flops 1000000000 | tf_op jit(solution)/shard_map/project/pallas_call | solution.py:871
  27.3 0.9 %collective-permute-done.7.late = bf16[64,256]{1,0:T(8,128)(2,1)S(1)} collective-permute-done((bf16[64,256]{1,0:T(8,128)(2,1)S(1)}, bf16[64,256]{1,0:T(8,128)(2,1)S(1)}, u32[]{:S(2)}, u32[]{:S(2)}) %collective-permute-start.7) | collective-permute-done | bytes 32800 | tf_op jit(solution)/shard_map/ppermute | solution.py:722
  28.2 0.7 %add.1 = bf16[256,256]{1,0:T(8,128)(2,1)} custom-call(bf16[256,256]{1,0:T(8,128)(2,1)S(1)} %project.3.kept, bf16[192,256]{1,0:T(8,128)(2,1)S(1)} %collective-permute-done.6.early, bf16[64,256]{1,0:T(8,128)(2,1)S(1)} %collective-permute-done.7.late), custom_call_target="tpu_custom_call" | custom-call | tf_op jit(solution)/shard_map/add/pallas_call | solution.py:886
  (25 shorter events, 0.1 us)
Async XLA Ops:
  0.0 2.9 %copy-start = (bf16[16,256,1,128]{3,1,2,0:T(8,128)(2,1)S(1)}, bf16[16,256,1,128]{3,1,2,0:T(8,128)(2,1)}, u32[]{:S(2)}) copy-start(bf16[16,256,1,128]{3,1,2,0:T(8,128)(2,1)} %param.29) | copy-start | bytes 3145732
  0.0 2.9 %copy-start.1 = (bf16[16,256,1,128]{3,1,2,0:T(8,128)(2,1)S(1)}, bf16[16,256,1,128]{3,1,2,0:T(8,128)(2,1)}, u32[]{:S(2)}) copy-start(bf16[16,256,1,128]{3,1,2,0:T(8,128)(2,1)} %param.30) | copy-start | bytes 3145732
  0.0 2.9 %copy-start.2 = (bf16[16,16,2048]{2,1,0:T(8,128)(2,1)S(1)}, bf16[16,16,2048]{2,1,0:T(8,128)(2,1)}, u32[]{:S(2)}) copy-start(bf16[16,16,2048]{2,1,0:T(8,128)(2,1)} %param.19) | copy-start | bytes 3145732
  0.0 2.9 %copy-start.3 = (f32[2048]{0:T(1024)S(1)}, f32[2048]{0:T(1024)}, u32[]{:S(2)}) copy-start(f32[2048]{0:T(1024)} %param.20) | copy-start | bytes 24580
  0.0 2.9 %copy-start.4 = (f32[128]{0:T(128)S(1)}, f32[128]{0:T(128)}, u32[]{:S(2)}) copy-start(f32[128]{0:T(128)} %param.26) | copy-start | bytes 1540
  4.0 6.4 %copy-start.5 = (bf16[2048,128]{1,0:T(8,128)(2,1)S(1)}, bf16[2048,128]{1,0:T(8,128)(2,1)}, u32[]{:S(2)}) copy-start(bf16[2048,128]{1,0:T(8,128)(2,1)} %key_weight.1) | copy-start | bytes 1572868
  4.0 6.4 %copy-start.6 = (bf16[2048,128]{1,0:T(8,128)(2,1)S(1)}, bf16[2048,128]{1,0:T(8,128)(2,1)}, u32[]{:S(2)}) copy-start(bf16[2048,128]{1,0:T(8,128)(2,1)} %value_weight.1) | copy-start | bytes 1572868
  4.0 6.4 %copy-start.8 = (bf16[2048,8]{0,1:T(8,128)(2,1)S(1)}, bf16[2048,8]{0,1:T(8,128)(2,1)}, u32[]{:S(2)}) copy-start(bf16[2048,8]{0,1:T(8,128)(2,1)} %param.24) | copy-start | bytes 98308
  4.0 6.4 %copy-start.9 = (bf16[16,4,1,128]{3,1,2,0:T(4,128)(2,1)S(1)}, bf16[16,4,1,128]{3,1,2,0:T(4,128)(2,1)}, u32[]{:S(2)}) copy-start(bf16[16,4,1,128]{3,1,2,0:T(4,128)(2,1)} %param.32) | copy-start | bytes 49156
  4.0 6.4 %copy-start.10 = (bf16[16,4,1,128]{3,1,2,0:T(4,128)(2,1)S(1)}, bf16[16,4,1,128]{3,1,2,0:T(4,128)(2,1)}, u32[]{:S(2)}) copy-start(bf16[16,4,1,128]{3,1,2,0:T(4,128)(2,1)} %param.33) | copy-start | bytes 49156
  4.0 6.4 %copy-start.11 = (s32[16,16]{1,0:T(8,128)S(1)}, s32[16,16]{1,0:T(8,128)}, u32[]{:S(2)}) copy-start(s32[16,16]{1,0:T(8,128)} %parents.1) | copy-start | bytes 3076
  4.0 6.4 %copy-start.12 = (f32[16,4,4]{0,2,1:T(4,128)S(1)}, f32[16,4,4]{0,2,1:T(4,128)}, u32[]{:S(2)}) copy-start(f32[16,4,4]{0,2,1:T(4,128)} %param.34) | copy-start | bytes 3076
  4.1 6.4 %copy-start.13 = (s32[16]{0:T(128)S(1)}, s32[16]{0:T(128)}, u32[]{:S(2)}) copy-start(s32[16]{0:T(128)} %accepted.1) | copy-start | bytes 196
  4.1 6.4 %copy-start.14 = (f32[8]{0:T(128)S(1)}, f32[8]{0:T(128)}, u32[]{:S(2)}) copy-start(f32[8]{0:T(128)} %forget_bias.1) | copy-start | bytes 100
  4.1 6.4 %copy-start.15 = (f32[128]{0:T(128)S(1)}, f32[128]{0:T(128)}, u32[]{:S(2)}) copy-start(f32[128]{0:T(128)} %param.27) | copy-start | bytes 1540
  4.1 8.9 %collective-permute-start = (bf16[272,128]{1,0:T(8,128)(2,1)S(1)}, bf16[272,128]{1,0:T(8,128)(2,1)S(1)}, u32[]{:S(2)}, u32[]{:S(2)}) collective-permute-start(bf16[272,128]{1,0:T(8,128)(2,1)S(1)} %shard_map.181), channel_id=1, source_target_pairs={{0,2},{2,0},{4,6},{6,4},{1,3},{3,1},{5,7},{7,5},{8,10},{10,8},{12,... | collective-permute-start | bytes 208904 | tf_op jit(solution)/shard_map/ppermute | solution.py:722
  7.7 6.9 %collective-permute-start.2 = (bf16[272,128]{1,0:T(8,128)(2,1)S(1)}, bf16[272,128]{1,0:T(8,128)(2,1)S(1)}, u32[]{:S(2)}, u32[]{:S(2)}) collective-permute-start(bf16[272,128]{1,0:T(8,128)(2,1)S(1)} %second.1), channel_id=1, source_target_pairs={{0,6},{2,4},{4,2},{6,0},{1,7},{3,5},{5,3},{7,1},{8,14},{10,12},{12... | collective-permute-start | bytes 208904 | tf_op jit(solution)/shard_map/ppermute | solution.py:722
  10.2 6.8 %collective-permute-start.1 = (bf16[272,128]{1,0:T(8,128)(2,1)S(1)}, bf16[272,128]{1,0:T(8,128)(2,1)S(1)}, u32[]{:S(2)}, u32[]{:S(2)}) collective-permute-start(bf16[272,128]{1,0:T(8,128)(2,1)S(1)} %get-tuple-element.15), channel_id=1, source_target_pairs={{0,4},{2,6},{4,0},{6,2},{1,5},{3,7},{5,1},{7,3},{8,12},{10,14},{12... | collective-permute-start | bytes 208904 | tf_op jit(solution)/shard_map/ppermute | solution.py:722
  10.5 13.7 %copy-start.7 = (bf16[512,512]{1,0:T(8,128)(2,1)S(1)}, bf16[512,512]{1,0:T(8,128)(2,1)}, u32[]{:S(2)}) copy-start(bf16[512,512]{1,0:T(8,128)(2,1)} %weight.5) | copy-start | bytes 1572868
  17.3 4.3 %collective-permute-start.3 = (bf16[64,512]{1,0:T(8,128)(2,1)S(1)}, bf16[64,512]{1,0:T(8,128)(2,1)S(1)}, u32[]{:S(2)}, u32[]{:S(2)}) collective-permute-start(bf16[64,512]{1,0:T(8,128)(2,1)S(1)} %merge.1.refs_0_), channel_id=1, source_target_pairs={{0,2},{2,0},{4,6},{6,4},{1,3},{3,1},{5,7},{7,5},{8,10},{10,8},{12,... | collective-permute-start | bytes 196616 | tf_op jit(solution)/shard_map/ppermute | solution.py:722
  17.3 6.8 %collective-permute-start.4 = (bf16[64,512]{1,0:T(8,128)(2,1)S(1)}, bf16[64,512]{1,0:T(8,128)(2,1)S(1)}, u32[]{:S(2)}, u32[]{:S(2)}) collective-permute-start(bf16[64,512]{1,0:T(8,128)(2,1)S(1)} %merge.1.refs_0_), channel_id=1, source_target_pairs={{0,6},{2,4},{4,2},{6,0},{1,7},{3,5},{5,3},{7,1},{8,14},{10,12},{12... | collective-permute-start | bytes 196616 | tf_op jit(solution)/shard_map/ppermute | solution.py:722
  19.8 7.0 %collective-permute-start.5 = (bf16[64,512]{1,0:T(8,128)(2,1)S(1)}, bf16[64,512]{1,0:T(8,128)(2,1)S(1)}, u32[]{:S(2)}, u32[]{:S(2)}) collective-permute-start(bf16[64,512]{1,0:T(8,128)(2,1)S(1)} %merge.1.refs_0_), channel_id=1, source_target_pairs={{0,4},{2,6},{4,0},{6,2},{1,5},{3,7},{5,1},{7,3},{8,12},{10,14},{12... | collective-permute-start | bytes 196616 | tf_op jit(solution)/shard_map/ppermute | solution.py:722
  24.4 3.8 %collective-permute-start.6 = (bf16[192,256]{1,0:T(8,128)(2,1)S(1)}, bf16[192,256]{1,0:T(8,128)(2,1)S(1)}, u32[]{:S(2)}, u32[]{:S(2)}) collective-permute-start(bf16[192,256]{1,0:T(8,128)(2,1)S(1)} %project.4), channel_id=1, source_target_pairs={{0,1},{1,0},{2,3},{3,2},{4,5},{5,4},{6,7},{7,6},{8,9},{9,8},{10,11... | collective-permute-start | bytes 294920 | tf_op jit(solution)/shard_map/ppermute | solution.py:722
  26.9 1.3 %collective-permute-start.7 = (bf16[64,256]{1,0:T(8,128)(2,1)S(1)}, bf16[64,256]{1,0:T(8,128)(2,1)S(1)}, u32[]{:S(2)}, u32[]{:S(2)}) collective-permute-start(bf16[64,256]{1,0:T(8,128)(2,1)S(1)} %project.5), channel_id=1, source_target_pairs={{0,1},{1,0},{2,3},{3,2},{4,5},{5,4},{6,7},{7,6},{8,9},{9,8},{10,11... | collective-permute-start | bytes 98312 | tf_op jit(solution)/shard_map/ppermute | solution.py:722

commit v6 on v5

--- a/solution.py
+++ b/solution.py
@@ -400,25 +400,27 @@
         )
         for i in range(depth_parts)
     ]
-    for copy in small[:3] + weight_copies + small[3:]:
+    for copy in small[:6] + weight_copies + small[6:]:
         copy.start()
 
     small[0].wait()
     for item in range(2):
         small[1 + item].wait()
         normalized(token_buf.at[item], 0, count, nodes, gain_buf[...], normed.at[pl.ds(item * count, count)])
+    for copy in small[3:6]:
+        copy.wait()
+    column = lax.broadcasted_iota(jnp.int32, (heads, block_len), 1)
+    for seq in range(seq_count):
+        valid = length_buf[seq] - place * block_len
+        decay_buf[seq] = jnp.where(column < valid, logcum_buf[seq] * LOG2E, MASKED)
     summed = None
     for part in range(depth_parts):
         weight_copies[part].wait()
         span = pl.ds(part * depth, depth)
         product = jnp.dot(normed[:, span], weight_buf[span, :], preferred_element_type=jnp.float32)
         summed = product if part == 0 else summed + product
-    for copy in small[3:]:
+    for copy in small[6:]:
         copy.wait()
-    column = lax.broadcasted_iota(jnp.int32, (heads, block_len), 1)
-    for seq in range(seq_count):
-        valid = length_buf[seq] - place * block_len
-        decay_buf[seq] = jnp.where(column < valid, logcum_buf[seq] * LOG2E, MASKED)
     queries = queries_of(summed, query_gain_buf[...], nodes)
     for item in range(group):
         second_queries[item] = queries[group + item]

time: 29 us -> 29 us (level)
  no operation moved by 1% of the time
where the time goes in v6:
time: 29 us; the launch traced here: 28.9 us
  waiting for transfers between devices  10.4 us (36%)
  starting transfers between devices  9.49 us (33%)
  Pallas kernels  8.66 us (30%)
    ppermute x8, waiting for transfers between devices, exchange(): return lax.ppermute(array, axis, [(i, i ^ step) for i in range(size)])  10.4 us
    ppermute x8, starting transfers between devices, exchange(): return lax.ppermute(array, axis, [(i, i ^ step) for i in range(size)])  9.49 us
    pallas_call x1, Pallas kernels, fast_shards(): pl.pallas_call(functools.partial(first_kernel, kv_size), compiler_params=...  2.86 us
    pallas_call x1, Pallas kernels, fast_shards(): pl.pallas_call(functools.partial(own_kernel, tp_size, nodes), compiler_pa...  2.55 us
    pallas_call x1, Pallas kernels, fast_shards(): pl.pallas_call(functools.partial(next_kernel, step, nodes), compiler_para...  1.07 us
    pallas_call x3, Pallas kernels, project(): pl.pallas_call(functools.partial(project_kernel, other), compiler_params=...  0.73 us
    pallas_call x1, Pallas kernels, fast_shards(): pl.pallas_call(add_kernel, compiler_params=pltpu.CompilerParams(vmem_limi...  0.69 us
  transfers between devices with their start and end apart: 8, of which 6 were waited for; matrix products, arithmetic and copies ran while one was open for 0% of the time, Pallas kernels for 13%

profile of v6, /device:TPU:0, one launch (start us, length us, event | category | flops | bytes accessed | tf_op | source)
XLA Modules:
  0.0 28.9 jit_solution(9553265012851264908)
XLA Ops:
  0.0 2.9 %first.1 = (bf16[272,128]{1,0:T(8,128)(2,1)S(1)}, bf16[4,64,128]{2,1,0:T(8,128)(2,1)S(1)}, bf16[2048,512]{1,0:T(8,128)(2,1)S(1)}, f32[16,4,256]{2,1,0:T(4,128)S(1)}) custom-call(s32[16]{0:T(128)} %lengths.1, bf16[256,2048]{1,0:T(8,128)(2,1)} %bitcast.20, f32[1,2048]{1,0:T(1,128)} %bitcast.23, bf16[2048,512]{1,0:T(8,128)(2,1)} %query_weight.1, ...), custom_call_target="tpu_custom_call" | custom-call | tf_op jit(solution)/shard_map/first/pallas_call | solution.py:771
  2.9 1.1 %shard_map.181 = bf16[272,128]{1,0:T(8,128)(2,1)S(1)} custom-call(bf16[256,2048]{1,0:T(8,128)(2,1)S(1)} %bitcast.21, f32[1,2048]{1,0:T(1,128)S(1)} %bitcast.24, bf16[2048,512]{1,0:T(8,128)(2,1)S(1)} %get-tuple-element.11.query_weight.refs_2_, f32[1,128]{1,0:T(1,128)S(1)} %bitcast.27, bf16[16,256,128]{2,1,0:T(8,128)(2,1)S(1)} %bitcast.13, ...), custom_call_target="tpu_custom_call" | custom-call | tf_op jit(solution)/shard_map/pallas_call | solution.py:824
  4.0 0.0 copy-start.8
  4.0 0.0 copy-start.9
  4.0 0.0 copy-start.10
  4.1 0.0 copy-start.11
  4.1 0.0 copy-start.12
  4.1 0.0 copy-start.13
  4.1 0.0 copy-start.14
  4.1 0.0 copy-start.15
  4.1 3.1 %collective-permute-start = (bf16[272,128]{1,0:T(8,128)(2,1)S(1)}, bf16[272,128]{1,0:T(8,128)(2,1)S(1)}, u32[]{:S(2)}, u32[]{:S(2)}) collective-permute-start(bf16[272,128]{1,0:T(8,128)(2,1)S(1)} %shard_map.181), channel_id=1, source_target_pairs={{0,2},{2,0},{4,6},{6,4},{1,3},{3,1},{5,7},{7,5},{8,10},{10,8},{12,... | collective-permute-start | bytes 208904 | tf_op jit(solution)/shard_map/ppermute | solution.py:724
  7.3 0.5 %second.1 = bf16[272,128]{1,0:T(8,128)(2,1)S(1)} custom-call(bf16[4,64,128]{2,1,0:T(8,128)(2,1)S(1)} %get-tuple-element.16.queries, bf16[16,256,128]{2,1,0:T(8,128)(2,1)S(1)} %bitcast.14, bf16[16,256,128]{2,1,0:T(8,128)(2,1)S(1)} %bitcast.18, f32[16,4,256]{2,1,0:T(4,128)S(1)} %get-tuple-element.12.decays.refs_6_), custom_call_target="tpu_custom_call" | custom-call | tf_op jit(solution)/shard_map/second/pallas_call | solution.py:815
  7.7 2.5 %collective-permute-start.2 = (bf16[272,128]{1,0:T(8,128)(2,1)S(1)}, bf16[272,128]{1,0:T(8,128)(2,1)S(1)}, u32[]{:S(2)}, u32[]{:S(2)}) collective-permute-start(bf16[272,128]{1,0:T(8,128)(2,1)S(1)} %second.1), channel_id=1, source_target_pairs={{0,6},{2,4},{4,2},{6,0},{1,7},{3,5},{5,3},{7,1},{8,14},{10,12},{12... | collective-permute-start | bytes 208904 | tf_op jit(solution)/shard_map/ppermute | solution.py:724
  10.2 0.2 collective-permute-start.1
  10.5 0.0 copy-start.7
  10.5 2.6 %own.1 = (bf16[272,128]{1,0:T(8,128)(2,1)S(1)}, f32[8,64]{1,0:T(8,128)S(1)}) custom-call(s32[16]{0:T(128)S(1)} %copy-done.13, f32[8]{0:T(128)S(1)} %copy-done.14, s32[16,16]{1,0:T(8,128)S(1)} %copy-done.11, bf16[8,2048]{1,0:T(8,128)(2,1)S(1)} %bitcast.29, bf16[16,4,128]{2,1,0:T(4,128)(2,1)S(1)} %bitcast.30, bf16[16,4,128]{2,1,0:T(4,128)(2,1)S(1)} %bitcast.31, ...), custom_call_target="tpu_custom_call" | custom-call | flops 4000000000 | bytes 1000000 | tf_op jit(solution)/shard_map/own/pallas_call | solution.py:835
  13.1 1.5 %collective-permute-done.2.refs_3_ = bf16[272,128]{1,0:T(8,128)(2,1)S(1)} collective-permute-done((bf16[272,128]{1,0:T(8,128)(2,1)S(1)}, bf16[272,128]{1,0:T(8,128)(2,1)S(1)}, u32[]{:S(2)}, u32[]{:S(2)}) %collective-permute-start.2) | collective-permute-done | bytes 69664 | tf_op jit(solution)/shard_map/ppermute | solution.py:724
  14.6 2.4 %collective-permute-done.1.refs_2_ = bf16[272,128]{1,0:T(8,128)(2,1)S(1)} collective-permute-done((bf16[272,128]{1,0:T(8,128)(2,1)S(1)}, bf16[272,128]{1,0:T(8,128)(2,1)S(1)}, u32[]{:S(2)}, u32[]{:S(2)}) %collective-permute-start.1) | collective-permute-done | bytes 69664 | tf_op jit(solution)/shard_map/ppermute | solution.py:724
  17.0 0.3 %merge.1.refs_0_ = bf16[64,512]{1,0:T(8,128)(2,1)S(1)} custom-call(f32[8,64]{1,0:T(8,128)S(1)} %get-tuple-element.13.terms, bf16[272,128]{1,0:T(8,128)(2,1)S(1)} %get-tuple-element.14.refs_0_, bf16[272,128]{1,0:T(8,128)(2,1)S(1)} %collective-permute-done.refs_1_, bf16[272,128]{1,0:T(8,128)(2,1)S(1)} %collective-permute-done.1.refs_2_, ...), custom_call_target="tpu_custom_call" | custom-call | tf_op jit(solution)/shard_map/merge/pallas_call | solution.py:858
  17.3 0.0 collective-permute-start.3
  17.3 2.4 %collective-permute-start.4 = (bf16[64,512]{1,0:T(8,128)(2,1)S(1)}, bf16[64,512]{1,0:T(8,128)(2,1)S(1)}, u32[]{:S(2)}, u32[]{:S(2)}) collective-permute-start(bf16[64,512]{1,0:T(8,128)(2,1)S(1)} %merge.1.refs_0_), channel_id=1, source_target_pairs={{0,6},{2,4},{4,2},{6,0},{1,7},{3,5},{5,3},{7,1},{8,14},{10,12},{12... | collective-permute-start | bytes 196616 | tf_op jit(solution)/shard_map/ppermute | solution.py:724
  19.8 1.0 %collective-permute-start.5 = (bf16[64,512]{1,0:T(8,128)(2,1)S(1)}, bf16[64,512]{1,0:T(8,128)(2,1)S(1)}, u32[]{:S(2)}, u32[]{:S(2)}) collective-permute-start(bf16[64,512]{1,0:T(8,128)(2,1)S(1)} %merge.1.refs_0_), channel_id=1, source_target_pairs={{0,4},{2,6},{4,0},{6,2},{1,5},{3,7},{5,1},{7,3},{8,12},{10,14},{12... | collective-permute-start | bytes 196616 | tf_op jit(solution)/shard_map/ppermute | solution.py:724
  20.8 0.8 %collective-permute-done.3.refs_1_ = bf16[64,512]{1,0:T(8,128)(2,1)S(1)} collective-permute-done((bf16[64,512]{1,0:T(8,128)(2,1)S(1)}, bf16[64,512]{1,0:T(8,128)(2,1)S(1)}, u32[]{:S(2)}, u32[]{:S(2)}) %collective-permute-start.3) | collective-permute-done | bytes 65568 | tf_op jit(solution)/shard_map/ppermute | solution.py:724
  21.6 2.6 %collective-permute-done.4.refs_2_ = bf16[64,512]{1,0:T(8,128)(2,1)S(1)} collective-permute-done((bf16[64,512]{1,0:T(8,128)(2,1)S(1)}, bf16[64,512]{1,0:T(8,128)(2,1)S(1)}, u32[]{:S(2)}, u32[]{:S(2)}) %collective-permute-start.4) | collective-permute-done | bytes 65568 | tf_op jit(solution)/shard_map/ppermute | solution.py:724
  24.2 0.3 project.4
  24.4 0.1 collective-permute-start.6
  24.5 2.2 %collective-permute-done.5.refs_3_.refs_0_ = bf16[64,512]{1,0:T(8,128)(2,1)S(1)} collective-permute-done((bf16[64,512]{1,0:T(8,128)(2,1)S(1)}, bf16[64,512]{1,0:T(8,128)(2,1)S(1)}, u32[]{:S(2)}, u32[]{:S(2)}) %collective-permute-start.5) | collective-permute-done | bytes 65568 | tf_op jit(solution)/shard_map/ppermute | solution.py:724
  26.7 0.2 project.5
  26.9 0.1 collective-permute-start.7
  27.0 0.3 %project.3.kept = bf16[256,256]{1,0:T(8,128)(2,1)S(1)} custom-call(bf16[512,512]{1,0:T(8,128)(2,1)S(1)} %copy-done.7, bf16[64,512]{1,0:T(8,128)(2,1)S(1)} %merge.1.refs_0_, bf16[64,512]{1,0:T(8,128)(2,1)S(1)} %collective-permute-done.3.refs_1_, bf16[64,512]{1,0:T(8,128)(2,1)S(1)} %collective-permute-done.4.refs_2_, ...), custom_call_target="tpu_custom_call" | custom-call | flops 1000000000 | tf_op jit(solution)/shard_map/project/pallas_call | solution.py:873
  27.3 0.9 %collective-permute-done.7.late = bf16[64,256]{1,0:T(8,128)(2,1)S(1)} collective-permute-done((bf16[64,256]{1,0:T(8,128)(2,1)S(1)}, bf16[64,256]{1,0:T(8,128)(2,1)S(1)}, u32[]{:S(2)}, u32[]{:S(2)}) %collective-permute-start.7) | collective-permute-done | bytes 32800 | tf_op jit(solution)/shard_map/ppermute | solution.py:724
  28.2 0.7 %add.1 = bf16[256,256]{1,0:T(8,128)(2,1)} custom-call(bf16[256,256]{1,0:T(8,128)(2,1)S(1)} %project.3.kept, bf16[192,256]{1,0:T(8,128)(2,1)S(1)} %collective-permute-done.6.early, bf16[64,256]{1,0:T(8,128)(2,1)S(1)} %collective-permute-done.7.late), custom_call_target="tpu_custom_call" | custom-call | tf_op jit(solution)/shard_map/add/pallas_call | solution.py:888
  (25 shorter events, 0.0 us)
Async XLA Ops:
  0.0 2.9 %copy-start = (bf16[16,256,1,128]{3,1,2,0:T(8,128)(2,1)S(1)}, bf16[16,256,1,128]{3,1,2,0:T(8,128)(2,1)}, u32[]{:S(2)}) copy-start(bf16[16,256,1,128]{3,1,2,0:T(8,128)(2,1)} %param.29) | copy-start | bytes 3145732
  0.0 2.9 %copy-start.1 = (bf16[16,256,1,128]{3,1,2,0:T(8,128)(2,1)S(1)}, bf16[16,256,1,128]{3,1,2,0:T(8,128)(2,1)}, u32[]{:S(2)}) copy-start(bf16[16,256,1,128]{3,1,2,0:T(8,128)(2,1)} %param.30) | copy-start | bytes 3145732
  0.0 2.9 %copy-start.2 = (bf16[16,16,2048]{2,1,0:T(8,128)(2,1)S(1)}, bf16[16,16,2048]{2,1,0:T(8,128)(2,1)}, u32[]{:S(2)}) copy-start(bf16[16,16,2048]{2,1,0:T(8,128)(2,1)} %param.19) | copy-start | bytes 3145732
  0.0 2.9 %copy-start.3 = (f32[2048]{0:T(1024)S(1)}, f32[2048]{0:T(1024)}, u32[]{:S(2)}) copy-start(f32[2048]{0:T(1024)} %param.20) | copy-start | bytes 24580
  0.0 2.9 %copy-start.4 = (f32[128]{0:T(128)S(1)}, f32[128]{0:T(128)}, u32[]{:S(2)}) copy-start(f32[128]{0:T(128)} %param.26) | copy-start | bytes 1540
  4.0 6.4 %copy-start.5 = (bf16[2048,128]{1,0:T(8,128)(2,1)S(1)}, bf16[2048,128]{1,0:T(8,128)(2,1)}, u32[]{:S(2)}) copy-start(bf16[2048,128]{1,0:T(8,128)(2,1)} %key_weight.1) | copy-start | bytes 1572868
  4.0 6.4 %copy-start.6 = (bf16[2048,128]{1,0:T(8,128)(2,1)S(1)}, bf16[2048,128]{1,0:T(8,128)(2,1)}, u32[]{:S(2)}) copy-start(bf16[2048,128]{1,0:T(8,128)(2,1)} %value_weight.1) | copy-start | bytes 1572868
  4.0 6.4 %copy-start.8 = (bf16[2048,8]{0,1:T(8,128)(2,1)S(1)}, bf16[2048,8]{0,1:T(8,128)(2,1)}, u32[]{:S(2)}) copy-start(bf16[2048,8]{0,1:T(8,128)(2,1)} %param.24) | copy-start | bytes 98308
  4.0 6.4 %copy-start.9 = (bf16[16,4,1,128]{3,1,2,0:T(4,128)(2,1)S(1)}, bf16[16,4,1,128]{3,1,2,0:T(4,128)(2,1)}, u32[]{:S(2)}) copy-start(bf16[16,4,1,128]{3,1,2,0:T(4,128)(2,1)} %param.32) | copy-start | bytes 49156
  4.0 6.4 %copy-start.10 = (bf16[16,4,1,128]{3,1,2,0:T(4,128)(2,1)S(1)}, bf16[16,4,1,128]{3,1,2,0:T(4,128)(2,1)}, u32[]{:S(2)}) copy-start(bf16[16,4,1,128]{3,1,2,0:T(4,128)(2,1)} %param.33) | copy-start | bytes 49156
  4.1 6.4 %copy-start.11 = (s32[16,16]{1,0:T(8,128)S(1)}, s32[16,16]{1,0:T(8,128)}, u32[]{:S(2)}) copy-start(s32[16,16]{1,0:T(8,128)} %parents.1) | copy-start | bytes 3076
  4.1 6.4 %copy-start.12 = (f32[16,4,4]{0,2,1:T(4,128)S(1)}, f32[16,4,4]{0,2,1:T(4,128)}, u32[]{:S(2)}) copy-start(f32[16,4,4]{0,2,1:T(4,128)} %param.34) | copy-start | bytes 3076
  4.1 6.4 %copy-start.13 = (s32[16]{0:T(128)S(1)}, s32[16]{0:T(128)}, u32[]{:S(2)}) copy-start(s32[16]{0:T(128)} %accepted.1) | copy-start | bytes 196
  4.1 6.4 %copy-start.14 = (f32[8]{0:T(128)S(1)}, f32[8]{0:T(128)}, u32[]{:S(2)}) copy-start(f32[8]{0:T(128)} %forget_bias.1) | copy-start | bytes 100
  4.1 6.4 %copy-start.15 = (f32[128]{0:T(128)S(1)}, f32[128]{0:T(128)}, u32[]{:S(2)}) copy-start(f32[128]{0:T(128)} %param.27) | copy-start | bytes 1540
  4.1 8.9 %collective-permute-start = (bf16[272,128]{1,0:T(8,128)(2,1)S(1)}, bf16[272,128]{1,0:T(8,128)(2,1)S(1)}, u32[]{:S(2)}, u32[]{:S(2)}) collective-permute-start(bf16[272,128]{1,0:T(8,128)(2,1)S(1)} %shard_map.181), channel_id=1, source_target_pairs={{0,2},{2,0},{4,6},{6,4},{1,3},{3,1},{5,7},{7,5},{8,10},{10,8},{12,... | collective-permute-start | bytes 208904 | tf_op jit(solution)/shard_map/ppermute | solution.py:724
  7.7 6.9 %collective-permute-start.2 = (bf16[272,128]{1,0:T(8,128)(2,1)S(1)}, bf16[272,128]{1,0:T(8,128)(2,1)S(1)}, u32[]{:S(2)}, u32[]{:S(2)}) collective-permute-start(bf16[272,128]{1,0:T(8,128)(2,1)S(1)} %second.1), channel_id=1, source_target_pairs={{0,6},{2,4},{4,2},{6,0},{1,7},{3,5},{5,3},{7,1},{8,14},{10,12},{12... | collective-permute-start | bytes 208904 | tf_op jit(solution)/shard_map/ppermute | solution.py:724
  10.2 6.8 %collective-permute-start.1 = (bf16[272,128]{1,0:T(8,128)(2,1)S(1)}, bf16[272,128]{1,0:T(8,128)(2,1)S(1)}, u32[]{:S(2)}, u32[]{:S(2)}) collective-permute-start(bf16[272,128]{1,0:T(8,128)(2,1)S(1)} %get-tuple-element.15), channel_id=1, source_target_pairs={{0,4},{2,6},{4,0},{6,2},{1,5},{3,7},{5,1},{7,3},{8,12},{10,14},{12... | collective-permute-start | bytes 208904 | tf_op jit(solution)/shard_map/ppermute | solution.py:724
  10.5 13.7 %copy-start.7 = (bf16[512,512]{1,0:T(8,128)(2,1)S(1)}, bf16[512,512]{1,0:T(8,128)(2,1)}, u32[]{:S(2)}) copy-start(bf16[512,512]{1,0:T(8,128)(2,1)} %weight.5) | copy-start | bytes 1572868
  17.3 4.3 %collective-permute-start.3 = (bf16[64,512]{1,0:T(8,128)(2,1)S(1)}, bf16[64,512]{1,0:T(8,128)(2,1)S(1)}, u32[]{:S(2)}, u32[]{:S(2)}) collective-permute-start(bf16[64,512]{1,0:T(8,128)(2,1)S(1)} %merge.1.refs_0_), channel_id=1, source_target_pairs={{0,2},{2,0},{4,6},{6,4},{1,3},{3,1},{5,7},{7,5},{8,10},{10,8},{12,... | collective-permute-start | bytes 196616 | tf_op jit(solution)/shard_map/ppermute | solution.py:724
  17.3 6.8 %collective-permute-start.4 = (bf16[64,512]{1,0:T(8,128)(2,1)S(1)}, bf16[64,512]{1,0:T(8,128)(2,1)S(1)}, u32[]{:S(2)}, u32[]{:S(2)}) collective-permute-start(bf16[64,512]{1,0:T(8,128)(2,1)S(1)} %merge.1.refs_0_), channel_id=1, source_target_pairs={{0,6},{2,4},{4,2},{6,0},{1,7},{3,5},{5,3},{7,1},{8,14},{10,12},{12... | collective-permute-start | bytes 196616 | tf_op jit(solution)/shard_map/ppermute | solution.py:724
  19.8 7.0 %collective-permute-start.5 = (bf16[64,512]{1,0:T(8,128)(2,1)S(1)}, bf16[64,512]{1,0:T(8,128)(2,1)S(1)}, u32[]{:S(2)}, u32[]{:S(2)}) collective-permute-start(bf16[64,512]{1,0:T(8,128)(2,1)S(1)} %merge.1.refs_0_), channel_id=1, source_target_pairs={{0,4},{2,6},{4,0},{6,2},{1,5},{3,7},{5,1},{7,3},{8,12},{10,14},{12... | collective-permute-start | bytes 196616 | tf_op jit(solution)/shard_map/ppermute | solution.py:724
  24.4 3.8 %collective-permute-start.6 = (bf16[192,256]{1,0:T(8,128)(2,1)S(1)}, bf16[192,256]{1,0:T(8,128)(2,1)S(1)}, u32[]{:S(2)}, u32[]{:S(2)}) collective-permute-start(bf16[192,256]{1,0:T(8,128)(2,1)S(1)} %project.4), channel_id=1, source_target_pairs={{0,1},{1,0},{2,3},{3,2},{4,5},{5,4},{6,7},{7,6},{8,9},{9,8},{10,11... | collective-permute-start | bytes 294920 | tf_op jit(solution)/shard_map/ppermute | solution.py:724
  26.9 1.3 %collective-permute-start.7 = (bf16[64,256]{1,0:T(8,128)(2,1)S(1)}, bf16[64,256]{1,0:T(8,128)(2,1)S(1)}, u32[]{:S(2)}, u32[]{:S(2)}) collective-permute-start(bf16[64,256]{1,0:T(8,128)(2,1)S(1)} %project.5), channel_id=1, source_target_pairs={{0,1},{1,0},{2,3},{3,2},{4,5},{5,4},{6,7},{7,6},{8,9},{9,8},{10,11... | collective-permute-start | bytes 98312 | tf_op jit(solution)/shard_map/ppermute | solution.py:724
